TPU v7x, 256 devices: a whole 4x4x8 slice. The times are simulated.
256 devices in a mesh: sp: 32 (over z, x), tp: 8 (over y, core).
Axes of the slice: x: 4, y: 4, z: 8, core: 2. Of those that a mesh axis runs over, the one named last changes fastest.
Arguments:
- tokens: bfloat16 [16384, 2048], P(('sp', 'tp')), may hold values from -6 to 6
- input_gain: bfloat16 [2048], replicated, may hold values from 0.099609375 to 1.8984375
- weight_query: bfloat16 [2048, 1024], P(None, 'tp'), may hold values from -0.125 to 0.125
- weight_key: bfloat16 [2048, 1024], P(None, 'tp'), may hold values from -0.125 to 0.125
- weight_value: bfloat16 [2048, 2048], P(None, 'tp'), may hold values from -8 to 8
- weight_outgate: bfloat16 [2048, 2048], P(None, 'tp'), may hold values from -0.125 to 0.125
- weight_ingate: bfloat16 [2048, 8], replicated, may hold values from -0.125 to 0.125
- weight_forget: bfloat16 [2048, 8], replicated, may hold values from -0.125 to 0.125
- forget_shift: float32 [16384, 8], P('sp', 'tp'), may hold values from 0 to 20
- mem_gain: bfloat16 [2048], replicated, may hold values from 0.099609375 to 1.8984375
- query_down_weight: bfloat16 [2048, 768], P(None, 'tp'), may hold values from -0.125 to 0.125
- latent_down_weight: bfloat16 [2048, 512], P(None, 'tp'), may hold values from -0.125 to 0.125
- down_rotary: bfloat16 [2048, 64], replicated, may hold values from -0.125 to 0.125
- query_gain: float32 [768], replicated, may hold values from 0.15 to 12
- latent_gain: float32 [512], replicated, may hold values from 0.15 to 12
- query_up_weight: bfloat16 [768, 1536], P(None, 'tp'), may hold values from -0.4375 to 0.4375
- key_up_weight: bfloat16 [512, 1024], P(None, 'tp'), may hold values from -0.25 to 0.25
- value_up_weight: bfloat16 [512, 1024], P(None, 'tp'), may hold values from -0.25 to 0.25
- out_memory: bfloat16 [2048, 2048], P('tp'), may hold values from -0.5 to 0.5
- out_attend: bfloat16 [1024, 2048], P('tp'), may hold values from -0.75 to 0.75
Outputs:
- mixed: bfloat16 [16384, 2048], P(('sp', 'tp'))
All inputs are finite; a program needn't handle non-finite values.
Results may differ from a plain program's by a relative error of at most 0.04.
The roundings to bfloat16 on the way count: a program that leaves them out, or rounds other values in their place, can miss the bound.
Values may be sent and summed in bfloat16 or wider, within the bound.
A program may use at most 128 MiB of HBM per device.

v0:
```python
import math

import jax
import jax.numpy as jnp
from jax import lax
from jax.sharding import Mesh
from jax.sharding import PartitionSpec as P

MEMORY_HEADS = 8
M_QK = 128
M_V = 256
PLAIN_CHANNELS = 128
ROTARY_CHANNELS = 64
VALUE_CHANNELS = 128
BLOCK = 64
SP = ("sp_0", "sp_1")
SP_TP = ("sp_0", "sp_1", "tp")


SMALL_CONSTANT = 1e-06
SOFTCAP = 15.0
ROTARY_BASE = 10000.0
PRECISE = lax.Precision.HIGHEST
FAR_BELOW = -1e30


def copy_for_each(shard, axis):
    copies = jnp.broadcast_to(shard, (lax.axis_size(axis), *shard.shape))
    return lax.all_to_all(copies, axis, split_axis=0, concat_axis=0, tiled=True)


def laid_out(tiles, dim):
    shape = list(tiles.shape[1:])
    shape[dim] *= tiles.shape[0]
    return jnp.moveaxis(tiles, 0, dim).reshape(shape)


def gather_directly(shard, axis, dim):
    tiles = copy_for_each(shard, axis)
    return laid_out(tiles, dim)


def nothing_yet(shard, identity):
    return jax.tree.map(
        lambda a, e: jnp.broadcast_to(jnp.asarray(e, a.dtype), a.shape), shard, identity
    )


def gathered_once(shard, axis):
    leaves = jax.tree.leaves(shard)
    order = sorted(range(len(leaves)), key=lambda k: -leaves[k].size)
    width = (1, *leaves[order[0]].shape)[-1]
    lines = [
        jnp.pad(leaves[k].reshape(-1), (0, -leaves[k].size % width)).reshape(-1, width)
        for k in order
    ]
    both, at, found = (lax.all_gather(jnp.concatenate(lines), axis), 0, {})
    for k, line in zip(order, lines):
        slab = both[:, at : at + len(line)].reshape(len(both), -1)
        found[k] = slab[:, : leaves[k].size].reshape(-1, *leaves[k].shape)
        at += len(line)
    numbers = iter(range(len(leaves)))
    return jax.tree.map(lambda _: found[next(numbers)], shard)


def entering(shard, axes, combine, identity):
    before = start = nothing_yet(shard, identity)
    running = shard
    for axis in reversed(axes):
        peers, index = (lax.axis_size(axis), lax.axis_index(axis))
        pieces = gathered_once(running, axis)
        inside, running = (start, start)
        for k in range(peers):
            passed = k < index
            running = combine(running, jax.tree.map(lambda part: part[k], pieces))
            inside = jax.tree.map(lambda new, old: jnp.where(passed, new, old), running, inside)
        before = combine(inside, before)
    return before


def side_by_side(arrays, axis, dim, along):
    ends, at = ([], 0)
    for a in arrays[:-1]:
        at += a.shape[along]
        ends.append(at)
    both = jnp.concatenate(arrays, axis=along)
    return tuple(jnp.split(lax.all_gather(both, axis, axis=dim, tiled=True), ends, axis=along))


def in_blocks(shard, dim, peers):
    shape = shard.shape
    tiles = shard.reshape(*shape[:dim], peers, shape[dim] // peers, *shape[dim + 1 :])
    return jnp.moveaxis(tiles, dim, 0)


def sum_at_owner(shard, axis, dim):
    tiles = in_blocks(shard, dim, lax.axis_size(axis))
    arrived = lax.all_to_all(tiles, axis, split_axis=0, concat_axis=0, tiled=True)
    return arrived.astype(jnp.float32).sum(axis=0)


def rms_scale(values, gain):
    widened = values.astype(jnp.float32)
    return (
        widened
        * lax.rsqrt(jnp.mean(widened * widened, axis=-1, keepdims=True) + SMALL_CONSTANT)
        * gain.astype(jnp.float32)
    )


def rotate(values, positions):
    halfway = values.shape[-1] // 2
    inverse = jnp.power(ROTARY_BASE, -jnp.arange(halfway, dtype=jnp.float32) / halfway)
    angles = positions.astype(jnp.float32)[:, None] * inverse
    cosine = jnp.cos(angles)
    sine_part = jnp.sin(angles)
    if values.ndim == 3:
        cosine = cosine[:, None, :]
        sine_part = sine_part[:, None, :]
    widened = values.astype(jnp.float32)
    first = widened[..., :halfway]
    second = widened[..., halfway:]
    turned = jnp.concatenate(
        [first * cosine - second * sine_part, second * cosine + first * sine_part], axis=-1
    )
    return turned.astype(jnp.bfloat16)


def update_state(carried, key_rows, value_rows, input_gate, cumulative):
    matrix, normal, stabilizer = carried
    last_total = cumulative[:, -1]
    weight_log = last_total[:, None] - cumulative + input_gate
    new_max = jnp.maximum(last_total + stabilizer, jnp.max(weight_log, axis=-1))
    weights = jnp.exp(weight_log - new_max[:, None])
    decay = jnp.exp(last_total + stabilizer - new_max)
    matrix = decay[:, None, None] * matrix + jnp.einsum(
        "hsv,hsd->hvd", weights[:, :, None] * value_rows, key_rows, precision=PRECISE
    )
    normal = decay[:, None] * normal + jnp.einsum(
        "hs,hsd->hd", weights, key_rows, precision=PRECISE
    )
    return (matrix, normal, new_max)


def block_step(carried, inputs):
    query_rows, key_rows, value_rows, input_gate, log_forget = inputs
    matrix, normal, stabilizer = carried
    cumulative = jnp.cumsum(log_forget, axis=-1)
    block_len = log_forget.shape[-1]
    causal = jnp.tril(jnp.ones((block_len, block_len), dtype=bool))
    pair_log = cumulative[:, :, None] - cumulative[:, None, :] + input_gate[:, None, :]
    pair_log = jnp.where(causal, pair_log, -jnp.inf)
    carried_log = cumulative + stabilizer[:, None]
    row_max = jnp.maximum(carried_log, jnp.max(pair_log, axis=-1))
    within = jnp.exp(pair_log - row_max[:, :, None])
    across = jnp.exp(carried_log - row_max)
    affinity = jnp.einsum("hjd,hsd->hjs", query_rows, key_rows, precision=PRECISE) * within
    numerator = jnp.einsum("hjs,hsv->hjv", affinity, value_rows, precision=PRECISE)
    numerator = numerator + across[:, :, None] * jnp.einsum(
        "hjd,hvd->hjv", query_rows, matrix, precision=PRECISE
    )
    denominator = jnp.sum(affinity, axis=-1) + across * jnp.einsum(
        "hjd,hd->hj", query_rows, normal, precision=PRECISE
    )
    output = numerator / jnp.maximum(jnp.abs(denominator), jnp.exp(-row_max))[:, :, None]
    return (update_state(carried, key_rows, value_rows, input_gate, cumulative), output)


def summary_step(carried, inputs):
    key_rows, value_rows, input_gate, log_forget = inputs
    return (
        update_state(carried, key_rows, value_rows, input_gate, jnp.cumsum(log_forget, axis=-1)),
        None,
    )


def merge_states(earlier, later):
    decayed = later[3] + earlier[2]
    joined = jnp.maximum(decayed, later[2])
    early_part = jnp.exp(decayed - joined)
    late_part = jnp.exp(later[2] - joined)
    return (
        early_part[:, None, None] * earlier[0] + late_part[:, None, None] * later[0],
        early_part[:, None] * earlier[1] + late_part[:, None] * later[1],
        joined,
        earlier[3] + later[3],
    )


def per_device(
    tokens,
    input_gain,
    weight_query,
    weight_key,
    weight_value,
    weight_outgate,
    weight_ingate,
    weight_forget,
    forget_shift,
    mem_gain,
    query_down_weight,
    latent_down_weight,
    down_rotary,
    query_gain,
    latent_gain,
    query_up_weight,
    key_up_weight,
    value_up_weight,
    out_memory,
    out_attend,
):
    normed = rms_scale(tokens, input_gain).astype(jnp.bfloat16)
    tp_index = lax.axis_index("tp")
    mem_heads = weight_query.shape[1] // M_QK
    att_heads = key_up_weight.shape[1] // PLAIN_CHANNELS
    ingate_cols = lax.dynamic_slice_in_dim(weight_ingate, tp_index * mem_heads, mem_heads, 1)
    forget_cols = lax.dynamic_slice_in_dim(weight_forget, tp_index * mem_heads, mem_heads, 1)
    weight_list = (
        weight_query,
        weight_key,
        weight_value,
        weight_outgate,
        query_down_weight,
        latent_down_weight,
        down_rotary,
        ingate_cols,
        forget_cols,
    )

    def project(portion):
        return jnp.concatenate(
            [
                jnp.dot(portion, weight, preferred_element_type=jnp.float32)
                for weight in weight_list
            ],
            axis=1,
        )

    projected = project(gather_directly(normed, "tp", 0))
    sections = []
    offset = 0
    for weight in weight_list:
        sections.append(projected[:, offset : offset + weight.shape[1]])
        offset = offset + weight.shape[1]
    stored = tuple((section.astype(jnp.bfloat16) for section in sections[:7]))
    mem_query, mem_key, mem_value, mem_outgate, query_latent, keyval_latent, key_raw = (
        lax.optimization_barrier(stored)
    )
    in_gate = SOFTCAP * jnp.tanh(sections[7] / SOFTCAP)
    log_forget = jax.nn.log_sigmoid(SOFTCAP * jnp.tanh((sections[8] + forget_shift) / SOFTCAP))
    length = projected.shape[0]
    positions = lax.axis_index(SP) * length + jnp.arange(length, dtype=jnp.int32)
    query_whole, latent_whole = (
        lax.all_gather(query_latent, "tp", axis=1, tiled=True),
        lax.all_gather(keyval_latent, "tp", axis=1, tiled=True),
    )
    normed_query = rms_scale(query_whole, query_gain).astype(jnp.bfloat16)
    normed_latent = rms_scale(latent_whole, latent_gain).astype(jnp.bfloat16)
    block_count = length // BLOCK

    def to_blocks(array, width):
        return (
            array.astype(jnp.float32)
            .reshape(block_count, BLOCK, mem_heads, width)
            .transpose(0, 2, 1, 3)
        )

    def gate_blocks(array):
        return array.reshape(block_count, BLOCK, mem_heads).transpose(0, 2, 1)

    query_blocks = to_blocks(mem_query, M_QK)
    key_blocks = to_blocks(mem_key, M_QK) * M_QK ** (-0.5)
    value_blocks = to_blocks(mem_value, M_V)
    ingate_blocks = gate_blocks(in_gate)
    forget_blocks = gate_blocks(log_forget)
    empty_state = (
        jnp.zeros((mem_heads, M_V, M_QK), jnp.float32),
        jnp.zeros((mem_heads, M_QK), jnp.float32),
        jnp.full((mem_heads,), FAR_BELOW, jnp.float32),
    )
    local_state, _ = lax.scan(
        summary_step, empty_state, (key_blocks, value_blocks, ingate_blocks, forget_blocks)
    )
    identity = empty_state + (jnp.zeros((mem_heads,), jnp.float32),)
    prefix = entering(
        (local_state[0], local_state[1], local_state[2], jnp.sum(log_forget, axis=0)),
        SP,
        merge_states,
        identity,
    )
    start_max = jnp.maximum(prefix[3], prefix[2])
    rescale = jnp.exp(prefix[2] - start_max)
    initial = (prefix[0] * rescale[:, None, None], prefix[1] * rescale[:, None], start_max)
    _, cell = lax.scan(
        block_step, initial, (query_blocks, key_blocks, value_blocks, ingate_blocks, forget_blocks)
    )
    cell = cell.transpose(0, 2, 1, 3).reshape(length, mem_heads * M_V)
    cell_total = lax.psum(jnp.sum(cell * cell, axis=1), "tp")
    gain_part = lax.dynamic_slice_in_dim(mem_gain, tp_index * mem_heads * M_V, mem_heads * M_V, 0)
    gated = (
        cell
        * lax.rsqrt(cell_total / (MEMORY_HEADS * M_V) + SMALL_CONSTANT)[:, None]
        * gain_part.astype(jnp.float32)
    )
    gated = gated * jax.nn.sigmoid(mem_outgate.astype(jnp.float32))
    gated = gated.astype(jnp.bfloat16)
    query_all = jnp.dot(normed_query, query_up_weight, preferred_element_type=jnp.float32).astype(
        jnp.bfloat16
    )
    query_all = query_all.reshape(length, att_heads, PLAIN_CHANNELS + ROTARY_CHANNELS)
    query_nope = query_all[..., :PLAIN_CHANNELS]
    query_rot = rotate(query_all[..., PLAIN_CHANNELS:], positions)
    key_rot = rotate(key_raw, positions)
    factor = (PLAIN_CHANNELS + ROTARY_CHANNELS) ** (-0.5)

    def attend_block(carried, key_nope, key_rotary, value_rows, key_start):
        row_max, summed, accum = carried
        number = key_nope.shape[0]
        key_pos = key_start + jnp.arange(number, dtype=jnp.int32)
        scores = jnp.einsum(
            "qhd,khd->hqk",
            query_nope,
            key_nope.reshape(number, att_heads, PLAIN_CHANNELS),
            preferred_element_type=jnp.float32,
        )
        scores = (
            scores
            + jnp.einsum("qhd,kd->hqk", query_rot, key_rotary, preferred_element_type=jnp.float32)
        ) * factor
        allowed = key_pos[None, :] <= positions[:, None]
        scores = jnp.where(allowed[None], scores, -jnp.inf)
        new_max = jnp.maximum(row_max, jnp.max(scores, axis=-1))
        probs = jnp.exp(scores - new_max[:, :, None])
        shrink = jnp.exp(row_max - new_max)
        summed = summed * shrink + jnp.sum(probs, axis=-1)
        accum = accum * shrink[:, :, None] + jnp.einsum(
            "hqk,khd->hqd",
            probs.astype(jnp.bfloat16),
            value_rows.reshape(number, att_heads, VALUE_CHANNELS),
            preferred_element_type=jnp.float32,
        )
        return (new_max, summed, accum)

    initial_att = (
        jnp.full((att_heads, length), FAR_BELOW, jnp.float32),
        jnp.zeros((att_heads, length), jnp.float32),
        jnp.zeros((att_heads, length, VALUE_CHANNELS), jnp.float32),
    )
    own_nope = jnp.dot(normed_latent, key_up_weight, preferred_element_type=jnp.float32).astype(
        jnp.bfloat16
    )
    own_values = jnp.dot(normed_latent, value_up_weight, preferred_element_type=jnp.float32).astype(
        jnp.bfloat16
    )
    carried = initial_att
    piece_rows = side_by_side((own_nope, key_rot, own_values), SP, 0, 1)
    number = piece_rows[0].shape[0]
    size = math.gcd(number, 1024)

    def one_block(state, block_number):
        begin = block_number * size
        sub_rows = tuple(
            (lax.dynamic_slice_in_dim(member, begin, size, 0) for member in piece_rows)
        )

        def compute(current):
            key_nope, key_rotary, value_rows = sub_rows
            return attend_block(current, key_nope, key_rotary, value_rows, begin)

        return (
            lax.cond(begin <= positions[length - 1], compute, lambda current: current, state),
            None,
        )

    carried, _ = lax.scan(one_block, carried, jnp.arange(number // size, dtype=jnp.int32))
    attended = (carried[2] / carried[1][:, :, None]).astype(jnp.bfloat16)
    attended = attended.transpose(1, 0, 2).reshape(length, att_heads * VALUE_CHANNELS)
    mixed = sum_at_owner(
        (
            jnp.dot(gated, out_memory, preferred_element_type=jnp.float32)
            + jnp.dot(attended, out_attend, preferred_element_type=jnp.float32)
        ).astype(jnp.bfloat16),
        "tp",
        0,
    )
    return mixed.astype(jnp.bfloat16)


def solution(mesh):
    torus = Mesh(mesh.devices.reshape(8, 4, mesh.shape["tp"]), ("sp_0", "sp_1", "tp"))
    in_specs = (
        P(SP_TP, None),
        P(),
        P(None, "tp"),
        P(None, "tp"),
        P(None, "tp"),
        P(None, "tp"),
        P(),
        P(),
        P(SP, "tp"),
        P(),
        P(None, "tp"),
        P(None, "tp"),
        P(),
        P(),
        P(),
        P(None, "tp"),
        P(None, "tp"),
        P(None, "tp"),
        P("tp", None),
        P("tp", None),
    )
    out_specs = P(SP_TP, None)
    return jax.shard_map(
        per_device, mesh=torus, in_specs=in_specs, out_specs=out_specs, check_vma=False
    )
```

profile of v0, /device:TPU:224, one launch (start us, length us, event | category | flops | bytes accessed | tf_op | source)
XLA Modules:
  0.0 447.8 jit_solution(11439639850587882562)
XLA Ops:
  9.5 1.6 broadcast_in_dim.36
  11.1 4.5 all-to-all-start
  15.7 27.1 %all-to-all-done = bf16[8,64,2048]{2,1,0:T(8,128)(2,1)S(1)} async-done(((bf16[8,64,2048]{2,1,0:T(8,128)(2,1)}), bf16[8,64,2048]{2,1,0:T(8,128)(2,1)S(1)}, u32[]{:S(2)}, u32[]{:S(2)}) %all-to-all-start) | async-done | bytes 2097184 | tf_op jit(solution)/shard_map/all_to_all | solution.py:29
  44.3 2.1 negate_reduce_fusion
  54.4 40.7 %while.47 = (s32[]{:T(128)}, f32[1,256,128]{2,1,0:T(8,128)S(1)}, f32[1,128]{1,0:T(1,128)S(1)}, f32[1]{0:T(128)}, f32[8,1,64]{2,1,0:T(1,128)S(1)}, /*index=5*/f32...) while((s32[]{:T(128)}, f32[1,256,128]{2,1,0:T(8,128)S(1)}, ...), condition=%wide.region_4.5_spmd.clone, body=%wide.region_1.0_spmd.clone.sunk | while | flops 25383812 | bytes 401378 | solution.py:281
  95.1 13.3 %all-gather.2 = f32[4,259,128]{2,1,0:T(8,128)S(1)} all-gather(f32[1,259,128]{2,1,0:T(8,128)S(1)} %maximum_bitcast_fusion), channel_id=2, replica_groups=mesh['sp_0'=8,'sp_1'=4,'tp'=8] {'sp_1'}, dimensions={0}, use_global_device_ids=true | all-gather | bytes 663040 | tf_op jit(solution)/shard_map/all_gather | solution.py:57
  120.4 13.1 %all_gather.25 = bf16[512,512]{0,1:T(8,128)(2,1)S(1)} all-gather(bf16[512,64]{0,1:T(8,128)(2,1)S(1)} %copy-done.8), channel_id=1, replica_groups=mesh['sp_0'=8,'sp_1'=4,'tp'=8] {'tp'}, dimensions={1}, use_global_device_ids=true | all-gather | bytes 589824 | tf_op jit(solution)/shard_map/all_gather | solution.py:255
  137.8 13.4 %all_gather.27 = bf16[512,768]{0,1:T(8,128)(2,1)S(1)} all-gather(bf16[512,96]{0,1:T(8,128)(2,1)S(1)} %convolution_convert_fusion.7), channel_id=1, replica_groups=mesh['sp_0'=8,'sp_1'=4,'tp'=8] {'tp'}, dimensions={1}, use_global_device_ids=true | all-gather | bytes 884736 | tf_op jit(solution)/shard_map/all_gather | solution.py:254
  153.3 2.3 all-gather.9.cloned.1.call-done
  179.1 1.6 fusion.110
  180.7 68.9 %while.45 = (s32[]{:T(128)}, f32[1,256,128]{2,1,0:T(8,128)S(1)}, f32[1,128]{1,0:T(1,128)S(1)}, f32[1]{0:T(128)}, f32[8,1,64,256]{3,2,1,0:T(8,128)S(1)}, /*index=...) while((s32[]{:T(128)}, f32[1,256,128]{2,1,0:T(8,128)S(1)}, ...), condition=%wide.region_11.12_spmd, body=%wide.region_6.11_spmd.sunk | while | flops 69588096 | bytes 982777 | solution.py:294
  249.8 13.4 %psum.7 = f32[512]{0:T(512)S(1)} all-reduce(f32[512]{0:T(512)S(1)} %reduce_sum.82), channel_id=1, replica_groups=mesh['sp_0'=8,'sp_1'=4,'tp'=8] {'tp'}, use_global_device_ids=true, to_apply=%region_13.14 | all-reduce | flops 512 | bytes 4096 | tf_op jit(solution)/shard_map/psum | solution.py:298
  263.4 2.8 fusion.176
  266.2 4.8 %all-gather.7.cloned.1.call-done = bf16[16384,320]{0,1:T(8,128)(2,1)} async-done(((bf16[512,320]{0,1:T(8,128)(2,1)}), bf16[16384,320]{0,1:T(8,128)(2,1)}) %all-gather.7.cloned.1.call-update) | async-done | bytes 10485776 | tf_op jit(solution)/shard_map/all_gather | solution.py:87
  270.9 6.0 %fusion.169 = (bf16[16384,128]{0,1:T(8,128)(2,1)}, bf16[16384,128]{0,1:T(8,128)(2,1)}) fusion(bf16[16384,320]{0,1:T(8,128)(2,1)} %all-gather.7.cloned.1.call-done), kind=kLoop, calls=%fused_computation.273 | loop fusion | bytes 16777216 | tf_op jit(solution)/shard_map/split | solution.py:87
  277.0 6.4 %copy.48 = bf16[16384,128]{1,0:T(8,128)(2,1)} copy(bf16[16384,128]{0,1:T(8,128)(2,1)} %get-tuple-element.494) | data formatting | bytes 8388608 | tf_op jit(solution)/shard_map/while | solution.py:375
  283.4 1.6 slice-done
  284.9 3.1 copy.47
  288.1 6.4 %copy.45 = bf16[16384,128]{1,0:T(8,128)(2,1)} copy(bf16[16384,128]{0,1:T(8,128)(2,1)} %get-tuple-element.495) | data formatting | bytes 8388608 | tf_op jit(solution)/shard_map/while | solution.py:375
  294.5 111.7 %while.46 = (s32[]{:T(128)}, f32[1,512]{1,0:T(1,128)S(1)}, f32[1,512]{1,0:T(1,128)S(1)}, f32[1,512,128]{2,1,0:T(8,128)S(1)}, s32[16]{0:T(128)S(1)}, /*index=5*/s...) while((s32[]{:T(128)}, f32[1,512]{1,0:T(1,128)S(1)}, ...), condition=%wide.region_21.22_spmd, body=%wide.region_16.21_spmd.sunk | while | flops 340396032 | bytes 12036461 | solution.py:375
  296.9 4.9 %conditional.2 = ((f32[1,512]{1,0:T(1,128)S(1)}, f32[1,512]{1,0:T(1,128)S(1)}, f32[1,512,128]{2,1,0:T(8,128)S(1)})) conditional(s32[]{:T(128)} %convert_element_type.198, (f32[1,512]{1,0:T(1,128)S(1)}, f32[1,512]{1,0:T(1,128)S(1)}, f32[1,512,128]{2,1,0:T(8,128)S(1)}) %tuple.113, (s32[]{:T(128)}, s32[512]{0:T(512)S(1)}, ...), branch_computations={%region_17.17_spmd, %region_18.20_spmd} | conditional | flops 340396032 | bytes 12036178 | solution.py:371
  304.2 4.9 %conditional.2 = ((f32[1,512]{1,0:T(1,128)S(1)}, f32[1,512]{1,0:T(1,128)S(1)}, f32[1,512,128]{2,1,0:T(8,128)S(1)})) conditional(s32[]{:T(128)} %convert_element_type.198, (f32[1,512]{1,0:T(1,128)S(1)}, f32[1,512]{1,0:T(1,128)S(1)}, f32[1,512,128]{2,1,0:T(8,128)S(1)}) %tuple.113, (s32[]{:T(128)}, s32[512]{0:T(512)S(1)}, ...), branch_computations={%region_17.17_spmd, %region_18.20_spmd} | conditional | flops 340396032 | bytes 12036178 | solution.py:371
  311.5 4.9 %conditional.2 = ((f32[1,512]{1,0:T(1,128)S(1)}, f32[1,512]{1,0:T(1,128)S(1)}, f32[1,512,128]{2,1,0:T(8,128)S(1)})) conditional(s32[]{:T(128)} %convert_element_type.198, (f32[1,512]{1,0:T(1,128)S(1)}, f32[1,512]{1,0:T(1,128)S(1)}, f32[1,512,128]{2,1,0:T(8,128)S(1)}) %tuple.113, (s32[]{:T(128)}, s32[512]{0:T(512)S(1)}, ...), branch_computations={%region_17.17_spmd, %region_18.20_spmd} | conditional | flops 340396032 | bytes 12036178 | solution.py:371
  314.8 1.5 fusion.50
  318.8 4.9 %conditional.2 = ((f32[1,512]{1,0:T(1,128)S(1)}, f32[1,512]{1,0:T(1,128)S(1)}, f32[1,512,128]{2,1,0:T(8,128)S(1)})) conditional(s32[]{:T(128)} %convert_element_type.198, (f32[1,512]{1,0:T(1,128)S(1)}, f32[1,512]{1,0:T(1,128)S(1)}, f32[1,512,128]{2,1,0:T(8,128)S(1)}) %tuple.113, (s32[]{:T(128)}, s32[512]{0:T(512)S(1)}, ...), branch_computations={%region_17.17_spmd, %region_18.20_spmd} | conditional | flops 340396032 | bytes 12036178 | solution.py:371
  322.1 1.5 fusion.50
  326.1 4.9 %conditional.2 = ((f32[1,512]{1,0:T(1,128)S(1)}, f32[1,512]{1,0:T(1,128)S(1)}, f32[1,512,128]{2,1,0:T(8,128)S(1)})) conditional(s32[]{:T(128)} %convert_element_type.198, (f32[1,512]{1,0:T(1,128)S(1)}, f32[1,512]{1,0:T(1,128)S(1)}, f32[1,512,128]{2,1,0:T(8,128)S(1)}) %tuple.113, (s32[]{:T(128)}, s32[512]{0:T(512)S(1)}, ...), branch_computations={%region_17.17_spmd, %region_18.20_spmd} | conditional | flops 340396032 | bytes 12036178 | solution.py:371
  329.4 1.5 fusion.50
  333.4 4.9 %conditional.2 = ((f32[1,512]{1,0:T(1,128)S(1)}, f32[1,512]{1,0:T(1,128)S(1)}, f32[1,512,128]{2,1,0:T(8,128)S(1)})) conditional(s32[]{:T(128)} %convert_element_type.198, (f32[1,512]{1,0:T(1,128)S(1)}, f32[1,512]{1,0:T(1,128)S(1)}, f32[1,512,128]{2,1,0:T(8,128)S(1)}) %tuple.113, (s32[]{:T(128)}, s32[512]{0:T(512)S(1)}, ...), branch_computations={%region_17.17_spmd, %region_18.20_spmd} | conditional | flops 340396032 | bytes 12036178 | solution.py:371
  336.7 1.5 fusion.50
  340.6 4.9 %conditional.2 = ((f32[1,512]{1,0:T(1,128)S(1)}, f32[1,512]{1,0:T(1,128)S(1)}, f32[1,512,128]{2,1,0:T(8,128)S(1)})) conditional(s32[]{:T(128)} %convert_element_type.198, (f32[1,512]{1,0:T(1,128)S(1)}, f32[1,512]{1,0:T(1,128)S(1)}, f32[1,512,128]{2,1,0:T(8,128)S(1)}) %tuple.113, (s32[]{:T(128)}, s32[512]{0:T(512)S(1)}, ...), branch_computations={%region_17.17_spmd, %region_18.20_spmd} | conditional | flops 340396032 | bytes 12036178 | solution.py:371
  344.0 1.5 fusion.50
  347.9 4.9 %conditional.2 = ((f32[1,512]{1,0:T(1,128)S(1)}, f32[1,512]{1,0:T(1,128)S(1)}, f32[1,512,128]{2,1,0:T(8,128)S(1)})) conditional(s32[]{:T(128)} %convert_element_type.198, (f32[1,512]{1,0:T(1,128)S(1)}, f32[1,512]{1,0:T(1,128)S(1)}, f32[1,512,128]{2,1,0:T(8,128)S(1)}) %tuple.113, (s32[]{:T(128)}, s32[512]{0:T(512)S(1)}, ...), branch_computations={%region_17.17_spmd, %region_18.20_spmd} | conditional | flops 340396032 | bytes 12036178 | solution.py:371
  351.2 1.5 fusion.50
  355.2 4.9 %conditional.2 = ((f32[1,512]{1,0:T(1,128)S(1)}, f32[1,512]{1,0:T(1,128)S(1)}, f32[1,512,128]{2,1,0:T(8,128)S(1)})) conditional(s32[]{:T(128)} %convert_element_type.198, (f32[1,512]{1,0:T(1,128)S(1)}, f32[1,512]{1,0:T(1,128)S(1)}, f32[1,512,128]{2,1,0:T(8,128)S(1)}) %tuple.113, (s32[]{:T(128)}, s32[512]{0:T(512)S(1)}, ...), branch_computations={%region_17.17_spmd, %region_18.20_spmd} | conditional | flops 340396032 | bytes 12036178 | solution.py:371
  358.5 1.5 fusion.50
  362.5 4.9 %conditional.2 = ((f32[1,512]{1,0:T(1,128)S(1)}, f32[1,512]{1,0:T(1,128)S(1)}, f32[1,512,128]{2,1,0:T(8,128)S(1)})) conditional(s32[]{:T(128)} %convert_element_type.198, (f32[1,512]{1,0:T(1,128)S(1)}, f32[1,512]{1,0:T(1,128)S(1)}, f32[1,512,128]{2,1,0:T(8,128)S(1)}) %tuple.113, (s32[]{:T(128)}, s32[512]{0:T(512)S(1)}, ...), branch_computations={%region_17.17_spmd, %region_18.20_spmd} | conditional | flops 340396032 | bytes 12036178 | solution.py:371
  369.8 4.9 %conditional.2 = ((f32[1,512]{1,0:T(1,128)S(1)}, f32[1,512]{1,0:T(1,128)S(1)}, f32[1,512,128]{2,1,0:T(8,128)S(1)})) conditional(s32[]{:T(128)} %convert_element_type.198, (f32[1,512]{1,0:T(1,128)S(1)}, f32[1,512]{1,0:T(1,128)S(1)}, f32[1,512,128]{2,1,0:T(8,128)S(1)}) %tuple.113, (s32[]{:T(128)}, s32[512]{0:T(512)S(1)}, ...), branch_computations={%region_17.17_spmd, %region_18.20_spmd} | conditional | flops 340396032 | bytes 12036178 | solution.py:371
  373.1 1.5 fusion.50
  377.1 4.9 %conditional.2 = ((f32[1,512]{1,0:T(1,128)S(1)}, f32[1,512]{1,0:T(1,128)S(1)}, f32[1,512,128]{2,1,0:T(8,128)S(1)})) conditional(s32[]{:T(128)} %convert_element_type.198, (f32[1,512]{1,0:T(1,128)S(1)}, f32[1,512]{1,0:T(1,128)S(1)}, f32[1,512,128]{2,1,0:T(8,128)S(1)}) %tuple.113, (s32[]{:T(128)}, s32[512]{0:T(512)S(1)}, ...), branch_computations={%region_17.17_spmd, %region_18.20_spmd} | conditional | flops 340396032 | bytes 12036178 | solution.py:371
  384.3 4.9 %conditional.2 = ((f32[1,512]{1,0:T(1,128)S(1)}, f32[1,512]{1,0:T(1,128)S(1)}, f32[1,512,128]{2,1,0:T(8,128)S(1)})) conditional(s32[]{:T(128)} %convert_element_type.198, (f32[1,512]{1,0:T(1,128)S(1)}, f32[1,512]{1,0:T(1,128)S(1)}, f32[1,512,128]{2,1,0:T(8,128)S(1)}) %tuple.113, (s32[]{:T(128)}, s32[512]{0:T(512)S(1)}, ...), branch_computations={%region_17.17_spmd, %region_18.20_spmd} | conditional | flops 340396032 | bytes 12036178 | solution.py:371
  387.7 1.5 fusion.50
  391.6 4.9 %conditional.2 = ((f32[1,512]{1,0:T(1,128)S(1)}, f32[1,512]{1,0:T(1,128)S(1)}, f32[1,512,128]{2,1,0:T(8,128)S(1)})) conditional(s32[]{:T(128)} %convert_element_type.198, (f32[1,512]{1,0:T(1,128)S(1)}, f32[1,512]{1,0:T(1,128)S(1)}, f32[1,512,128]{2,1,0:T(8,128)S(1)}) %tuple.113, (s32[]{:T(128)}, s32[512]{0:T(512)S(1)}, ...), branch_computations={%region_17.17_spmd, %region_18.20_spmd} | conditional | flops 340396032 | bytes 12036178 | solution.py:371
  395.0 1.5 fusion.50
  398.9 4.9 %conditional.2 = ((f32[1,512]{1,0:T(1,128)S(1)}, f32[1,512]{1,0:T(1,128)S(1)}, f32[1,512,128]{2,1,0:T(8,128)S(1)})) conditional(s32[]{:T(128)} %convert_element_type.198, (f32[1,512]{1,0:T(1,128)S(1)}, f32[1,512]{1,0:T(1,128)S(1)}, f32[1,512,128]{2,1,0:T(8,128)S(1)}) %tuple.113, (s32[]{:T(128)}, s32[512]{0:T(512)S(1)}, ...), branch_computations={%region_17.17_spmd, %region_18.20_spmd} | conditional | flops 340396032 | bytes 12036178 | solution.py:371
  402.2 1.5 fusion.50
  406.2 3.0 add_convert_fusion
  409.2 30.7 %all_to_all.10 = bf16[8,64,2048]{2,1,0:T(8,128)(2,1)S(1)} all-to-all(bf16[8,64,2048]{2,1,0:T(8,128)(2,1)S(1)} %bitcast.447), channel_id=1, replica_groups=mesh['sp_0'=8,'sp_1'=4,'tp'=8] {'tp'}, dimensions={0} | all-to-all | bytes 4194304 | tf_op jit(solution)/shard_map/all_to_all | solution.py:98
  (404 shorter events, 186.7 us)
Async XLA Ops:
  6.5 256.9 %copy-start = (bf16[256,2048]{1,0:T(8,128)(2,1)S(1)}, bf16[256,2048]{1,0:T(8,128)(2,1)}, u32[]{:S(2)}) copy-start(bf16[256,2048]{1,0:T(8,128)(2,1)} %param.46) | copy-start | bytes 3145732
  11.1 31.6 %all-to-all-start = ((bf16[8,64,2048]{2,1,0:T(8,128)(2,1)}), bf16[8,64,2048]{2,1,0:T(8,128)(2,1)S(1)}, u32[]{:S(2)}, u32[]{:S(2)}) async-start(bf16[8,64,2048]{2,1,0:T(8,128)(2,1)} %broadcast_in_dim.36), calls=%async_computation | async-start | bytes 4194304 | tf_op jit(solution)/shard_map/all_to_all | solution.py:29
  15.6 28.7 %copy-start.10 = (f32[512,1]{0,1:T(1,128)S(1)}, f32[512,1]{0,1:T(1,128)}, u32[]{:S(2)}) copy-start(f32[512,1]{0,1:T(1,128)} %param.36) | copy-start | bytes 6148
  15.6 139.9 %all-gather.9.cloned.1.call-start = ((), (), s32[]{:S(2)}) async-start(), calls=%async_computation.3 | async-start | bytes 1216512 | tf_op jit(solution)/shard_map/all_gather | solution.py:57
  42.8 4.3 copy-start.5
  47.1 1.4 copy-start.6
  47.1 2.8 copy-start.4
  48.5 2.2 copy-start.1
  49.9 1.5 copy-start.2
  50.7 1.5 copy-start.11
  52.1 1.4 copy-start.12
  54.4 66.0 %copy-start.9 = (bf16[512,64]{0,1:T(8,128)(2,1)S(1)}, bf16[512,64]{0,1:T(8,128)(2,1)}, u32[]{:S(2)}) copy-start(bf16[512,64]{0,1:T(8,128)(2,1)} %convolution_convert_fusion.8) | copy-start | bytes 196612
  54.4 66.0 %copy-start.8 = (bf16[512,64]{0,1:T(8,128)(2,1)S(1)}, bf16[512,64]{0,1:T(8,128)(2,1)}, u32[]{:S(2)}) copy-start(bf16[512,64]{0,1:T(8,128)(2,1)} %convolution_convert_fusion.9) | copy-start | bytes 196612
  95.0 39.0 %copy-start.13 = (bf16[512,128]{1,0:T(8,128)(2,1)S(1)}, bf16[512,128]{1,0:T(8,128)(2,1)}, u32[]{:S(2)}) copy-start(bf16[512,128]{1,0:T(8,128)(2,1)} %param.45) | copy-start | bytes 393220
  95.1 39.0 %copy-start.16 = (f32[512]{0:T(512)S(1)}, f32[512]{0:T(512)}, u32[]{:S(2)}) copy-start(f32[512]{0:T(512)} %param.42) | copy-start | bytes 6148
  108.4 26.0 %copy-start.14 = (bf16[512,128]{1,0:T(8,128)(2,1)S(1)}, bf16[512,128]{1,0:T(8,128)(2,1)}, u32[]{:S(2)}) copy-start(bf16[512,128]{1,0:T(8,128)(2,1)} %param.44) | copy-start | bytes 393220
  120.3 150.6 %all-gather.7.cloned.1.call-start = ((), (), s32[]{:S(2)}) async-start(), calls=%async_computation.2 | async-start | bytes 10813440 | tf_op jit(solution)/shard_map/all_gather | solution.py:87
  134.4 17.0 %copy-start.15 = (f32[768]{0:T(1024)S(1)}, f32[768]{0:T(1024)}, u32[]{:S(2)}) copy-start(f32[768]{0:T(1024)} %param.41) | copy-start | bytes 9220
  180.6 82.6 %copy-start.7 = (bf16[512,256]{1,0:T(8,128)(2,1)S(1)}, bf16[512,256]{1,0:T(8,128)(2,1)}, u32[]{:S(2)}) copy-start(bf16[512,256]{1,0:T(8,128)(2,1)} %convolution_convert_fusion) | copy-start | bytes 786436
  283.4 1.6 slice-start
  294.5 111.7 %copy-start.3 = (bf16[128,2048]{1,0:T(8,128)(2,1)S(1)}, bf16[128,2048]{1,0:T(8,128)(2,1)}, u32[]{:S(2)}) copy-start(bf16[128,2048]{1,0:T(8,128)(2,1)} %param.47) | copy-start | bytes 1572868
Sparse Core Ops, SparseCore 0:
  120.4 35.0 all-gather.8
  158.0 112.9 all-gather.6
where the time goes:
time: 457 us; the launch traced here: 448 us
  matrix products  130 us (28%)
  blocking collectives  83.8 us (18%)
  local copies, waits for them, and re-layouts  57.2 us (13%)
  other arithmetic  50.9 us (11%)
  between operations  45.9 us (10%)
  loops' own time  41.5 us (9%)
  waiting for transfers between devices  34.1 us (7%)
    all_to_all x1, blocking collectives, sum_at_owner(): lax.all_to_all(tiles, axis, split_axis=0, concat_axis=0, tiled=True)  30.7 us
    all_to_all x1, waiting for transfers between devices, copy_for_each(): return lax.all_to_all(copies, axis, split_axis=0, concat_axis=0, tiled=True)  27.1 us
    dot_general x15, matrix products, attend_block(): jnp.einsum('hqk,khd->hqd', probs.astype(jnp.bfloat16), value_rows.reshape...  22.9 us
    dot_general x15, matrix products, attend_block(): jnp.einsum('qhd,kd->hqk', query_rot, key_rotary, preferred_element_type=j...  22.4 us
    dot_general x15, matrix products, attend_block(): jnp.einsum('qhd,khd->hqk', query_nope, key_nope.reshape(number, att_heads...  21 us
    another operation x1, loops' own time, per_device(): lax.scan(one_block, carried, jnp.arange(number // size, dtype=jnp.int32))  20 us
    reduce_max x16, other arithmetic, update_state(): new_max = jnp.maximum(last_total + stabilizer, jnp.max(weight_log, axis=-1))  19.6 us
    while x4, local copies, waits for them, and re-layouts, per_device(): lax.scan(one_block, carried, jnp.arange(number // size, dtype=jnp.int32))  16 us
  transfers between devices with their start and end apart: 3, of which 3 were waited for; matrix products, arithmetic and copies ran while one was open for 16% of the time, Pallas kernels for 0%

commit v1 on v0

v1 whole, which is shorter than its diff:
```python
import jax
import jax.numpy as jnp
from jax import lax
from jax.experimental import pallas as pl
from jax.experimental.pallas import tpu as pltpu
from jax.sharding import Mesh
from jax.sharding import PartitionSpec as P

MEMORY_HEADS = 8
M_QK = 128
M_V = 256
PLAIN_CHANNELS = 128
ROTARY_CHANNELS = 64
VALUE_CHANNELS = 128
BLOCK = 64
SP = ("z", "x")
TP = ("y", "c")
SP_TP = ("z", "x", "y", "c")


SMALL_CONSTANT = 1e-06
SOFTCAP = 15.0
ROTARY_BASE = 10000.0
PRECISE = lax.Precision.HIGHEST
FAR_BELOW = -1e30


def copy_for_each(shard, axis):
    copies = jnp.broadcast_to(shard, (lax.axis_size(axis), *shard.shape))
    return lax.all_to_all(copies, axis, split_axis=0, concat_axis=0, tiled=True)


def laid_out(tiles, dim):
    shape = list(tiles.shape[1:])
    shape[dim] *= tiles.shape[0]
    return jnp.moveaxis(tiles, 0, dim).reshape(shape)


def gather_directly(shard, axis, dim):
    tiles = copy_for_each(shard, axis)
    return laid_out(tiles, dim)


def nothing_yet(shard, identity):
    return jax.tree.map(
        lambda a, e: jnp.broadcast_to(jnp.asarray(e, a.dtype), a.shape), shard, identity
    )


def gathered_once(shard, axis):
    leaves = jax.tree.leaves(shard)
    order = sorted(range(len(leaves)), key=lambda k: -leaves[k].size)
    width = (1, *leaves[order[0]].shape)[-1]
    lines = [
        jnp.pad(leaves[k].reshape(-1), (0, -leaves[k].size % width)).reshape(-1, width)
        for k in order
    ]
    both, at, found = (lax.all_gather(jnp.concatenate(lines), axis), 0, {})
    for k, line in zip(order, lines):
        slab = both[:, at : at + len(line)].reshape(len(both), -1)
        found[k] = slab[:, : leaves[k].size].reshape(-1, *leaves[k].shape)
        at += len(line)
    numbers = iter(range(len(leaves)))
    return jax.tree.map(lambda _: found[next(numbers)], shard)


def entering(shard, axes, combine, identity):
    before = start = nothing_yet(shard, identity)
    running = shard
    for axis in reversed(axes):
        peers, index = (lax.axis_size(axis), lax.axis_index(axis))
        pieces = gathered_once(running, axis)
        inside, running = (start, start)
        for k in range(peers):
            passed = k < index
            running = combine(running, jax.tree.map(lambda part: part[k], pieces))
            inside = jax.tree.map(lambda new, old: jnp.where(passed, new, old), running, inside)
        before = combine(inside, before)
    return before


def in_blocks(shard, dim, peers):
    shape = shard.shape
    tiles = shard.reshape(*shape[:dim], peers, shape[dim] // peers, *shape[dim + 1 :])
    return jnp.moveaxis(tiles, dim, 0)


def sum_at_owner(shard, axis, dim):
    tiles = in_blocks(shard, dim, lax.axis_size(axis))
    arrived = lax.all_to_all(tiles, axis, split_axis=0, concat_axis=0, tiled=True)
    return arrived.astype(jnp.float32).sum(axis=0)


def rms_scale(values, gain):
    widened = values.astype(jnp.float32)
    return (
        widened
        * lax.rsqrt(jnp.mean(widened * widened, axis=-1, keepdims=True) + SMALL_CONSTANT)
        * gain.astype(jnp.float32)
    )


def rotate(values, positions):
    halfway = values.shape[-1] // 2
    inverse = jnp.power(ROTARY_BASE, -jnp.arange(halfway, dtype=jnp.float32) / halfway)
    angles = positions.astype(jnp.float32)[:, None] * inverse
    cosine = jnp.cos(angles)
    sine_part = jnp.sin(angles)
    if values.ndim == 3:
        cosine = cosine[:, None, :]
        sine_part = sine_part[:, None, :]
    widened = values.astype(jnp.float32)
    first = widened[..., :halfway]
    second = widened[..., halfway:]
    turned = jnp.concatenate(
        [first * cosine - second * sine_part, second * cosine + first * sine_part], axis=-1
    )
    return turned.astype(jnp.bfloat16)


def merge_states(earlier, later):
    decayed = later[3] + earlier[2]
    joined = jnp.maximum(decayed, later[2])
    early_part = jnp.exp(decayed - joined)
    late_part = jnp.exp(later[2] - joined)
    return (
        early_part[:, None, None] * earlier[0] + late_part[:, None, None] * later[0],
        early_part[:, None] * earlier[1] + late_part[:, None] * later[1],
        joined,
        earlier[3] + later[3],
    )


LOG2E = 1.4426950408889634
N_Z = 8
N_X = 4
ROWS = 512
MESH_ID = pl.DeviceIdType.MESH
CONTRACT_LAST = (((1,), (1,)), ((), ()))


def attend_kernel(
    q_ref,
    kv_ref,
    o_ref,
    q_all,
    kv_all,
    k_cat,
    top,
    total,
    accum,
    part_out,
    stat_out,
    part_in,
    stat_in,
    q_send,
    q_recv,
    up_send,
    up_recv,
    down_send,
    down_recv,
    part_send,
    part_recv,
    stat_send,
    stat_recv,
):
    z = lax.axis_index("z")
    x = lax.axis_index("x")
    above, below = lax.rem(z + 1, N_Z), lax.rem(z + N_Z - 1, N_Z)
    peers = [lax.rem(x + d, N_X) for d in range(1, N_X)]

    barrier = pltpu.get_barrier_semaphore()
    for other in (above, below):
        pl.semaphore_signal(barrier, inc=1, device_id={"z": other}, device_id_type=MESH_ID)
    for other in peers:
        pl.semaphore_signal(barrier, inc=1, device_id={"x": other}, device_id_type=MESH_ID)
    pl.semaphore_wait(barrier, N_X + 1)

    half = kv_ref.shape[0] // 2
    width = PLAIN_CHANNELS

    def kv_copy(up, step, h):
        shift = (N_Z - step + 1) if up else (step - 1)
        owner = lax.rem(z + shift, N_Z)
        rows = pl.ds(h * half, half)
        source = kv_ref.at[rows] if step == 1 else kv_all.at[owner, rows]
        send, recv = (up_send, up_recv) if up else (down_send, down_recv)
        return pltpu.make_async_remote_copy(
            src_ref=source,
            dst_ref=kv_all.at[owner, rows],
            send_sem=send.at[step - 1, h],
            recv_sem=recv.at[step - 1, h],
            device_id={"z": above if up else below},
            device_id_type=MESH_ID,
        )

    def q_copy(d):
        return pltpu.make_async_remote_copy(
            src_ref=q_ref,
            dst_ref=q_all.at[x],
            send_sem=q_send.at[d],
            recv_sem=q_recv.at[d],
            device_id={"x": peers[d]},
            device_id_type=MESH_ID,
        )

    def part_copy(d):
        return pltpu.make_async_remote_copy(
            src_ref=part_out.at[d],
            dst_ref=part_in.at[d],
            send_sem=part_send.at[d],
            recv_sem=part_recv.at[d],
            device_id={"x": peers[d]},
            device_id_type=MESH_ID,
        )

    def stat_copy(d):
        return pltpu.make_async_remote_copy(
            src_ref=stat_out.at[d],
            dst_ref=stat_in.at[d],
            send_sem=stat_send.at[d],
            recv_sem=stat_recv.at[d],
            device_id={"x": peers[d]},
            device_id_type=MESH_ID,
        )

    started = []
    for h in range(2):
        for up in (True, False):
            copy = kv_copy(up, 1, h)
            copy.start()
            started.append(copy)
    for d in range(N_X - 1):
        copy = q_copy(d)
        copy.start()
        started.append(copy)

    q_all[x] = q_ref[...]
    top[...] = jnp.full(top.shape, FAR_BELOW, jnp.float32)
    total[...] = jnp.zeros(total.shape, jnp.float32)
    accum[...] = jnp.zeros(accum.shape, jnp.float32)

    lane = lax.broadcasted_iota(jnp.int32, (ROWS // 2, width), 1)
    low = (lane < ROTARY_CHANNELS).astype(jnp.bfloat16)
    high = (lane >= ROTARY_CHANNELS).astype(jnp.bfloat16)
    scale = LOG2E * (PLAIN_CHANNELS + ROTARY_CHANNELS) ** (-0.5)
    tall = 256

    def keys_from(ref):
        k_cat[:, :width] = ref[:ROWS]
        packed = ref[2 * ROWS :]
        k_cat[: ROWS // 2, width:] = packed * low
        k_cat[ROWS // 2 :, width:] = packed * high

    def attend(first, last, values, masked):
        def one(t, carry):
            shard = t // (ROWS // tall)
            rows = pl.ds(pl.multiple_of(t * tall, tall), tall)
            inner = pl.ds(pl.multiple_of((t % (ROWS // tall)) * tall, tall), tall)
            queries = q_all[shard, inner]
            scores = lax.dot_general(
                queries, k_cat[...], CONTRACT_LAST, preferred_element_type=jnp.float32
            )
            scores = scores * scale
            if masked:
                row = lax.broadcasted_iota(jnp.int32, scores.shape, 0) + t * tall
                col = lax.broadcasted_iota(jnp.int32, scores.shape, 1) + x * ROWS
                scores = jnp.where(col <= row, scores, -jnp.inf)
            old = top[rows]
            new = jnp.maximum(old, jnp.max(scores, axis=1, keepdims=True))
            probs = jnp.exp2(scores - new[:, :1])
            shrink = jnp.exp2(old - new)
            total[rows] = total[rows] * shrink + jnp.sum(probs, axis=1, keepdims=True)
            accum[rows] = accum[rows] * shrink + jnp.dot(
                probs.astype(jnp.bfloat16), values(), preferred_element_type=jnp.float32
            )
            top[rows] = new
            return carry

        lax.fori_loop(first, last, one, 0)

    steps = ROWS // tall
    keys_from(kv_ref)
    own_values = lambda: kv_ref[ROWS : 2 * ROWS]
    attend(x * steps, (x + 1) * steps, own_values, True)
    for d in range(N_X - 1):
        q_copy(d).wait_recv()
    attend((x + 1) * steps, N_X * steps, own_values, False)

    def arrived(owner, useful):
        @pl.when(useful)
        def _():
            keys_from(kv_all.at[owner])
            attend(0, N_X * steps, lambda: kv_all[owner, ROWS : 2 * ROWS], False)

    last = N_Z // 2
    for step in range(1, last + 1):
        for h in range(2):
            for up in (True, False):
                if step == last and up != (h == 0):
                    continue
                kv_copy(up, step, h).wait_recv()
                if step < last - 1 or (step == last - 1 and up == (h == 0)):
                    copy = kv_copy(up, step + 1, h)
                    copy.start()
                    started.append(copy)
        if step < last:
            arrived(lax.rem(z + N_Z - step, N_Z), z >= step)
            arrived(lax.rem(z + step, N_Z), z + step >= N_Z)
        else:
            arrived(lax.rem(z + step, N_Z), z >= step)

    def finish(shard):
        rows = pl.ds(pl.multiple_of(shard * ROWS, ROWS), ROWS)
        summed = jnp.maximum(total[rows], 1.0)
        seen = total[rows] > 0.0
        log_total = jnp.where(seen, top[rows] + jnp.log2(summed), FAR_BELOW)
        return accum[rows] / summed, log_total

    for d in range(N_X - 1):
        part, log_total = finish(peers[d])
        part_out[d] = part.astype(jnp.bfloat16)
        stat_out[d] = log_total.T[:8]
        for copy in (part_copy(d), stat_copy(d)):
            copy.start()
            started.append(copy)
    own, own_log = finish(x)
    parts, logs = [], []
    for d in range(N_X - 1):
        part_copy(d).wait_recv()
        stat_copy(d).wait_recv()
        logs.append(jnp.broadcast_to(stat_in[d, 0:1, :], (width, ROWS)).T)
    highest = own_log
    for one in logs:
        highest = jnp.maximum(highest, one)
    weight = jnp.exp2(own_log - highest)
    numerator = own * weight
    denominator = weight
    for d in range(N_X - 1):
        weight = jnp.exp2(logs[d] - highest)
        numerator = numerator + part_in[d].astype(jnp.float32) * weight
        denominator = denominator + weight
    o_ref[...] = (numerator / denominator).astype(jnp.bfloat16)
    for copy in started:
        copy.wait_send()


def attend(queries, keys_values):
    f32, bf16 = jnp.float32, jnp.bfloat16
    last = N_Z // 2
    dma = pltpu.SemaphoreType.DMA
    return pl.pallas_call(
        attend_kernel,
        out_shape=jax.ShapeDtypeStruct((ROWS, VALUE_CHANNELS), bf16),
        in_specs=[pl.BlockSpec(memory_space=pltpu.VMEM)] * 2,
        out_specs=pl.BlockSpec(memory_space=pltpu.VMEM),
        scratch_shapes=[
            pltpu.VMEM((N_X, ROWS, 256), bf16),
            pltpu.VMEM((N_Z, *keys_values.shape), bf16),
            pltpu.VMEM((ROWS, 256), bf16),
            pltpu.VMEM((N_X * ROWS, 128), f32),
            pltpu.VMEM((N_X * ROWS, 128), f32),
            pltpu.VMEM((N_X * ROWS, VALUE_CHANNELS), f32),
            pltpu.VMEM((N_X - 1, ROWS, VALUE_CHANNELS), bf16),
            pltpu.VMEM((N_X - 1, 8, ROWS), f32),
            pltpu.VMEM((N_X - 1, ROWS, VALUE_CHANNELS), bf16),
            pltpu.VMEM((N_X - 1, 8, ROWS), f32),
            dma((N_X - 1,)),
            dma((N_X - 1,)),
            dma((last, 2)),
            dma((last, 2)),
            dma((last, 2)),
            dma((last, 2)),
            dma((N_X - 1,)),
            dma((N_X - 1,)),
            dma((N_X - 1,)),
            dma((N_X - 1,)),
        ],
        compiler_params=pltpu.CompilerParams(
            collective_id=1, has_side_effects=True, vmem_limit_bytes=48 * 1024 * 1024
        ),
        cost_estimate=pl.CostEstimate(
            flops=4 * 10**9, bytes_accessed=10**7, transcendentals=4 * 10**6
        ),
        name="attend",
    )(queries, keys_values)


def per_device(
    tokens,
    input_gain,
    weight_query,
    weight_key,
    weight_value,
    weight_outgate,
    weight_ingate,
    weight_forget,
    forget_shift,
    mem_gain,
    query_down_weight,
    latent_down_weight,
    down_rotary,
    query_gain,
    latent_gain,
    query_up_weight,
    key_up_weight,
    value_up_weight,
    out_memory,
    out_attend,
):
    normed = rms_scale(tokens, input_gain).astype(jnp.bfloat16)
    tp_index = lax.axis_index(TP)
    mem_heads = weight_query.shape[1] // M_QK
    att_heads = key_up_weight.shape[1] // PLAIN_CHANNELS
    ingate_cols = lax.dynamic_slice_in_dim(weight_ingate, tp_index * mem_heads, mem_heads, 1)
    forget_cols = lax.dynamic_slice_in_dim(weight_forget, tp_index * mem_heads, mem_heads, 1)
    weight_list = (
        weight_query,
        weight_key,
        weight_value,
        weight_outgate,
        query_down_weight,
        latent_down_weight,
        down_rotary,
        ingate_cols,
        forget_cols,
    )

    def project(portion):
        return jnp.concatenate(
            [
                jnp.dot(portion, weight, preferred_element_type=jnp.float32)
                for weight in weight_list
            ],
            axis=1,
        )

    projected = project(gather_directly(normed, TP, 0))
    sections = []
    offset = 0
    for weight in weight_list:
        sections.append(projected[:, offset : offset + weight.shape[1]])
        offset = offset + weight.shape[1]
    stored = tuple((section.astype(jnp.bfloat16) for section in sections[:7]))
    mem_query, mem_key, mem_value, mem_outgate, query_latent, keyval_latent, key_raw = (
        lax.optimization_barrier(stored)
    )
    in_gate = SOFTCAP * jnp.tanh(sections[7] / SOFTCAP)
    log_forget = jax.nn.log_sigmoid(SOFTCAP * jnp.tanh((sections[8] + forget_shift) / SOFTCAP))
    length = projected.shape[0]
    positions = lax.axis_index(SP) * length + jnp.arange(length, dtype=jnp.int32)
    query_whole, latent_whole = (
        lax.all_gather(query_latent, TP, axis=1, tiled=True),
        lax.all_gather(keyval_latent, TP, axis=1, tiled=True),
    )
    normed_query = rms_scale(query_whole, query_gain).astype(jnp.bfloat16)
    normed_latent = rms_scale(latent_whole, latent_gain).astype(jnp.bfloat16)
    cumulative = jnp.cumsum(log_forget[:, 0])
    relative = in_gate[:, 0] - cumulative
    running = lax.cummax(relative)
    ends_at = running[-1]
    key_scale = M_QK ** (-0.5)
    wide_value = mem_value.astype(jnp.float32)
    weights = jnp.exp(relative - ends_at) * key_scale
    local_matrix = lax.dot_general(
        weights[:, None] * wide_value,
        mem_key.astype(jnp.float32),
        (((0,), (0,)), ((), ())),
        precision=PRECISE,
    )
    local_normal = jnp.sum(weights[:, None] * mem_key.astype(jnp.float32), axis=0)
    local_state = (
        local_matrix[None],
        local_normal[None],
        (cumulative[-1] + ends_at)[None],
        cumulative[-1:],
    )
    identity = (
        jnp.zeros((mem_heads, M_V, M_QK), jnp.float32),
        jnp.zeros((mem_heads, M_QK), jnp.float32),
        jnp.full((mem_heads,), FAR_BELOW, jnp.float32),
        jnp.zeros((mem_heads,), jnp.float32),
    )
    prefix = entering(local_state, SP, merge_states, identity)
    start_max = jnp.maximum(prefix[3], prefix[2])
    rescale = jnp.exp(prefix[2] - start_max)
    start_matrix = (prefix[0] * rescale[:, None, None])[0]
    start_normal = (prefix[1] * rescale[:, None])[0]
    highest = jnp.maximum(start_max[0], running)
    causal = jnp.tril(jnp.ones((length, length), dtype=bool))
    within = jnp.where(causal, relative[None, :] - highest[:, None], -jnp.inf)
    affinity = lax.dot_general(
        mem_query, mem_key, (((1,), (1,)), ((), ())), preferred_element_type=jnp.float32
    )
    affinity = affinity * (jnp.exp(within) * key_scale)
    across = jnp.exp(start_max[0] - highest)
    wide_query = mem_query.astype(jnp.float32)
    numerator = jnp.dot(affinity, wide_value, precision=PRECISE) + across[:, None] * lax.dot_general(
        wide_query, start_matrix, (((1,), (1,)), ((), ())), precision=PRECISE
    )
    denominator = jnp.sum(affinity, axis=1) + across * jnp.sum(
        wide_query * start_normal[None, :], axis=1
    )
    floor = jnp.exp(-(cumulative + highest))
    cell = numerator / jnp.maximum(jnp.abs(denominator), floor)[:, None]
    cell_total = lax.psum(jnp.sum(cell * cell, axis=1), TP)
    gain_part = lax.dynamic_slice_in_dim(mem_gain, tp_index * mem_heads * M_V, mem_heads * M_V, 0)
    gated = (
        cell
        * lax.rsqrt(cell_total / (MEMORY_HEADS * M_V) + SMALL_CONSTANT)[:, None]
        * gain_part.astype(jnp.float32)
    )
    gated = gated * jax.nn.sigmoid(mem_outgate.astype(jnp.float32))
    gated = gated.astype(jnp.bfloat16)
    query_all = jnp.dot(normed_query, query_up_weight, preferred_element_type=jnp.float32).astype(
        jnp.bfloat16
    )
    query_all = query_all.reshape(length, att_heads, PLAIN_CHANNELS + ROTARY_CHANNELS)
    query_nope = query_all[..., :PLAIN_CHANNELS]
    query_rot = rotate(query_all[..., PLAIN_CHANNELS:], positions)
    key_rot = rotate(key_raw, positions)
    own_nope = jnp.dot(normed_latent, key_up_weight, preferred_element_type=jnp.float32).astype(
        jnp.bfloat16
    )
    own_values = jnp.dot(normed_latent, value_up_weight, preferred_element_type=jnp.float32).astype(
        jnp.bfloat16
    )
    turned = query_rot.reshape(length, ROTARY_CHANNELS)
    queries = jnp.concatenate([query_nope.reshape(length, PLAIN_CHANNELS), turned, turned], axis=1)
    packed = jnp.concatenate([key_rot[: length // 2], key_rot[length // 2 :]], axis=1)
    attended = attend(queries, jnp.concatenate([own_nope, own_values, packed], axis=0))
    mixed = sum_at_owner(
        (
            jnp.dot(gated, out_memory, preferred_element_type=jnp.float32)
            + jnp.dot(attended, out_attend, preferred_element_type=jnp.float32)
        ).astype(jnp.bfloat16),
        TP,
        0,
    )
    return mixed.astype(jnp.bfloat16)


def solution(mesh):
    torus = Mesh(mesh.devices.reshape(N_Z, N_X, 4, 2), SP_TP)
    in_specs = (
        P(SP_TP, None),
        P(),
        P(None, TP),
        P(None, TP),
        P(None, TP),
        P(None, TP),
        P(),
        P(),
        P(SP, TP),
        P(),
        P(None, TP),
        P(None, TP),
        P(),
        P(),
        P(),
        P(None, TP),
        P(None, TP),
        P(None, TP),
        P(TP, None),
        P(TP, None),
    )
    out_specs = P(SP_TP, None)
    return jax.shard_map(
        per_device, mesh=torus, in_specs=in_specs, out_specs=out_specs, check_vma=False
    )
```

time: 457 us -> 261 us (0.57); the launches traced: 448 us -> 259 us
  matrix products: 130 us -> 17.4 us
  Pallas kernels: 0 us -> 61.5 us
  local copies, waits for them, and re-layouts: 57.2 us -> 7.82 us
  loops' own time: 41.5 us -> 0 us
  other arithmetic: 50.9 us -> 11.3 us
  waiting for transfers between devices: 34.1 us -> 26.3 us
    dot_general x109 -> x4, matrix products: 111 us -> 4.05 us  [the longest x1 1.97 us: per_device(): lax.dot_general(wide_query, start_matrix, (((1,), (1,)), ((), ())), preci...]
    pallas_call x0 -> x1, Pallas kernels: none -> 61.5 us  [attend(): pl.pallas_call(attend_kernel, out_shape=jax.ShapeDtypeStruct((ROWS, VALUE...]
    another operation x19 -> x0, loops' own time: 41.5 us -> none  [the longest x1 20 us: per_device(): lax.scan(one_block, carried, jnp.arange(number // size, dtype=jnp.int32))]
    reduce_max x24 -> x0, other arithmetic: 20.4 us -> none  [the longest x16 19.6 us: update_state(): new_max = jnp.maximum(last_total + stabilizer, jnp.max(weight_log, axis=-1))]
    slice x33 -> x3, local copies, waits for them, and re-layouts: 18.9 us -> 1.34 us  [the longest x1 0.67 us: per_device(): cumulative[-1] + ends_at]
    while x4 -> x0, local copies, waits for them, and re-layouts: 16 us -> none  [per_device(): lax.scan(one_block, carried, jnp.arange(number // size, dtype=jnp.int32))]
    exp x16 -> x1, other arithmetic: 9.85 us -> 0.01 us  [per_device(): across = jnp.exp(start_max[0] - highest)]
    dynamic_slice x16 -> x0, local copies, waits for them, and re-layouts: 9.31 us -> none  [per_device(): lax.scan(one_block, carried, jnp.arange(number // size, dtype=jnp.int32))]
  transfers between devices with their start and end apart: 3 -> 2, of which waited for: 3 -> 1; matrix products, arithmetic and copies ran while one was open for 16% -> 2% of each run, Pallas kernels for 0% -> 24%
where the time goes in v1:
time: 261 us; the launch traced here: 259 us
  blocking collectives  82.1 us (31%)
  Pallas kernels  61.5 us (24%)
  between operations  47.8 us (18%)
  waiting for transfers between devices  26.3 us (10%)
  matrix products  17.4 us (7%)
  other arithmetic  11.3 us (4%)
  local copies, waits for them, and re-layouts  7.82 us (3%)
  starting transfers between devices  4.51 us (2%)
    pallas_call x1, Pallas kernels, attend(): pl.pallas_call(attend_kernel, out_shape=jax.ShapeDtypeStruct((ROWS, VALUE...  61.5 us
    all_to_all x1, blocking collectives, sum_at_owner(): lax.all_to_all(tiles, axis, split_axis=0, concat_axis=0, tiled=True)  29.7 us
    all_to_all x1, waiting for transfers between devices, copy_for_each(): return lax.all_to_all(copies, axis, split_axis=0, concat_axis=0, tiled=True)  26.3 us
    all_gather x1, blocking collectives, per_device(): lax.all_gather(query_latent, TP, axis=1, tiled=True)  13.4 us
    all_gather x1, blocking collectives, gathered_once(): both, at, found = (lax.all_gather(jnp.concatenate(lines), axis), 0, {})  13.3 us
    all_gather x1, blocking collectives, per_device(): lax.all_gather(keyval_latent, TP, axis=1, tiled=True)  13.3 us
    psum x1, blocking collectives, per_device(): cell_total = lax.psum(jnp.sum(cell * cell, axis=1), TP)  12.4 us
    dot_general x9, matrix products, project(): jnp.dot(portion, weight, preferred_element_type=jnp.float32)  10.4 us
  transfers between devices with their start and end apart: 2, of which 1 were waited for; matrix products, arithmetic and copies ran while one was open for 2% of the time, Pallas kernels for 24%

profile of v1, /device:TPU:224, one launch (start us, length us, event | category | flops | bytes accessed | tf_op | source)
XLA Modules:
  0.0 258.8 jit_solution(4656624106841525778)
XLA Ops:
  6.5 1.2 fusion.19
  7.7 0.7 convert_element_type.100
  8.4 1.1 fusion.21
  9.5 1.6 broadcast_in_dim.12
  11.1 4.5 %all-to-all-start = ((bf16[8,64,2048]{2,1,0:T(8,128)(2,1)}), bf16[8,64,2048]{2,1,0:T(8,128)(2,1)S(1)}, u32[]{:S(2)}, u32[]{:S(2)}) async-start(bf16[8,64,2048]{2,1,0:T(8,128)(2,1)} %broadcast_in_dim.12), calls=%async_computation | async-start | bytes 4194304 | tf_op jit(solution)/shard_map/all_to_all | solution.py:30
  15.7 0.8 dynamic-slice_convert_fusion
  16.5 26.3 %all-to-all-done = bf16[8,64,2048]{2,1,0:T(8,128)(2,1)S(1)} async-done(((bf16[8,64,2048]{2,1,0:T(8,128)(2,1)}), bf16[8,64,2048]{2,1,0:T(8,128)(2,1)S(1)}, u32[]{:S(2)}, u32[]{:S(2)}) %all-to-all-start) | async-done | bytes 2097184 | tf_op jit(solution)/shard_map/all_to_all | solution.py:30
  42.8 1.4 fusion.144
  44.2 1.5 fusion.146
  45.7 0.3 reduce-window.16
  46.3 0.3 reduce-window.24
  46.9 0.6 slice.273
  47.5 0.7 exponential_multiply_fusion
  48.2 0.7 slice.274
  50.2 0.7 pad_bitcast_fusion.2
  50.9 1.4 convolution_convert_fusion.9
  52.3 1.8 convolution_convert_fusion.8
  54.2 0.7 convolution_convert_fusion.5
  54.9 0.7 convolution_convert_fusion.6
  55.7 0.7 convolution_convert_fusion.7
  56.4 1.4 convolution_convert_fusion
  57.8 0.7 convolution_convert_fusion.1
  58.7 0.7 fusion.22
  59.4 13.3 %all-gather.2 = f32[4,259,128]{2,1,0:T(8,128)S(1)} all-gather(f32[1,259,128]{2,1,0:T(8,128)S(1)} %maximum_bitcast_fusion), channel_id=2, replica_groups=mesh['z'=8,'x'=4,'y'=4,'c'=2] {'x'}, dimensions={0}, use_global_device_ids=true | all-gather | bytes 663040 | tf_op jit(solution)/shard_map/all_gather | solution.py:58
  72.7 0.6 fusion.177
  73.3 0.6 fusion.176
  84.4 0.7 maximum_bitcast_fusion.1
  85.1 13.4 %all_gather.22 = bf16[512,768]{0,1:T(8,128)(2,1)S(1)} all-gather(bf16[512,96]{0,1:T(8,128)(2,1)S(1)} %convolution_convert_fusion.8), channel_id=1, replica_groups=mesh['z'=8,'x'=4,'y'=4,'c'=2] {'y','c'}, dimensions={1}, use_global_device_ids=true | all-gather | bytes 884736 | tf_op jit(solution)/shard_map/all_gather | solution.py:453
  98.7 0.6 fusion.4
  99.4 1.2 fusion.39
  100.6 1.2 fusion.99
  103.0 13.3 %all_gather.23 = bf16[512,512]{0,1:T(8,128)(2,1)S(1)} all-gather(bf16[512,64]{0,1:T(8,128)(2,1)S(1)} %copy-done.6), channel_id=1, replica_groups=mesh['z'=8,'x'=4,'y'=4,'c'=2] {'y','c'}, dimensions={1}, use_global_device_ids=true | all-gather | bytes 589824 | tf_op jit(solution)/shard_map/all_gather | solution.py:454
  116.5 0.5 convolution_convert_fusion.3
  117.0 0.5 convolution_convert_fusion.4
  117.6 61.5 %attend.1 = bf16[512,128]{1,0:T(8,128)(2,1)S(1)} custom-call(bf16[512,256]{1,0:T(8,128)(2,1)S(1)} %concatenate.33.q_ref, bf16[1280,128]{1,0:T(8,128)(2,1)S(1)} %fusion.37.kv_ref), custom_call_target="tpu_custom_call" | custom-call | flops 4000000000 | bytes 10000000 | tf_op jit(solution)/shard_map/attend/pallas_call | solution.py:352
  179.1 0.8 fusion.172
  180.0 0.6 fusion.175
  181.2 0.6 fusion.174
  202.6 0.8 fusion.167
  203.6 0.3 fusion.178
  203.9 2.0 convolution_multiply_fusion.1
  205.9 1.1 multiply_reduce_fusion
  207.0 12.4 %psum.7 = f32[512]{0:T(512)S(1)} all-reduce(f32[512]{0:T(512)S(1)} %get-tuple-element.60), channel_id=1, replica_groups=mesh['z'=8,'x'=4,'y'=4,'c'=2] {'y','c'}, use_global_device_ids=true, to_apply=%region_9.10 | all-reduce | flops 512 | bytes 4096 | tf_op jit(solution)/shard_map/psum | solution.py:506
  219.4 0.8 fusion.46
  220.2 0.3 copy-done.3
  220.5 0.7 add_convert_fusion
  221.2 29.7 %all_to_all.10 = bf16[8,64,2048]{2,1,0:T(8,128)(2,1)S(1)} all-to-all(bf16[8,64,2048]{2,1,0:T(8,128)(2,1)S(1)} %bitcast.177), channel_id=1, replica_groups=mesh['z'=8,'x'=4,'y'=4,'c'=2] {'y','c'}, dimensions={0} | all-to-all | bytes 4194304 | tf_op jit(solution)/shard_map/all_to_all | solution.py:90
  250.8 1.1 reduce_sum.82
  (70 shorter events, 2.1 us)
Async XLA Ops:
  6.5 212.9 %copy-start = (bf16[256,2048]{1,0:T(8,128)(2,1)S(1)}, bf16[256,2048]{1,0:T(8,128)(2,1)}, u32[]{:S(2)}) copy-start(bf16[256,2048]{1,0:T(8,128)(2,1)} %param.38) | copy-start | bytes 3145732
  11.1 31.6 %all-to-all-start = ((bf16[8,64,2048]{2,1,0:T(8,128)(2,1)}), bf16[8,64,2048]{2,1,0:T(8,128)(2,1)S(1)}, u32[]{:S(2)}, u32[]{:S(2)}) async-start(bf16[8,64,2048]{2,1,0:T(8,128)(2,1)} %broadcast_in_dim.12), calls=%async_computation | async-start | bytes 4194304 | tf_op jit(solution)/shard_map/all_to_all | solution.py:30
  15.6 28.6 %copy-start.9 = (f32[512,1]{0,1:T(1,128)S(1)}, f32[512,1]{0,1:T(1,128)}, u32[]{:S(2)}) copy-start(f32[512,1]{0,1:T(1,128)} %param.28) | copy-start | bytes 6148
  15.6 163.5 %all-gather.6.cloned.1.call-start = ((), (), s32[]{:S(2)}) async-start(), calls=%async_computation.2 | async-start | bytes 1216512 | tf_op jit(solution)/shard_map/all_gather | solution.py:58
  42.8 8.1 %copy-start.4 = (bf16[2048,64]{0,1:T(8,128)(2,1)S(1)}, bf16[2048,64]{0,1:T(8,128)(2,1)}, u32[]{:S(2)}) copy-start(bf16[2048,64]{0,1:T(8,128)(2,1)} %param.31) | copy-start | bytes 786436
  50.9 3.3 %copy-start.13 = (bf16[2048,64]{0,1:T(8,128)(2,1)S(1)}, bf16[2048,64]{0,1:T(8,128)(2,1)}, u32[]{:S(2)}) copy-start(bf16[2048,64]{0,1:T(8,128)(2,1)} %param.32) | copy-start | bytes 786436
  52.3 2.6 copy-start.1
  54.2 1.5 copy-start.2
  54.9 1.5 copy-start.10
  56.4 1.4 copy-start.11
  58.5 24.5 %copy-start.7 = (bf16[512,256]{1,0:T(8,128)(2,1)}, bf16[512,256]{1,0:T(8,128)(2,1)S(1)}, u32[]{:S(2)}) copy-start(bf16[512,256]{1,0:T(8,128)(2,1)S(1)} %convolution_convert_fusion.1) | copy-start | bytes 786436
  59.4 39.3 %copy-start.12 = (bf16[768,192]{0,1:T(8,128)(2,1)S(1)}, bf16[768,192]{0,1:T(8,128)(2,1)}, u32[]{:S(2)}) copy-start(bf16[768,192]{0,1:T(8,128)(2,1)} %param.35) | copy-start | bytes 884740
  59.4 39.3 %copy-start.16 = (f32[768]{0:T(1024)S(1)}, f32[768]{0:T(1024)}, u32[]{:S(2)}) copy-start(f32[768]{0:T(1024)} %param.33) | copy-start | bytes 9220
  99.4 3.7 %copy-start.6 = (bf16[512,64]{0,1:T(8,128)(2,1)S(1)}, bf16[512,64]{0,1:T(8,128)(2,1)}, u32[]{:S(2)}) copy-start(bf16[512,64]{0,1:T(8,128)(2,1)} %convolution_convert_fusion.9) | copy-start | bytes 196612
  99.4 17.1 %copy-start.14 = (bf16[512,128]{1,0:T(8,128)(2,1)S(1)}, bf16[512,128]{1,0:T(8,128)(2,1)}, u32[]{:S(2)}) copy-start(bf16[512,128]{1,0:T(8,128)(2,1)} %param.37) | copy-start | bytes 393220
  99.4 17.1 %copy-start.17 = (f32[512]{0:T(512)S(1)}, f32[512]{0:T(512)}, u32[]{:S(2)}) copy-start(f32[512]{0:T(512)} %param.34) | copy-start | bytes 6148
  101.9 15.1 %copy-start.15 = (bf16[512,128]{1,0:T(8,128)(2,1)S(1)}, bf16[512,128]{1,0:T(8,128)(2,1)}, u32[]{:S(2)}) copy-start(bf16[512,128]{1,0:T(8,128)(2,1)} %param.36) | copy-start | bytes 393220
  203.6 2.3 copy-start.8
  203.9 15.5 %copy-start.5 = (bf16[512,256]{1,0:T(8,128)(2,1)S(1)}, bf16[512,256]{1,0:T(8,128)(2,1)}, u32[]{:S(2)}) copy-start(bf16[512,256]{1,0:T(8,128)(2,1)} %convolution_convert_fusion) | copy-start | bytes 786436
  219.4 1.0 copy-start.3
Sparse Core Ops, SparseCore 0:
  85.2 35.0 all-gather.5

commit v2 on v1

--- a/solution.py
+++ b/solution.py
@@ -23,22 +23,6 @@
 ROTARY_BASE = 10000.0
 PRECISE = lax.Precision.HIGHEST
 FAR_BELOW = -1e30
-
-
-def copy_for_each(shard, axis):
-    copies = jnp.broadcast_to(shard, (lax.axis_size(axis), *shard.shape))
-    return lax.all_to_all(copies, axis, split_axis=0, concat_axis=0, tiled=True)
-
-
-def laid_out(tiles, dim):
-    shape = list(tiles.shape[1:])
-    shape[dim] *= tiles.shape[0]
-    return jnp.moveaxis(tiles, 0, dim).reshape(shape)
-
-
-def gather_directly(shard, axis, dim):
-    tiles = copy_for_each(shard, axis)
-    return laid_out(tiles, dim)
 
 
 def nothing_yet(shard, identity):
@@ -77,45 +61,6 @@
             inside = jax.tree.map(lambda new, old: jnp.where(passed, new, old), running, inside)
         before = combine(inside, before)
     return before
-
-
-def in_blocks(shard, dim, peers):
-    shape = shard.shape
-    tiles = shard.reshape(*shape[:dim], peers, shape[dim] // peers, *shape[dim + 1 :])
-    return jnp.moveaxis(tiles, dim, 0)
-
-
-def sum_at_owner(shard, axis, dim):
-    tiles = in_blocks(shard, dim, lax.axis_size(axis))
-    arrived = lax.all_to_all(tiles, axis, split_axis=0, concat_axis=0, tiled=True)
-    return arrived.astype(jnp.float32).sum(axis=0)
-
-
-def rms_scale(values, gain):
-    widened = values.astype(jnp.float32)
-    return (
-        widened
-        * lax.rsqrt(jnp.mean(widened * widened, axis=-1, keepdims=True) + SMALL_CONSTANT)
-        * gain.astype(jnp.float32)
-    )
-
-
-def rotate(values, positions):
-    halfway = values.shape[-1] // 2
-    inverse = jnp.power(ROTARY_BASE, -jnp.arange(halfway, dtype=jnp.float32) / halfway)
-    angles = positions.astype(jnp.float32)[:, None] * inverse
-    cosine = jnp.cos(angles)
-    sine_part = jnp.sin(angles)
-    if values.ndim == 3:
-        cosine = cosine[:, None, :]
-        sine_part = sine_part[:, None, :]
-    widened = values.astype(jnp.float32)
-    first = widened[..., :halfway]
-    second = widened[..., halfway:]
-    turned = jnp.concatenate(
-        [first * cosine - second * sine_part, second * cosine + first * sine_part], axis=-1
-    )
-    return turned.astype(jnp.bfloat16)
 
 
 def merge_states(earlier, later):
@@ -386,6 +331,470 @@
     )(queries, keys_values)
 
 
+N_Y = 4
+N_C = 2
+SHARE = 64
+QUERY_LATENT = 768
+LATENT_WIDTH = 512
+QUERY_PART = QUERY_LATENT // (N_Y * N_C)
+LATENT_PART = LATENT_WIDTH // (N_Y * N_C)
+PARAMS = pltpu.CompilerParams
+
+
+class TpGather:
+    def __init__(self, full, sends, recvs):
+        self.full, self.sends, self.recvs = full, sends, recvs
+        self.y, self.c = lax.axis_index("y"), lax.axis_index("c")
+        self.half = full.shape[1] // 2
+        self.started = []
+
+    def _copy(self, number, shift, part, target):
+        slot = lax.rem(self.y + shift, N_Y) * N_C + self.c
+        if part is None:
+            ref = self.full.at[slot]
+        else:
+            ref = self.full.at[slot, pl.ds(part * self.half, self.half)]
+        if target == "core":
+            device = {"c": 1 - self.c}
+        else:
+            device = {"y": lax.rem(self.y + (1 if target == "up" else N_Y - 1), N_Y)}
+        return pltpu.make_async_remote_copy(
+            src_ref=ref,
+            dst_ref=ref,
+            send_sem=self.sends.at[number],
+            recv_sem=self.recvs.at[number],
+            device_id=device,
+            device_id_type=MESH_ID,
+        )
+
+    def _start(self, *what):
+        copy = self._copy(*what)
+        copy.start()
+        self.started.append(copy)
+
+    def start(self):
+        self._start(0, 0, 0, "up")
+        self._start(3, 0, 1, "down")
+        self._start(1, 0, 1, "up")
+        self._start(2, 0, 0, "down")
+        self._start(6, 0, None, "core")
+
+    def relay(self):
+        self._copy(0, 0, 0, "up").wait_recv()
+        self._start(4, N_Y - 1, 0, "up")
+        self._copy(3, 0, 1, "down").wait_recv()
+        self._start(5, 1, 1, "down")
+        self._copy(1, 0, 1, "up").wait_recv()
+        self._start(7, N_Y - 1, None, "core")
+        self._copy(2, 0, 0, "down").wait_recv()
+        self._start(8, 1, None, "core")
+
+    def near(self):
+        for number, shift in ((6, 0), (7, N_Y - 1), (8, 1)):
+            self._copy(number, shift, None, "core").wait_recv()
+
+    def far(self):
+        self._copy(4, 0, 0, "up").wait_recv()
+        self._start(9, 2, 0, "core")
+        self._copy(5, 0, 1, "down").wait_recv()
+        self._start(10, 2, 1, "core")
+        for part in range(2):
+            self._copy(9 + part, 2, part, "core").wait_recv()
+
+    def finish(self):
+        for copy in self.started:
+            copy.wait_send()
+
+
+def greet_tp(barrier):
+    y, c = lax.axis_index("y"), lax.axis_index("c")
+    for device in (
+        {"c": 1 - c},
+        {"y": lax.rem(y + 1, N_Y)},
+        {"y": lax.rem(y + N_Y - 1, N_Y)},
+    ):
+        pl.semaphore_signal(barrier, inc=1, device_id=device, device_id_type=MESH_ID)
+
+
+def project_kernel(
+    tokens,
+    gain,
+    small_hbm,
+    query_hbm,
+    key_hbm,
+    value_hbm,
+    outgate_hbm,
+    query_up,
+    key_up,
+    value_up,
+    gains,
+    cosine,
+    sine_part,
+    mem_ref,
+    gate_ref,
+    q_ref,
+    kv_ref,
+    rows_all,
+    latents,
+    small,
+    big,
+    up_query,
+    up_latent,
+    wide_query,
+    wide_latent,
+    load_sem,
+    row_send,
+    row_recv,
+    lat_send,
+    lat_recv,
+):
+    f32, bf16 = jnp.float32, jnp.bfloat16
+    y, c = lax.axis_index("y"), lax.axis_index("c")
+    mine = y * N_C + c
+    width = 128
+    loads = [pltpu.make_async_copy(small_hbm, small, load_sem.at[0])]
+    at = 0
+    for k, ref in enumerate((query_hbm, key_hbm, value_hbm, outgate_hbm)):
+        columns = ref.shape[1]
+        loads.append(
+            pltpu.make_async_copy(ref, big.at[:, pl.ds(at, columns)], load_sem.at[1 + k])
+        )
+        at += columns
+    for load in loads:
+        load.start()
+
+    wide = tokens[...].astype(f32)
+    inverse = lax.rsqrt(jnp.mean(wide * wide, axis=1, keepdims=True) + SMALL_CONSTANT)
+    rows_all[mine] = (wide * inverse * gain[...].astype(f32)).astype(bf16)
+
+    barrier = pltpu.get_barrier_semaphore()
+    greet_tp(barrier)
+    pl.semaphore_wait(barrier, 3)
+    gather = TpGather(rows_all, row_send, row_recv)
+    gather.start()
+
+    up_query[...] = jnp.zeros(up_query.shape, bf16)
+    for s in range(N_Y * N_C):
+        up_query[s * width : s * width + QUERY_PART] = query_up[
+            s * QUERY_PART : (s + 1) * QUERY_PART
+        ]
+        part = slice(s * LATENT_PART, (s + 1) * LATENT_PART)
+        for h in range(2):
+            at = s * width + h * LATENT_PART
+            up_latent[at : at + LATENT_PART, :width] = key_up[part]
+            up_latent[at : at + LATENT_PART, width:] = value_up[part]
+    for load in loads:
+        load.wait()
+
+    lane = lax.broadcasted_iota(jnp.int32, (1, width), 1)
+    row_id = lax.broadcasted_iota(jnp.int32, (width, width), 0)
+    col_id = lax.broadcasted_iota(jnp.int32, (width, width), 1)
+    channels = lax.rem(col_id, ROTARY_CHANNELS)
+    halfway = ROTARY_CHANNELS // 2
+    twin = (row_id == channels).astype(bf16)
+    partner = lax.rem(channels + halfway, ROTARY_CHANNELS)
+    sign = jnp.where(channels < halfway, -1.0, 1.0)
+
+    def duplicated(values, offset):
+        return jnp.dot(
+            values, (row_id == channels + offset).astype(bf16), preferred_element_type=f32
+        )
+
+    def rotated(values, offset):
+        swap = jnp.where(row_id == partner + offset, sign, 0.0).astype(bf16)
+        turned = jnp.dot(values, swap, preferred_element_type=f32)
+        return duplicated(values, offset) * cosine[...] + turned * sine_part[...]
+
+    def chip_rows(chip):
+        slots = [rows_all[chip * N_C + k] for k in range(N_C)]
+        return jnp.concatenate(slots, axis=0)
+
+    span = N_C * SHARE
+    tile = 256
+
+    def project_small(chip):
+        rows = pl.ds(pl.multiple_of(chip * span, span), span)
+        made = jnp.dot(chip_rows(chip), small[...], preferred_element_type=f32)
+        gate_ref[rows] = made[:, :width]
+        rounded = made.astype(bf16)
+        latents[mine, rows] = rounded[:, :width]
+        wide_latent[rows, :width] = rounded[:, width:]
+
+    def project_big(chip):
+        rows = pl.ds(pl.multiple_of(chip * span, span), span)
+
+        def one(t, carry):
+            columns = pl.ds(pl.multiple_of(t * tile, tile), tile)
+            made = jnp.dot(chip_rows(chip), big[:, columns], preferred_element_type=f32)
+            mem_ref[rows, columns] = made.astype(bf16)
+            return carry
+
+        lax.fori_loop(0, big.shape[1] // tile, one, 0)
+
+    gather.relay()
+    gather.near()
+    near = [y, lax.rem(y + N_Y - 1, N_Y), lax.rem(y + 1, N_Y)]
+    for chip in near:
+        project_small(chip)
+    opposite = lax.rem(y + 2, N_Y)
+    gather.far()
+    project_small(opposite)
+
+    second = wide_latent[:, :width]
+    both = duplicated(second, 0)
+    half = ROWS // 2
+    packed = jnp.where(lane < LATENT_PART, both[:half], both[half:])
+    latents[mine, ROWS:] = packed.astype(bf16)
+    exchange = TpGather(latents, lat_send, lat_recv)
+    exchange.start()
+    for chip in near[:2]:
+        project_big(chip)
+    exchange.relay()
+    for chip in (near[2], opposite):
+        project_big(chip)
+    key_turned = rotated(second, LATENT_PART)
+    kv_ref[2 * ROWS :] = jnp.where(
+        lane < ROTARY_CHANNELS, key_turned[:half], key_turned[half:]
+    ).astype(bf16)
+    exchange.near()
+    exchange.far()
+
+    query_mask = (lane < QUERY_PART).astype(f32)
+    squares = jnp.zeros((ROWS, width), f32)
+    low_squares = jnp.zeros((half, width), f32)
+    for s in range(N_Y * N_C):
+        part = latents[s, :ROWS].astype(f32) * query_mask
+        squares = squares + part * part
+        part = latents[s, ROWS:].astype(f32)
+        low_squares = low_squares + part * part
+    query_scale = lax.rsqrt(
+        jnp.sum(squares, axis=1, keepdims=True) / QUERY_LATENT + SMALL_CONSTANT
+    )
+    low = lane < LATENT_PART
+    low_scale = lax.rsqrt(
+        jnp.sum(jnp.where(low, low_squares, 0.0), axis=1, keepdims=True) / LATENT_WIDTH
+        + SMALL_CONSTANT
+    )
+    high_scale = lax.rsqrt(
+        jnp.sum(jnp.where(low, 0.0, low_squares), axis=1, keepdims=True) / LATENT_WIDTH
+        + SMALL_CONSTANT
+    )
+    latent_scale = jnp.where(low, low_scale, high_scale)
+    for s in range(N_Y * N_C):
+        columns = slice(s * width, (s + 1) * width)
+        part = latents[s, :ROWS].astype(f32) * query_mask
+        wide_query[:, columns] = (part * query_scale * gains[s : s + 1]).astype(bf16)
+        part = latents[s, ROWS:].astype(f32)
+        made = (part * latent_scale * gains[8 + s : 9 + s]).astype(bf16)
+        wide_latent[:half, columns] = jnp.where(low, made, jnp.zeros_like(made))
+        wide_latent[half:, columns] = jnp.where(low, jnp.zeros_like(made), made)
+    made = jnp.dot(wide_query[...], up_query[...], preferred_element_type=f32).astype(bf16)
+    q_ref[:, :width] = made[:, :width]
+    turning = jnp.concatenate([made[:, width:], jnp.zeros((ROWS, ROTARY_CHANNELS), bf16)], axis=1)
+    q_ref[:, width:] = rotated(turning, 0).astype(bf16)
+    made = jnp.dot(wide_latent[...], up_latent[...], preferred_element_type=f32).astype(bf16)
+    kv_ref[:ROWS] = made[:, :width]
+    kv_ref[ROWS : 2 * ROWS] = made[:, width:]
+    gather.finish()
+    exchange.finish()
+
+
+def project(tokens, gain, small, query, key, value, outgate, ups, gains, cosine, sine_part):
+    f32, bf16 = jnp.float32, jnp.bfloat16
+    depth = tokens.shape[1]
+    dma = pltpu.SemaphoreType.DMA
+    vmem = pl.BlockSpec(memory_space=pltpu.VMEM)
+    hbm = pl.BlockSpec(memory_space=pl.ANY)
+    mem_width = query.shape[1] + key.shape[1] + value.shape[1] + outgate.shape[1]
+    return pl.pallas_call(
+        project_kernel,
+        out_shape=(
+            jax.ShapeDtypeStruct((ROWS, mem_width), bf16),
+            jax.ShapeDtypeStruct((ROWS, 128), f32),
+            jax.ShapeDtypeStruct((ROWS, 256), bf16),
+            jax.ShapeDtypeStruct((ROWS * 5 // 2, 128), bf16),
+        ),
+        in_specs=[vmem] * 2 + [hbm] * 5 + [vmem] * 6,
+        out_specs=[vmem] * 4,
+        scratch_shapes=[
+            pltpu.VMEM((N_Y * N_C, SHARE, depth), bf16),
+            pltpu.VMEM((N_Y * N_C, ROWS * 3 // 2, 128), bf16),
+            pltpu.VMEM((depth, 256), bf16),
+            pltpu.VMEM((depth, mem_width), bf16),
+            pltpu.VMEM((1024, PLAIN_CHANNELS + ROTARY_CHANNELS), bf16),
+            pltpu.VMEM((1024, 256), bf16),
+            pltpu.VMEM((ROWS, 1024), bf16),
+            pltpu.VMEM((ROWS, 1024), bf16),
+            dma((5,)),
+            dma((11,)),
+            dma((11,)),
+            dma((11,)),
+            dma((11,)),
+        ],
+        compiler_params=PARAMS(
+            collective_id=2, has_side_effects=True, vmem_limit_bytes=48 * 1024 * 1024
+        ),
+        cost_estimate=pl.CostEstimate(
+            flops=3 * 10**9, bytes_accessed=10**7, transcendentals=10**4
+        ),
+        name="project",
+    )(tokens, gain, small, query, key, value, outgate, *ups, gains, cosine, sine_part)
+
+
+def output_kernel(
+    gated,
+    attended,
+    out_memory,
+    out_attend,
+    o_ref,
+    to_core,
+    from_core,
+    sums,
+    passing,
+    from_below,
+    from_above,
+    relay_in,
+    core_send,
+    core_recv,
+    relay_send,
+    relay_recv,
+    up_send,
+    up_recv,
+    down_send,
+    down_recv,
+):
+    f32, bf16 = jnp.float32, jnp.bfloat16
+    y, c = lax.axis_index("y"), lax.axis_index("c")
+    above, below = lax.rem(y + 1, N_Y), lax.rem(y + N_Y - 1, N_Y)
+    opposite = lax.rem(y + 2, N_Y)
+    half = out_memory.shape[1] // 2
+    tile = 512
+
+    barrier = pltpu.get_barrier_semaphore()
+    greet_tp(barrier)
+
+    def remote(source, target, send, recv, device):
+        return pltpu.make_async_remote_copy(
+            src_ref=source,
+            dst_ref=target,
+            send_sem=send,
+            recv_sem=recv,
+            device_id=device,
+            device_id_type=MESH_ID,
+        )
+
+    def rows_of(ref, core):
+        picked = [ref[pl.ds(pl.multiple_of((k * N_C + core) * SHARE, SHARE), SHARE)] for k in range(N_Y)]
+        return jnp.concatenate(picked, axis=0)
+
+    def partial(core, h, store):
+        memory_rows, attend_rows = rows_of(gated, core), rows_of(attended, core)
+        for t in range(half // tile):
+            columns = slice(h * half + t * tile, h * half + (t + 1) * tile)
+            made = jnp.dot(memory_rows, out_memory[:, columns], preferred_element_type=f32)
+            made = made + jnp.dot(attend_rows, out_attend[:, columns], preferred_element_type=f32)
+            store(t * tile, made.astype(bf16).reshape(N_Y, SHARE, tile))
+
+    def core_copy(h):
+        return remote(
+            to_core.at[h], from_core.at[h], core_send.at[h], core_recv.at[h], {"c": 1 - c}
+        )
+
+    def relay_copy(h):
+        return remote(
+            passing.at[h],
+            relay_in.at[h],
+            relay_send.at[h],
+            relay_recv.at[h],
+            {"y": above if h == 0 else below},
+        )
+
+    def up_copy(h):
+        return remote(
+            passing.at[2 + h], from_below.at[h], up_send.at[h], up_recv.at[h], {"y": above}
+        )
+
+    def down_copy(h):
+        return remote(
+            passing.at[4 + h], from_above.at[h], down_send.at[h], down_recv.at[h], {"y": below}
+        )
+
+    started = []
+
+    def start(copy):
+        copy.start()
+        started.append(copy)
+
+    for h in range(2):
+
+        def keep(at, block, h=h):
+            to_core[h, :, :, at : at + tile] = block
+
+        partial(1 - c, h, keep)
+        if h == 0:
+            pl.semaphore_wait(barrier, 3)
+        start(core_copy(h))
+    for h in range(2):
+
+        def keep(at, block, h=h):
+            sums[h, :, :, at : at + tile] = block.astype(f32)
+
+        partial(c, h, keep)
+    for h in range(2):
+        core_copy(h).wait_recv()
+        sums[h] = sums[h] + from_core[h].astype(f32)
+        passing[h] = sums[h, opposite].astype(bf16)
+        start(relay_copy(h))
+        if h == 0:
+            passing[4] = sums[0, below].astype(bf16)
+            start(down_copy(0))
+        else:
+            passing[3] = sums[1, above].astype(bf16)
+            start(up_copy(1))
+    relay_copy(0).wait_recv()
+    passing[2] = (sums[0, above] + relay_in[0].astype(f32)).astype(bf16)
+    start(up_copy(0))
+    relay_copy(1).wait_recv()
+    passing[5] = (sums[1, below] + relay_in[1].astype(f32)).astype(bf16)
+    start(down_copy(1))
+    for h in (1, 0):
+        up_copy(h).wait_recv()
+        down_copy(h).wait_recv()
+        made = sums[h, y] + from_below[h].astype(f32) + from_above[h].astype(f32)
+        o_ref[:, h * half : (h + 1) * half] = made.astype(bf16)
+    for copy in started:
+        copy.wait_send()
+
+
+def project_out(gated, attended, out_memory, out_attend):
+    f32, bf16 = jnp.float32, jnp.bfloat16
+    dma = pltpu.SemaphoreType.DMA
+    vmem = pl.BlockSpec(memory_space=pltpu.VMEM)
+    half = out_memory.shape[1] // 2
+    block = (2, SHARE, half)
+    return pl.pallas_call(
+        output_kernel,
+        out_shape=jax.ShapeDtypeStruct((SHARE, 2 * half), bf16),
+        in_specs=[vmem] * 4,
+        out_specs=vmem,
+        scratch_shapes=[
+            pltpu.VMEM((2, N_Y, SHARE, half), bf16),
+            pltpu.VMEM((2, N_Y, SHARE, half), bf16),
+            pltpu.VMEM((2, N_Y, SHARE, half), f32),
+            pltpu.VMEM((6, SHARE, half), bf16),
+            pltpu.VMEM(block, bf16),
+            pltpu.VMEM(block, bf16),
+            pltpu.VMEM(block, bf16),
+        ]
+        + [dma((2,))] * 8,
+        compiler_params=PARAMS(
+            collective_id=3, has_side_effects=True, vmem_limit_bytes=48 * 1024 * 1024
+        ),
+        cost_estimate=pl.CostEstimate(flops=10**9, bytes_accessed=10**7, transcendentals=0),
+        name="project_out",
+    )(gated, attended, out_memory, out_attend)
+
+
 def per_device(
     tokens,
     input_gain,
@@ -408,53 +817,54 @@
     out_memory,
     out_attend,
 ):
-    normed = rms_scale(tokens, input_gain).astype(jnp.bfloat16)
     tp_index = lax.axis_index(TP)
     mem_heads = weight_query.shape[1] // M_QK
-    att_heads = key_up_weight.shape[1] // PLAIN_CHANNELS
-    ingate_cols = lax.dynamic_slice_in_dim(weight_ingate, tp_index * mem_heads, mem_heads, 1)
-    forget_cols = lax.dynamic_slice_in_dim(weight_forget, tp_index * mem_heads, mem_heads, 1)
-    weight_list = (
+    length = forget_shift.shape[0]
+    small = jnp.concatenate(
+        [
+            query_down_weight,
+            weight_ingate,
+            weight_forget,
+            jnp.zeros((tokens.shape[1], 16), jnp.bfloat16),
+            latent_down_weight,
+            down_rotary,
+        ],
+        axis=1,
+    )
+    latent_rows = latent_gain.reshape(8, LATENT_PART)
+    gains = jnp.concatenate(
+        [
+            jnp.pad(query_gain.reshape(8, QUERY_PART), ((0, 0), (0, 128 - QUERY_PART))),
+            jnp.concatenate([latent_rows, latent_rows], axis=1),
+        ],
+        axis=0,
+    )
+    positions = lax.axis_index(SP) * length + jnp.arange(length, dtype=jnp.int32)
+    halfway = ROTARY_CHANNELS // 2
+    inverse = jnp.power(ROTARY_BASE, -jnp.arange(halfway, dtype=jnp.float32) / halfway)
+    angles = positions.astype(jnp.float32)[:, None] * inverse
+    cosine, sine_part = (jnp.tile(made, (1, 4)) for made in (jnp.cos(angles), jnp.sin(angles)))
+    memory_inputs, pre_gates, queries, keys_values = project(
+        tokens,
+        input_gain[None, :],
+        small,
         weight_query,
         weight_key,
         weight_value,
         weight_outgate,
-        query_down_weight,
-        latent_down_weight,
-        down_rotary,
-        ingate_cols,
-        forget_cols,
-    )
-
-    def project(portion):
-        return jnp.concatenate(
-            [
-                jnp.dot(portion, weight, preferred_element_type=jnp.float32)
-                for weight in weight_list
-            ],
-            axis=1,
-        )
-
-    projected = project(gather_directly(normed, TP, 0))
-    sections = []
-    offset = 0
-    for weight in weight_list:
-        sections.append(projected[:, offset : offset + weight.shape[1]])
-        offset = offset + weight.shape[1]
-    stored = tuple((section.astype(jnp.bfloat16) for section in sections[:7]))
-    mem_query, mem_key, mem_value, mem_outgate, query_latent, keyval_latent, key_raw = (
-        lax.optimization_barrier(stored)
-    )
-    in_gate = SOFTCAP * jnp.tanh(sections[7] / SOFTCAP)
-    log_forget = jax.nn.log_sigmoid(SOFTCAP * jnp.tanh((sections[8] + forget_shift) / SOFTCAP))
-    length = projected.shape[0]
-    positions = lax.axis_index(SP) * length + jnp.arange(length, dtype=jnp.int32)
-    query_whole, latent_whole = (
-        lax.all_gather(query_latent, TP, axis=1, tiled=True),
-        lax.all_gather(keyval_latent, TP, axis=1, tiled=True),
-    )
-    normed_query = rms_scale(query_whole, query_gain).astype(jnp.bfloat16)
-    normed_latent = rms_scale(latent_whole, latent_gain).astype(jnp.bfloat16)
+        (query_up_weight, key_up_weight, value_up_weight),
+        gains,
+        cosine,
+        sine_part,
+    )
+    mem_query = memory_inputs[:, :M_QK]
+    mem_key = memory_inputs[:, M_QK : 2 * M_QK]
+    mem_value = memory_inputs[:, 2 * M_QK : 2 * M_QK + M_V]
+    mem_outgate = memory_inputs[:, 2 * M_QK + M_V :]
+    in_pre = lax.dynamic_slice_in_dim(pre_gates, QUERY_PART + tp_index, 1, 1)
+    forget_pre = lax.dynamic_slice_in_dim(pre_gates, QUERY_PART + 8 + tp_index, 1, 1)
+    in_gate = SOFTCAP * jnp.tanh(in_pre / SOFTCAP)
+    log_forget = jax.nn.log_sigmoid(SOFTCAP * jnp.tanh((forget_pre + forget_shift) / SOFTCAP))
     cumulative = jnp.cumsum(log_forget[:, 0])
     relative = in_gate[:, 0] - cumulative
     running = lax.cummax(relative)
@@ -512,32 +922,8 @@
     )
     gated = gated * jax.nn.sigmoid(mem_outgate.astype(jnp.float32))
     gated = gated.astype(jnp.bfloat16)
-    query_all = jnp.dot(normed_query, query_up_weight, preferred_element_type=jnp.float32).astype(
-        jnp.bfloat16
-    )
-    query_all = query_all.reshape(length, att_heads, PLAIN_CHANNELS + ROTARY_CHANNELS)
-    query_nope = query_all[..., :PLAIN_CHANNELS]
-    query_rot = rotate(query_all[..., PLAIN_CHANNELS:], positions)
-    key_rot = rotate(key_raw, positions)
-    own_nope = jnp.dot(normed_latent, key_up_weight, preferred_element_type=jnp.float32).astype(
-        jnp.bfloat16
-    )
-    own_values = jnp.dot(normed_latent, value_up_weight, preferred_element_type=jnp.float32).astype(
-        jnp.bfloat16
-    )
-    turned = query_rot.reshape(length, ROTARY_CHANNELS)
-    queries = jnp.concatenate([query_nope.reshape(length, PLAIN_CHANNELS), turned, turned], axis=1)
-    packed = jnp.concatenate([key_rot[: length // 2], key_rot[length // 2 :]], axis=1)
-    attended = attend(queries, jnp.concatenate([own_nope, own_values, packed], axis=0))
-    mixed = sum_at_owner(
-        (
-            jnp.dot(gated, out_memory, preferred_element_type=jnp.float32)
-            + jnp.dot(attended, out_attend, preferred_element_type=jnp.float32)
-        ).astype(jnp.bfloat16),
-        TP,
-        0,
-    )
-    return mixed.astype(jnp.bfloat16)
+    attended = attend(queries, keys_values)
+    return project_out(gated, attended, out_memory, out_attend)
 
 
 def solution(mesh):

time: 261 us -> 216 us (0.83)
  blocking collectives: 82.1 us -> 26.4 us
  Pallas kernels: 61.5 us -> 106 us
  waiting for transfers between devices: 26.3 us -> 0.04 us
  local copies, waits for them, and re-layouts: 7.82 us -> 24.1 us
  matrix products: 17.4 us -> 4.03 us
  other arithmetic: 11.3 us -> 5.43 us
  starting transfers between devices: 4.51 us -> 0.01 us
    pallas_call x0 -> x2, Pallas kernels: none -> 43.2 us  [the longest x1 28.4 us: project(): pl.pallas_call(project_kernel, out_shape=(jax.ShapeDtypeStruct((ROWS, mem...]
    all_to_all x1 -> x0, blocking collectives: 29.7 us -> none  [sum_at_owner(): lax.all_to_all(tiles, axis, split_axis=0, concat_axis=0, tiled=True)]
    all_gather x2 -> x0, blocking collectives: 26.7 us -> none  [the longest x1 13.4 us: per_device(): lax.all_gather(query_latent, TP, axis=1, tiled=True)]
    all_to_all x1 -> x0, waiting for transfers between devices: 26.3 us -> none  [copy_for_each(): return lax.all_to_all(copies, axis, split_axis=0, concat_axis=0, tiled=True)]
    dot_general x14 -> x0, matrix products: 13.4 us -> none  [the longest x9 10.4 us: project(): jnp.dot(portion, weight, preferred_element_type=jnp.float32)]
    unnamed x36 -> x46, local copies, waits for them, and re-layouts: 0.37 us -> 13.1 us
    all_to_all x1 -> x0, starting transfers between devices: 4.47 us -> none  [copy_for_each(): return lax.all_to_all(copies, axis, split_axis=0, concat_axis=0, tiled=True)]
    concatenate x1, local copies, waits for them, and re-layouts: 0.24 us -> 3.17 us  [per_device(): jnp.concatenate([query_down_weight, weight_ingate, weight_forget, jnp.zer...]
  transfers between devices with their start and end apart: 2 -> 1, of which waited for: 1 -> 0; matrix products, arithmetic and copies ran while one was open for 2% -> 0% of each run, Pallas kernels for 24% -> 29%
where the time goes in v2:
time: 216 us; the launch traced here: 214 us
  Pallas kernels  106 us (49%)
  between operations  48.2 us (22%)
  blocking collectives  26.4 us (12%)
  local copies, waits for them, and re-layouts  24.1 us (11%)
  other arithmetic  5.43 us (3%)
  matrix products  4.03 us (2%)
    pallas_call x1, Pallas kernels, attend(): pl.pallas_call(attend_kernel, out_shape=jax.ShapeDtypeStruct((ROWS, VALUE...  62.4 us
    pallas_call x1, Pallas kernels, project(): pl.pallas_call(project_kernel, out_shape=(jax.ShapeDtypeStruct((ROWS, mem...  28.4 us
    pallas_call x1, Pallas kernels, project_out(): pl.pallas_call(output_kernel, out_shape=jax.ShapeDtypeStruct((SHARE, 2 *...  14.8 us
    all_gather x1, blocking collectives, gathered_once(): both, at, found = (lax.all_gather(jnp.concatenate(lines), axis), 0, {})  14 us
    unnamed x46, local copies, waits for them, and re-layouts  13.1 us
    psum x1, blocking collectives, per_device(): cell_total = lax.psum(jnp.sum(cell * cell, axis=1), TP)  12.4 us
  transfers between devices with their start and end apart: 1, of which 0 were waited for; matrix products, arithmetic and copies ran while one was open for 0% of the time, Pallas kernels for 29%

profile of v2, /device:TPU:224, one launch (start us, length us, event | category | flops | bytes accessed | tf_op | source)
XLA Modules:
  0.0 213.7 jit_solution(17518878350779227211)
XLA Ops:
  6.6 0.7 broadcast_in_dim.14.gain
  7.3 1.3 copy.54
  8.6 1.8 copy.55
  10.4 1.0 copy.56
  11.4 1.0 copy.57
  12.4 1.0 copy.58
  13.4 0.2 copy.59.query_up
  13.8 0.3 multiply_sine_fusion
  14.1 0.1 copy.60.cosine
  14.3 0.1 copy.61.sine_part
  14.5 0.9 copy.63
  15.4 0.9 broadcast_in_dim.15
  16.3 3.2 %concatenate.15.small_hbm = bf16[2048,256]{1,0:T(8,128)(2,1)S(1)} concatenate(bf16[2048,96]{1,0:T(8,128)(2,1)S(1)} %copy.54, bf16[2048,8]{1,0:T(8,128)(2,1)} %copy.55, bf16[2048,8]{1,0:T(8,128)(2,1)} %copy.56, bf16[2048,16]{1,0:T(8,128)(2,1)} %broadcast_in_dim.15, bf16[2048,64]{1,0:T(8,128)(2,1)} %copy.57, bf16[2048,64]{1,0:T(8,128)(2,1)} %copy.58), dimensions={1} | concatenate | bytes 2097152 | tf_op jit(solution)/shard_map/concatenate | solution.py:823
  19.5 1.0 copy-done.2
  20.5 0.9 copy-done.4
  21.5 0.9 copy-done.5
  22.4 0.9 copy-done.6
  23.3 28.4 %project.1 = (bf16[512,768]{1,0:T(8,128)(2,1)S(1)}, f32[512,128]{1,0:T(8,128)S(1)}, bf16[512,256]{1,0:T(8,128)(2,1)S(1)}, bf16[1280,128]{1,0:T(8,128)(2,1)S(1)}) custom-call(bf16[64,2048]{1,0:T(8,128)(2,1)S(1)} %copy-done.4, bf16[1,2048]{1,0:T(2,128)(2,1)S(1)} %broadcast_in_dim.14.gain, bf16[2048,256]{1,0:T(8,128)(2,1)S(1)} %concatenate.15.small_hbm, ...), custom_call_target="tpu_custom_call" | custom-call | flops 3000000000 | bytes 10000000 | tf_op jit(solution)/shard_map/project/pallas_call | solution.py:609
  51.7 0.7 copy-done.7
  52.4 0.7 copy-done.9
  53.1 0.4 fusion.9
  53.5 0.3 reduce-window.16
  54.1 0.3 reduce-window.24
  54.7 0.7 slice.263
  55.4 0.1 copy.65
  55.6 1.0 multiply_reduce_fusion.3
  56.5 0.2 multiply_reduce_fusion.2
  56.7 0.7 fusion.1
  57.4 0.6 slice.265
  59.3 0.7 pad_bitcast_fusion.2
  60.0 14.0 %all-gather.2 = f32[4,259,128]{2,1,0:T(8,128)S(1)} all-gather(f32[1,259,128]{2,1,0:T(8,128)S(1)} %maximum_bitcast_fusion), channel_id=2, replica_groups=mesh['z'=8,'x'=4,'y'=4,'c'=2] {'x'}, dimensions={0}, use_global_device_ids=true | all-gather | bytes 663040 | tf_op jit(solution)/shard_map/all_gather | solution.py:42
  74.0 0.6 fusion.124
  76.5 0.6 fusion.123
  86.1 0.7 maximum_bitcast_fusion.1
  87.6 0.8 dynamic-slice_convert_fusion
  88.3 62.4 %attend.1.attended = bf16[512,128]{1,0:T(8,128)(2,1)S(1)} custom-call(bf16[512,256]{1,0:T(8,128)(2,1)S(1)} %copy-done.10, bf16[1280,128]{1,0:T(8,128)(2,1)S(1)} %copy-done.8), custom_call_target="tpu_custom_call" | custom-call | flops 4000000000 | bytes 10000000 | tf_op jit(solution)/shard_map/attend/pallas_call | solution.py:297
  150.7 0.8 fusion.119
  151.6 0.6 fusion.122
  154.7 0.6 fusion.121
  174.4 0.8 fusion.116
  175.2 0.1 multiply_reduce_fusion.1
  175.3 0.3 fusion.125
  175.7 1.9 convolution_multiply_fusion.1
  177.7 1.1 multiply_reduce_fusion
  178.7 12.4 %psum.7 = f32[512]{0:T(512)S(1)} all-reduce(f32[512]{0:T(512)S(1)} %get-tuple-element.53), channel_id=1, replica_groups=mesh['z'=8,'x'=4,'y'=4,'c'=2] {'y','c'}, use_global_device_ids=true, to_apply=%region_8.9 | all-reduce | flops 512 | bytes 4096 | tf_op jit(solution)/shard_map/psum | solution.py:916
  191.2 0.2 multiply_convert_fusion.gated
  191.4 14.8 %project_out.1 = bf16[64,2048]{1,0:T(8,128)(2,1)S(1)} custom-call(bf16[512,256]{1,0:T(8,128)(2,1)S(1)} %multiply_convert_fusion.gated, bf16[512,128]{1,0:T(8,128)(2,1)S(1)} %attend.1.attended, bf16[256,2048]{1,0:T(8,128)(2,1)S(1)} %copy-done, bf16[128,2048]{1,0:T(8,128)(2,1)S(1)} %copy-done.3), custom_call_target="tpu_custom_call" | custom-call | flops 1000000000 | bytes 10000000 | tf_op jit(solution)/shard_map/project_out/pallas_call | solution.py:775
  206.2 0.7 copy.71
  (60 shorter events, 1.1 us)
Async XLA Ops:
  6.5 3.8 %copy-start.15 = (bf16[2048,8]{0,1:T(8,128)(2,1)S(1)}, bf16[2048,8]{0,1:T(8,128)(2,1)}, u32[]{:S(2)}) copy-start(bf16[2048,8]{0,1:T(8,128)(2,1)} %param.27) | copy-start | bytes 98308
  6.5 4.9 %copy-start.13 = (bf16[2048,64]{0,1:T(8,128)(2,1)S(1)}, bf16[2048,64]{0,1:T(8,128)(2,1)}, u32[]{:S(2)}) copy-start(bf16[2048,64]{0,1:T(8,128)(2,1)} %param.31) | copy-start | bytes 786436
  6.5 144.2 %all-gather.6.cloned.1.call-start = ((), (), s32[]{:S(2)}) async-start(), calls=%async_computation | async-start | bytes 1216512 | tf_op jit(solution)/shard_map/all_gather | solution.py:42
  8.6 3.9 %copy-start.14 = (bf16[2048,64]{0,1:T(8,128)(2,1)S(1)}, bf16[2048,64]{0,1:T(8,128)(2,1)}, u32[]{:S(2)}) copy-start(bf16[2048,64]{0,1:T(8,128)(2,1)} %param.32) | copy-start | bytes 786436
  10.4 3.1 %copy-start.12 = (bf16[768,192]{0,1:T(8,128)(2,1)S(1)}, bf16[768,192]{0,1:T(8,128)(2,1)}, u32[]{:S(2)}) copy-start(bf16[768,192]{0,1:T(8,128)(2,1)} %param.35) | copy-start | bytes 884740
  11.4 2.2 %copy-start.16 = (f32[768]{0:T(1024)S(1)}, f32[768]{0:T(1024)}, u32[]{:S(2)}) copy-start(f32[768]{0:T(1024)} %param.33) | copy-start | bytes 9220
  11.4 2.3 %copy-start.18 = (f32[512]{0:T(512)S(1)}, f32[512]{0:T(512)}, u32[]{:S(2)}) copy-start(f32[512]{0:T(512)} %param.34) | copy-start | bytes 6148
  13.6 0.8 copy-start.17
  16.3 3.2 %copy-start.1 = (bf16[2048,128]{1,0:T(8,128)(2,1)S(1)}, bf16[2048,128]{1,0:T(8,128)(2,1)}, u32[]{:S(2)}) copy-start(bf16[2048,128]{1,0:T(8,128)(2,1)} %query_hbm.1) | copy-start | bytes 1572868
  19.5 1.0 copy-start.2
  20.5 0.9 copy-start.4
  21.5 0.9 copy-start.5
  22.4 0.9 copy-start.6
  23.3 29.8 %copy-start.11 = (f32[512,1]{1,0:T(8,128)S(1)}, f32[512,1]{1,0:T(8,128)}, u32[]{:S(2)}) copy-start(f32[512,1]{1,0:T(8,128)} %copy.63) | copy-start | bytes 6148
  51.7 0.7 copy-start.7
  52.4 0.7 copy-start.9
  60.0 28.4 %copy-start.8 = (bf16[1280,128]{1,0:T(8,128)(2,1)S(1)}, bf16[1280,128]{1,0:T(8,128)(2,1)}, u32[]{:S(2)}) copy-start(bf16[1280,128]{1,0:T(8,128)(2,1)} %copy-done.7) | copy-start | bytes 983044
  60.0 28.4 %copy-start.10 = (bf16[512,256]{1,0:T(8,128)(2,1)S(1)}, bf16[512,256]{1,0:T(8,128)(2,1)}, u32[]{:S(2)}) copy-start(bf16[512,256]{1,0:T(8,128)(2,1)} %copy-done.9) | copy-start | bytes 786436
  177.6 13.7 %copy-start = (bf16[256,2048]{1,0:T(8,128)(2,1)S(1)}, bf16[256,2048]{1,0:T(8,128)(2,1)}, u32[]{:S(2)}) copy-start(bf16[256,2048]{1,0:T(8,128)(2,1)} %out_memory.1) | copy-start | bytes 3145732
  177.6 13.7 %copy-start.3 = (bf16[128,2048]{1,0:T(8,128)(2,1)S(1)}, bf16[128,2048]{1,0:T(8,128)(2,1)}, u32[]{:S(2)}) copy-start(bf16[128,2048]{1,0:T(8,128)(2,1)} %out_attend.1) | copy-start | bytes 1572868
Sparse Core Ops, SparseCore 0:
  86.9 36.8 all-gather.5

commit v3 on v2

--- a/solution.py
+++ b/solution.py
@@ -12,7 +12,6 @@
 PLAIN_CHANNELS = 128
 ROTARY_CHANNELS = 64
 VALUE_CHANNELS = 128
-BLOCK = 64
 SP = ("z", "x")
 TP = ("y", "c")
 SP_TP = ("z", "x", "y", "c")
@@ -24,56 +23,14 @@
 PRECISE = lax.Precision.HIGHEST
 FAR_BELOW = -1e30
 
-
-def nothing_yet(shard, identity):
-    return jax.tree.map(
-        lambda a, e: jnp.broadcast_to(jnp.asarray(e, a.dtype), a.shape), shard, identity
-    )
-
-
-def gathered_once(shard, axis):
-    leaves = jax.tree.leaves(shard)
-    order = sorted(range(len(leaves)), key=lambda k: -leaves[k].size)
-    width = (1, *leaves[order[0]].shape)[-1]
-    lines = [
-        jnp.pad(leaves[k].reshape(-1), (0, -leaves[k].size % width)).reshape(-1, width)
-        for k in order
-    ]
-    both, at, found = (lax.all_gather(jnp.concatenate(lines), axis), 0, {})
-    for k, line in zip(order, lines):
-        slab = both[:, at : at + len(line)].reshape(len(both), -1)
-        found[k] = slab[:, : leaves[k].size].reshape(-1, *leaves[k].shape)
-        at += len(line)
-    numbers = iter(range(len(leaves)))
-    return jax.tree.map(lambda _: found[next(numbers)], shard)
-
-
-def entering(shard, axes, combine, identity):
-    before = start = nothing_yet(shard, identity)
-    running = shard
-    for axis in reversed(axes):
-        peers, index = (lax.axis_size(axis), lax.axis_index(axis))
-        pieces = gathered_once(running, axis)
-        inside, running = (start, start)
-        for k in range(peers):
-            passed = k < index
-            running = combine(running, jax.tree.map(lambda part: part[k], pieces))
-            inside = jax.tree.map(lambda new, old: jnp.where(passed, new, old), running, inside)
-        before = combine(inside, before)
-    return before
-
-
-def merge_states(earlier, later):
-    decayed = later[3] + earlier[2]
-    joined = jnp.maximum(decayed, later[2])
-    early_part = jnp.exp(decayed - joined)
-    late_part = jnp.exp(later[2] - joined)
-    return (
-        early_part[:, None, None] * earlier[0] + late_part[:, None, None] * later[0],
-        early_part[:, None] * earlier[1] + late_part[:, None] * later[1],
-        joined,
-        earlier[3] + later[3],
-    )
+N_Y = 4
+N_C = 2
+SHARE = 64
+QUERY_LATENT = 768
+LATENT_WIDTH = 512
+QUERY_PART = QUERY_LATENT // (N_Y * N_C)
+LATENT_PART = LATENT_WIDTH // (N_Y * N_C)
+PARAMS = pltpu.CompilerParams
 
 
 LOG2E = 1.4426950408889634
@@ -82,12 +39,38 @@
 ROWS = 512
 MESH_ID = pl.DeviceIdType.MESH
 CONTRACT_LAST = (((1,), (1,)), ((), ()))
+CHUNK = M_QK // N_X
+STATE_ROWS = CHUNK + 8
+NORMAL_ROW, TOP_ROW, DECAY_ROW = CHUNK, CHUNK + 1, CHUNK + 2
+
+
+def merge_states(early, late):
+    moved = early[TOP_ROW : TOP_ROW + 1] + late[DECAY_ROW : DECAY_ROW + 1]
+    late_top = late[TOP_ROW : TOP_ROW + 1]
+    joined = jnp.maximum(moved, late_top)
+    both = early * jnp.exp(moved - joined) + late * jnp.exp(late_top - joined)
+    row = lax.broadcasted_iota(jnp.int32, both.shape, 0)
+    decay = early[DECAY_ROW : DECAY_ROW + 1] + late[DECAY_ROW : DECAY_ROW + 1]
+    return jnp.where(row == TOP_ROW, joined, jnp.where(row == DECAY_ROW, decay, both))
+
+
+def in_two(values):
+    high = values.astype(jnp.bfloat16)
+    return high, (values - high.astype(jnp.float32)).astype(jnp.bfloat16)
+
+
+def as_columns(row, width):
+    return jnp.broadcast_to(row, (width, row.shape[1])).T
 
 
 def attend_kernel(
     q_ref,
     kv_ref,
+    mem_ref,
+    gate_ref,
+    gain_ref,
     o_ref,
+    gated_ref,
     q_all,
     kv_all,
     k_cat,
@@ -98,6 +81,17 @@
     stat_out,
     part_in,
     stat_in,
+    cell,
+    cell_sum,
+    cell_top,
+    first_out,
+    first_in,
+    column_out,
+    column_in,
+    start_out,
+    start_in,
+    square_out,
+    square_in,
     q_send,
     q_recv,
     up_send,
@@ -108,21 +102,42 @@
     part_recv,
     stat_send,
     stat_recv,
+    first_send,
+    first_recv,
+    column_send,
+    column_recv,
+    start_send,
+    start_recv,
+    square_send,
+    square_recv,
 ):
-    z = lax.axis_index("z")
-    x = lax.axis_index("x")
+    f32, bf16 = jnp.float32, jnp.bfloat16
+    z, x = lax.axis_index("z"), lax.axis_index("x")
+    y, c = lax.axis_index("y"), lax.axis_index("c")
     above, below = lax.rem(z + 1, N_Z), lax.rem(z + N_Z - 1, N_Z)
     peers = [lax.rem(x + d, N_X) for d in range(1, N_X)]
-
-    barrier = pltpu.get_barrier_semaphore()
-    for other in (above, below):
-        pl.semaphore_signal(barrier, inc=1, device_id={"z": other}, device_id_type=MESH_ID)
-    for other in peers:
-        pl.semaphore_signal(barrier, inc=1, device_id={"x": other}, device_id_type=MESH_ID)
-    pl.semaphore_wait(barrier, N_X + 1)
-
+    right, left = peers[0], peers[-1]
+    rows_y = [lax.rem(y + d, N_Y) for d in range(1, N_Y)]
     half = kv_ref.shape[0] // 2
     width = PLAIN_CHANNELS
+
+    barrier = pltpu.get_barrier_semaphore()
+    devices = [{"z": lax.rem(z + d, N_Z)} for d in range(1, N_Z)]
+    devices += [{"x": other} for other in peers] + [{"y": other} for other in rows_y]
+    devices.append({"c": 1 - c})
+    for device in devices:
+        pl.semaphore_signal(barrier, inc=1, device_id=device, device_id_type=MESH_ID)
+    pl.semaphore_wait(barrier, len(devices))
+
+    def remote(source, target, send, recv, device):
+        return pltpu.make_async_remote_copy(
+            src_ref=source,
+            dst_ref=target,
+            send_sem=send,
+            recv_sem=recv,
+            device_id=device,
+            device_id_type=MESH_ID,
+        )
 
     def kv_copy(up, step, h):
         shift = (N_Z - step + 1) if up else (step - 1)
@@ -130,66 +145,159 @@
         rows = pl.ds(h * half, half)
         source = kv_ref.at[rows] if step == 1 else kv_all.at[owner, rows]
         send, recv = (up_send, up_recv) if up else (down_send, down_recv)
-        return pltpu.make_async_remote_copy(
-            src_ref=source,
-            dst_ref=kv_all.at[owner, rows],
-            send_sem=send.at[step - 1, h],
-            recv_sem=recv.at[step - 1, h],
-            device_id={"z": above if up else below},
-            device_id_type=MESH_ID,
-        )
-
-    def q_copy(d):
-        return pltpu.make_async_remote_copy(
-            src_ref=q_ref,
-            dst_ref=q_all.at[x],
-            send_sem=q_send.at[d],
-            recv_sem=q_recv.at[d],
-            device_id={"x": peers[d]},
-            device_id_type=MESH_ID,
+        return remote(
+            source,
+            kv_all.at[owner, rows],
+            send.at[step - 1, h],
+            recv.at[step - 1, h],
+            {"z": above if up else below},
+        )
+
+    q_half = ROWS // 2
+
+    def q_copy(number):
+        shift, part, to_right = (
+            (0, 0, True),
+            (0, 1, True),
+            (0, 0, False),
+            (0, 1, False),
+            (N_X - 1, 0, True),
+            (1, 1, False),
+        )[number]
+        owner = lax.rem(x + shift, N_X)
+        rows = pl.ds(part * q_half, q_half)
+        source = q_ref.at[rows] if shift == 0 else q_all.at[owner, rows]
+        return remote(
+            source,
+            q_all.at[owner, rows],
+            q_send.at[number],
+            q_recv.at[number],
+            {"x": right if to_right else left},
         )
 
     def part_copy(d):
-        return pltpu.make_async_remote_copy(
-            src_ref=part_out.at[d],
-            dst_ref=part_in.at[d],
-            send_sem=part_send.at[d],
-            recv_sem=part_recv.at[d],
-            device_id={"x": peers[d]},
-            device_id_type=MESH_ID,
+        return remote(
+            part_out.at[d], part_in.at[d], part_send.at[d], part_recv.at[d], {"x": peers[d]}
         )
 
     def stat_copy(d):
-        return pltpu.make_async_remote_copy(
-            src_ref=stat_out.at[d],
-            dst_ref=stat_in.at[d],
-            send_sem=stat_send.at[d],
-            recv_sem=stat_recv.at[d],
-            device_id={"x": peers[d]},
-            device_id_type=MESH_ID,
+        return remote(
+            stat_out.at[d], stat_in.at[d], stat_send.at[d], stat_recv.at[d], {"x": peers[d]}
+        )
+
+    def first_copy(d):
+        return remote(
+            first_out.at[peers[d]],
+            first_in.at[x],
+            first_send.at[d],
+            first_recv.at[d],
+            {"x": peers[d]},
+        )
+
+    def column_copy(target):
+        return remote(
+            column_out,
+            column_in.at[z],
+            column_send.at[target],
+            column_recv.at[z],
+            {"z": target},
+        )
+
+    def column_arrival(source):
+        return remote(
+            column_out,
+            column_in.at[source],
+            column_send.at[source],
+            column_recv.at[source],
+            {"z": source},
+        )
+
+    def start_copy(d):
+        return remote(
+            start_out.at[peers[d]],
+            start_in.at[x],
+            start_send.at[d],
+            start_recv.at[d],
+            {"x": peers[d]},
+        )
+
+    def square_copy(number):
+        device = {"c": 1 - c} if number == 0 else {"y": rows_y[number - 1]}
+        return remote(
+            square_out.at[min(number, 1)],
+            square_in.at[number],
+            square_send.at[number],
+            square_recv.at[number],
+            device,
         )
 
     started = []
+
+    def start(copy):
+        copy.start()
+        started.append(copy)
+
     for h in range(2):
         for up in (True, False):
-            copy = kv_copy(up, 1, h)
-            copy.start()
-            started.append(copy)
+            start(kv_copy(up, 1, h))
+    for number in (0, 3, 1, 2):
+        start(q_copy(number))
+
+    q_all[x] = q_ref[...]
+    top[...] = jnp.full(top.shape, FAR_BELOW, f32)
+    total[...] = jnp.zeros(total.shape, f32)
+    accum[...] = jnp.zeros(accum.shape, f32)
+
+    relative, cumulative = gate_ref[0:1], gate_ref[1:2]
+    key_scale = M_QK ** (-0.5)
+    tall = 256
+    for t in range(ROWS // tall):
+        rows, seen = slice(t * tall, (t + 1) * tall), (t + 1) * tall
+        row = lax.broadcasted_iota(jnp.int32, (tall, seen), 0) + t * tall
+        col = lax.broadcasted_iota(jnp.int32, (tall, seen), 1)
+        logs = jnp.where(col <= row, relative[:, :seen], -jnp.inf)
+        highest = jnp.max(logs, axis=1, keepdims=True)
+        affinity = lax.dot_general(
+            mem_ref[rows, :M_QK],
+            mem_ref[:seen, M_QK : 2 * M_QK],
+            CONTRACT_LAST,
+            preferred_element_type=f32,
+        )
+        affinity = affinity * (jnp.exp(logs - highest) * key_scale)
+        values = mem_ref[:seen, 2 * M_QK : 2 * M_QK + M_V]
+        cell[rows] = sum(
+            jnp.dot(piece, values, preferred_element_type=f32) for piece in in_two(affinity)
+        )
+        cell_sum[rows] = jnp.broadcast_to(
+            jnp.sum(affinity, axis=1, keepdims=True), (tall, width)
+        )
+        cell_top[rows] = jnp.broadcast_to(highest, (tall, width))
+    ends_at = jnp.max(relative, axis=1, keepdims=True)
+    weights = jnp.exp(relative - ends_at) * key_scale
+    wide_key = mem_ref[:, M_QK : 2 * M_QK].astype(f32)
+    normal = jnp.sum(as_columns(weights, width) * wide_key, axis=0, keepdims=True)
+    values = mem_ref[:, 2 * M_QK : 2 * M_QK + M_V]
+    matrix = sum(
+        jnp.dot(piece, values, preferred_element_type=f32)
+        for piece in in_two(wide_key.T * weights)
+    )
+    decay = cumulative[:, ROWS - 1 : ROWS]
+    row = lax.broadcasted_iota(jnp.int32, (8, M_V), 0)
+    lines = jnp.concatenate([normal, jnp.zeros_like(normal)], axis=1)
+    notes = jnp.where(
+        row == 0, lines, jnp.where(row == 1, ends_at + decay, jnp.where(row == 2, decay, 0.0))
+    )
+    for k in range(N_X):
+        first_out[k, :CHUNK] = matrix[k * CHUNK : (k + 1) * CHUNK]
+        first_out[k, CHUNK:] = notes
     for d in range(N_X - 1):
-        copy = q_copy(d)
-        copy.start()
-        started.append(copy)
-
-    q_all[x] = q_ref[...]
-    top[...] = jnp.full(top.shape, FAR_BELOW, jnp.float32)
-    total[...] = jnp.zeros(total.shape, jnp.float32)
-    accum[...] = jnp.zeros(accum.shape, jnp.float32)
+        start(first_copy(d))
+    first_in[x] = first_out[x]
 
     lane = lax.broadcasted_iota(jnp.int32, (ROWS // 2, width), 1)
-    low = (lane < ROTARY_CHANNELS).astype(jnp.bfloat16)
-    high = (lane >= ROTARY_CHANNELS).astype(jnp.bfloat16)
+    low = (lane < ROTARY_CHANNELS).astype(bf16)
+    high = (lane >= ROTARY_CHANNELS).astype(bf16)
     scale = LOG2E * (PLAIN_CHANNELS + ROTARY_CHANNELS) ** (-0.5)
-    tall = 256
 
     def keys_from(ref):
         k_cat[:, :width] = ref[:ROWS]
@@ -197,14 +305,14 @@
         k_cat[: ROWS // 2, width:] = packed * low
         k_cat[ROWS // 2 :, width:] = packed * high
 
-    def attend(first, last, values, masked):
+    def attend_rows(first, last, values, masked):
         def one(t, carry):
             shard = t // (ROWS // tall)
             rows = pl.ds(pl.multiple_of(t * tall, tall), tall)
             inner = pl.ds(pl.multiple_of((t % (ROWS // tall)) * tall, tall), tall)
             queries = q_all[shard, inner]
             scores = lax.dot_general(
-                queries, k_cat[...], CONTRACT_LAST, preferred_element_type=jnp.float32
+                queries, k_cat[...], CONTRACT_LAST, preferred_element_type=f32
             )
             scores = scores * scale
             if masked:
@@ -217,43 +325,108 @@
             shrink = jnp.exp2(old - new)
             total[rows] = total[rows] * shrink + jnp.sum(probs, axis=1, keepdims=True)
             accum[rows] = accum[rows] * shrink + jnp.dot(
-                probs.astype(jnp.bfloat16), values(), preferred_element_type=jnp.float32
+                probs.astype(bf16), values(), preferred_element_type=f32
             )
             top[rows] = new
             return carry
 
         lax.fori_loop(first, last, one, 0)
-
-    steps = ROWS // tall
-    keys_from(kv_ref)
-    own_values = lambda: kv_ref[ROWS : 2 * ROWS]
-    attend(x * steps, (x + 1) * steps, own_values, True)
-    for d in range(N_X - 1):
-        q_copy(d).wait_recv()
-    attend((x + 1) * steps, N_X * steps, own_values, False)
 
     def arrived(owner, useful):
         @pl.when(useful)
         def _():
             keys_from(kv_all.at[owner])
-            attend(0, N_X * steps, lambda: kv_all[owner, ROWS : 2 * ROWS], False)
+            attend_rows(0, N_X * steps, lambda: kv_all[owner, ROWS : 2 * ROWS], False)
 
     last = N_Z // 2
-    for step in range(1, last + 1):
+
+    def take(step):
         for h in range(2):
             for up in (True, False):
                 if step == last and up != (h == 0):
                     continue
                 kv_copy(up, step, h).wait_recv()
                 if step < last - 1 or (step == last - 1 and up == (h == 0)):
-                    copy = kv_copy(up, step + 1, h)
-                    copy.start()
-                    started.append(copy)
+                    start(kv_copy(up, step + 1, h))
+
+    def use(step):
+        arrived(lax.rem(z + N_Z - step, N_Z), z >= step)
         if step < last:
-            arrived(lax.rem(z + N_Z - step, N_Z), z >= step)
             arrived(lax.rem(z + step, N_Z), z + step >= N_Z)
-        else:
-            arrived(lax.rem(z + step, N_Z), z >= step)
+
+    steps = ROWS // tall
+    keys_from(kv_ref)
+    own_values = lambda: kv_ref[ROWS : 2 * ROWS]
+    attend_rows(x * steps, (x + 1) * steps, own_values, True)
+
+    for d in range(N_X - 1):
+        first_copy(d).wait_recv()
+    column = first_in[0]
+    for k in range(1, N_X):
+        column = merge_states(column, first_in[k])
+    column_out[...] = column
+    for target in range(1, N_Z):
+
+        @pl.when(target > z)
+        def _(target=target):
+            column_copy(target).start()
+
+    q_copy(0).wait_recv()
+    start(q_copy(4))
+    q_copy(3).wait_recv()
+    start(q_copy(5))
+    take(1)
+    for number in (1, 2, 4, 5):
+        q_copy(number).wait_recv()
+    attend_rows((x + 1) * steps, N_X * steps, own_values, False)
+
+    def gather_column(k, state):
+        column_arrival(k).wait_recv()
+        return merge_states(state, column_in[k])
+
+    state = lax.fori_loop(0, z, gather_column, jnp.zeros((STATE_ROWS, M_V), f32))
+    for k in range(N_X):
+        start_out[k] = state
+        if k < N_X - 1:
+            state = merge_states(state, first_in[k])
+    for d in range(N_X - 1):
+        start(start_copy(d))
+    start_in[x] = start_out[x]
+    use(1)
+    take(2)
+
+    for d in range(N_X - 1):
+        start_copy(d).wait_recv()
+    carried = jnp.concatenate([start_in[k, :CHUNK] for k in range(N_X)], axis=0)
+    carried_normal = start_in[0, NORMAL_ROW : NORMAL_ROW + 1, :M_QK]
+    carried_top = start_in[0, TOP_ROW : TOP_ROW + 1, :width]
+    queries = mem_ref[:, :M_QK]
+    from_start = sum(
+        jnp.dot(queries, piece, preferred_element_type=f32) for piece in in_two(carried)
+    )
+    highest = jnp.maximum(carried_top, cell_top[...])
+    across, within = jnp.exp(carried_top - highest), jnp.exp(cell_top[...] - highest)
+    twice = lambda one: jnp.concatenate([one, one], axis=1)
+    numerator = cell[...] * twice(within) + from_start * twice(across)
+    denominator = cell_sum[...] * within + across * jnp.sum(
+        queries.astype(f32) * carried_normal, axis=1, keepdims=True
+    )
+    floor = jnp.exp(-(as_columns(cumulative, width) + highest))
+    made = numerator / twice(jnp.maximum(jnp.abs(denominator), floor))
+    cell[...] = made
+    squares = jnp.sum(made * made, axis=1, keepdims=True)
+    square_out[0] = jnp.broadcast_to(squares, (ROWS, width)).T[:8]
+    start(square_copy(0))
+
+    use(2)
+    take(3)
+    square_copy(0).wait_recv()
+    square_out[1] = square_out[0] + square_in[0]
+    for number in range(1, N_Y):
+        start(square_copy(number))
+    use(3)
+    take(4)
+    use(4)
 
     def finish(shard):
         rows = pl.ds(pl.multiple_of(shard * ROWS, ROWS), ROWS)
@@ -262,19 +435,27 @@
         log_total = jnp.where(seen, top[rows] + jnp.log2(summed), FAR_BELOW)
         return accum[rows] / summed, log_total
 
+    for d in (1, 0, 2):
+        part, log_total = finish(peers[d])
+        part_out[d] = part.astype(bf16)
+        stat_out[d] = log_total.T[:8]
+        start(part_copy(d))
+        start(stat_copy(d))
+
+    squares = square_out[1]
+    for number in range(1, N_Y):
+        square_copy(number).wait_recv()
+        squares = squares + square_in[number]
+    inverse = lax.rsqrt(squares[:1] / (MEMORY_HEADS * M_V) + SMALL_CONSTANT)
+    gated = cell[...] * twice(as_columns(inverse, width)) * gain_ref[...].astype(f32)
+    gated = gated * jax.nn.sigmoid(mem_ref[:, 2 * M_QK + M_V :].astype(f32))
+    gated_ref[...] = gated.astype(bf16)
+
+    own, own_log = finish(x)
+    logs = []
     for d in range(N_X - 1):
-        part, log_total = finish(peers[d])
-        part_out[d] = part.astype(jnp.bfloat16)
-        stat_out[d] = log_total.T[:8]
-        for copy in (part_copy(d), stat_copy(d)):
-            copy.start()
-            started.append(copy)
-    own, own_log = finish(x)
-    parts, logs = [], []
-    for d in range(N_X - 1):
-        part_copy(d).wait_recv()
         stat_copy(d).wait_recv()
-        logs.append(jnp.broadcast_to(stat_in[d, 0:1, :], (width, ROWS)).T)
+        logs.append(as_columns(stat_in[d, 0:1, :], width))
     highest = own_log
     for one in logs:
         highest = jnp.maximum(highest, one)
@@ -282,23 +463,35 @@
     numerator = own * weight
     denominator = weight
     for d in range(N_X - 1):
+        part_copy(d).wait_recv()
         weight = jnp.exp2(logs[d] - highest)
-        numerator = numerator + part_in[d].astype(jnp.float32) * weight
+        numerator = numerator + part_in[d].astype(f32) * weight
         denominator = denominator + weight
-    o_ref[...] = (numerator / denominator).astype(jnp.bfloat16)
+    o_ref[...] = (numerator / denominator).astype(bf16)
     for copy in started:
         copy.wait_send()
-
-
-def attend(queries, keys_values):
+    for target in range(1, N_Z):
+
+        @pl.when(target > z)
+        def _(target=target):
+            column_copy(target).wait_send()
+
+
+def attend(queries, keys_values, memory_inputs, gates, gain):
     f32, bf16 = jnp.float32, jnp.bfloat16
     last = N_Z // 2
     dma = pltpu.SemaphoreType.DMA
+    vmem = pl.BlockSpec(memory_space=pltpu.VMEM)
+    state = (STATE_ROWS, M_V)
+    peers = (N_X - 1,)
     return pl.pallas_call(
         attend_kernel,
-        out_shape=jax.ShapeDtypeStruct((ROWS, VALUE_CHANNELS), bf16),
-        in_specs=[pl.BlockSpec(memory_space=pltpu.VMEM)] * 2,
-        out_specs=pl.BlockSpec(memory_space=pltpu.VMEM),
+        out_shape=(
+            jax.ShapeDtypeStruct((ROWS, VALUE_CHANNELS), bf16),
+            jax.ShapeDtypeStruct((ROWS, M_V), bf16),
+        ),
+        in_specs=[vmem] * 5,
+        out_specs=[vmem] * 2,
         scratch_shapes=[
             pltpu.VMEM((N_X, ROWS, 256), bf16),
             pltpu.VMEM((N_Z, *keys_values.shape), bf16),
@@ -310,16 +503,35 @@
             pltpu.VMEM((N_X - 1, 8, ROWS), f32),
             pltpu.VMEM((N_X - 1, ROWS, VALUE_CHANNELS), bf16),
             pltpu.VMEM((N_X - 1, 8, ROWS), f32),
-            dma((N_X - 1,)),
-            dma((N_X - 1,)),
+            pltpu.VMEM((ROWS, M_V), f32),
+            pltpu.VMEM((ROWS, 128), f32),
+            pltpu.VMEM((ROWS, 128), f32),
+            pltpu.VMEM((N_X, *state), f32),
+            pltpu.VMEM((N_X, *state), f32),
+            pltpu.VMEM(state, f32),
+            pltpu.VMEM((N_Z, *state), f32),
+            pltpu.VMEM((N_X, *state), f32),
+            pltpu.VMEM((N_X, *state), f32),
+            pltpu.VMEM((2, 8, ROWS), f32),
+            pltpu.VMEM((N_Y, 8, ROWS), f32),
+            dma((6,)),
+            dma((6,)),
             dma((last, 2)),
             dma((last, 2)),
             dma((last, 2)),
             dma((last, 2)),
-            dma((N_X - 1,)),
-            dma((N_X - 1,)),
-            dma((N_X - 1,)),
-            dma((N_X - 1,)),
+            dma(peers),
+            dma(peers),
+            dma(peers),
+            dma(peers),
+            dma(peers),
+            dma(peers),
+            dma((N_Z,)),
+            dma((N_Z,)),
+            dma(peers),
+            dma(peers),
+            dma((N_Y,)),
+            dma((N_Y,)),
         ],
         compiler_params=pltpu.CompilerParams(
             collective_id=1, has_side_effects=True, vmem_limit_bytes=48 * 1024 * 1024
@@ -328,17 +540,7 @@
             flops=4 * 10**9, bytes_accessed=10**7, transcendentals=4 * 10**6
         ),
         name="attend",
-    )(queries, keys_values)
-
-
-N_Y = 4
-N_C = 2
-SHARE = 64
-QUERY_LATENT = 768
-LATENT_WIDTH = 512
-QUERY_PART = QUERY_LATENT // (N_Y * N_C)
-LATENT_PART = LATENT_WIDTH // (N_Y * N_C)
-PARAMS = pltpu.CompilerParams
+    )(queries, keys_values, memory_inputs, gates, gain)
 
 
 class TpGather:
@@ -419,17 +621,22 @@
 def project_kernel(
     tokens,
     gain,
-    small_hbm,
+    gains,
+    cosine,
+    sine_part,
+    shift_row,
+    narrow_query,
+    narrow_latent,
+    narrow_rotary,
+    narrow_ingate,
+    narrow_forget,
     query_hbm,
     key_hbm,
     value_hbm,
     outgate_hbm,
-    query_up,
-    key_up,
-    value_up,
-    gains,
-    cosine,
-    sine_part,
+    query_up_hbm,
+    key_up_hbm,
+    value_up_hbm,
     mem_ref,
     gate_ref,
     q_ref,
@@ -437,7 +644,13 @@
     rows_all,
     latents,
     small,
+    ingate,
+    forget,
     big,
+    query_up,
+    key_up,
+    value_up,
+    pre_gates,
     up_query,
     up_latent,
     wide_query,
@@ -452,12 +665,25 @@
     y, c = lax.axis_index("y"), lax.axis_index("c")
     mine = y * N_C + c
     width = 128
-    loads = [pltpu.make_async_copy(small_hbm, small, load_sem.at[0])]
+    sources = (
+        (narrow_query, small.at[pl.ds(0, QUERY_PART)]),
+        (narrow_latent, small.at[pl.ds(width, LATENT_PART)]),
+        (narrow_rotary, small.at[pl.ds(width + LATENT_PART, ROTARY_CHANNELS)]),
+        (narrow_ingate, ingate),
+        (narrow_forget, forget),
+        (query_up_hbm, query_up),
+        (key_up_hbm, key_up),
+        (value_up_hbm, value_up),
+    )
+    loads = [
+        pltpu.make_async_copy(source, target, load_sem.at[k])
+        for k, (source, target) in enumerate(sources)
+    ]
     at = 0
     for k, ref in enumerate((query_hbm, key_hbm, value_hbm, outgate_hbm)):
         columns = ref.shape[1]
         loads.append(
-            pltpu.make_async_copy(ref, big.at[:, pl.ds(at, columns)], load_sem.at[1 + k])
+            pltpu.make_async_copy(ref, big.at[:, pl.ds(at, columns)], load_sem.at[8 + k])
         )
         at += columns
     for load in loads:
@@ -466,6 +692,7 @@
     wide = tokens[...].astype(f32)
     inverse = lax.rsqrt(jnp.mean(wide * wide, axis=1, keepdims=True) + SMALL_CONSTANT)
     rows_all[mine] = (wide * inverse * gain[...].astype(f32)).astype(bf16)
+    small[QUERY_PART:width] = jnp.zeros((width - QUERY_PART, small.shape[1]), bf16)
 
     barrier = pltpu.get_barrier_semaphore()
     greet_tp(barrier)
@@ -473,6 +700,8 @@
     gather = TpGather(rows_all, row_send, row_recv)
     gather.start()
 
+    for load in loads:
+        load.wait()
     up_query[...] = jnp.zeros(up_query.shape, bf16)
     for s in range(N_Y * N_C):
         up_query[s * width : s * width + QUERY_PART] = query_up[
@@ -483,8 +712,6 @@
             at = s * width + h * LATENT_PART
             up_latent[at : at + LATENT_PART, :width] = key_up[part]
             up_latent[at : at + LATENT_PART, width:] = value_up[part]
-    for load in loads:
-        load.wait()
 
     lane = lax.broadcasted_iota(jnp.int32, (1, width), 1)
     row_id = lax.broadcasted_iota(jnp.int32, (width, width), 0)
@@ -514,8 +741,12 @@
 
     def project_small(chip):
         rows = pl.ds(pl.multiple_of(chip * span, span), span)
-        made = jnp.dot(chip_rows(chip), small[...], preferred_element_type=f32)
-        gate_ref[rows] = made[:, :width]
+        here = chip_rows(chip)
+        made = lax.dot_general(here, small[...], CONTRACT_LAST, preferred_element_type=f32)
+        for k, ref in enumerate((ingate, forget)):
+            pre_gates[k, :, rows] = lax.dot_general(
+                ref[...], here, CONTRACT_LAST, preferred_element_type=f32
+            )
         rounded = made.astype(bf16)
         latents[mine, rows] = rounded[:, :width]
         wide_latent[rows, :width] = rounded[:, width:]
@@ -552,6 +783,29 @@
     exchange.relay()
     for chip in (near[2], opposite):
         project_big(chip)
+    heads = lax.broadcasted_iota(jnp.int32, (8, ROWS), 0) == mine
+    in_pre, forget_pre = (
+        jnp.sum(jnp.where(heads, pre_gates[k], 0.0), axis=0, keepdims=True) for k in range(2)
+    )
+    in_gate = SOFTCAP * jnp.tanh(in_pre / SOFTCAP)
+    capped = SOFTCAP * jnp.tanh((forget_pre + shift_row[...]) / SOFTCAP)
+    small_part = jnp.exp(-jnp.abs(capped))
+    above_one = 1.0 + small_part
+    grown = jnp.where(
+        above_one == 1.0, small_part, jnp.log(above_one) * small_part / (above_one - 1.0)
+    )
+    log_forget = jnp.minimum(capped, 0.0) - grown
+    earlier = lax.broadcasted_iota(jnp.int32, (ROWS, ROWS), 0) <= lax.broadcasted_iota(
+        jnp.int32, (ROWS, ROWS), 1
+    )
+    cumulative = jnp.dot(
+        jnp.broadcast_to(log_forget, (8, ROWS)),
+        earlier.astype(f32),
+        precision=PRECISE,
+        preferred_element_type=f32,
+    )
+    top_rows = lax.broadcasted_iota(jnp.int32, (8, ROWS), 0) == 0
+    gate_ref[...] = jnp.where(top_rows, in_gate - cumulative, cumulative)
     key_turned = rotated(second, LATENT_PART)
     kv_ref[2 * ROWS :] = jnp.where(
         lane < ROTARY_CHANNELS, key_turned[:half], key_turned[half:]
@@ -599,33 +853,37 @@
     exchange.finish()
 
 
-def project(tokens, gain, small, query, key, value, outgate, ups, gains, cosine, sine_part):
+def project(dense, narrow, weights):
     f32, bf16 = jnp.float32, jnp.bfloat16
-    depth = tokens.shape[1]
+    depth = weights[0].shape[0]
     dma = pltpu.SemaphoreType.DMA
     vmem = pl.BlockSpec(memory_space=pltpu.VMEM)
     hbm = pl.BlockSpec(memory_space=pl.ANY)
-    mem_width = query.shape[1] + key.shape[1] + value.shape[1] + outgate.shape[1]
+    mem_width = sum(one.shape[1] for one in weights[:4])
     return pl.pallas_call(
         project_kernel,
         out_shape=(
             jax.ShapeDtypeStruct((ROWS, mem_width), bf16),
-            jax.ShapeDtypeStruct((ROWS, 128), f32),
+            jax.ShapeDtypeStruct((8, ROWS), f32),
             jax.ShapeDtypeStruct((ROWS, 256), bf16),
             jax.ShapeDtypeStruct((ROWS * 5 // 2, 128), bf16),
         ),
-        in_specs=[vmem] * 2 + [hbm] * 5 + [vmem] * 6,
+        in_specs=[vmem] * len(dense) + [hbm] * (len(narrow) + len(weights)),
         out_specs=[vmem] * 4,
         scratch_shapes=[
             pltpu.VMEM((N_Y * N_C, SHARE, depth), bf16),
             pltpu.VMEM((N_Y * N_C, ROWS * 3 // 2, 128), bf16),
-            pltpu.VMEM((depth, 256), bf16),
+            pltpu.VMEM((256, depth), bf16),
+            pltpu.VMEM((8, depth), bf16),
+            pltpu.VMEM((8, depth), bf16),
             pltpu.VMEM((depth, mem_width), bf16),
+            *(pltpu.VMEM(one.shape, bf16) for one in weights[4:]),
+            pltpu.VMEM((2, 8, ROWS), f32),
             pltpu.VMEM((1024, PLAIN_CHANNELS + ROTARY_CHANNELS), bf16),
             pltpu.VMEM((1024, 256), bf16),
             pltpu.VMEM((ROWS, 1024), bf16),
             pltpu.VMEM((ROWS, 1024), bf16),
-            dma((5,)),
+            dma((12,)),
             dma((11,)),
             dma((11,)),
             dma((11,)),
@@ -638,7 +896,7 @@
             flops=3 * 10**9, bytes_accessed=10**7, transcendentals=10**4
         ),
         name="project",
-    )(tokens, gain, small, query, key, value, outgate, *ups, gains, cosine, sine_part)
+    )(*dense, *narrow, *weights)
 
 
 def output_kernel(
@@ -817,20 +1075,7 @@
     out_memory,
     out_attend,
 ):
-    tp_index = lax.axis_index(TP)
-    mem_heads = weight_query.shape[1] // M_QK
     length = forget_shift.shape[0]
-    small = jnp.concatenate(
-        [
-            query_down_weight,
-            weight_ingate,
-            weight_forget,
-            jnp.zeros((tokens.shape[1], 16), jnp.bfloat16),
-            latent_down_weight,
-            down_rotary,
-        ],
-        axis=1,
-    )
     latent_rows = latent_gain.reshape(8, LATENT_PART)
     gains = jnp.concatenate(
         [
@@ -844,85 +1089,27 @@
     inverse = jnp.power(ROTARY_BASE, -jnp.arange(halfway, dtype=jnp.float32) / halfway)
     angles = positions.astype(jnp.float32)[:, None] * inverse
     cosine, sine_part = (jnp.tile(made, (1, 4)) for made in (jnp.cos(angles), jnp.sin(angles)))
-    memory_inputs, pre_gates, queries, keys_values = project(
-        tokens,
-        input_gain[None, :],
-        small,
-        weight_query,
-        weight_key,
-        weight_value,
-        weight_outgate,
-        (query_up_weight, key_up_weight, value_up_weight),
-        gains,
-        cosine,
-        sine_part,
-    )
-    mem_query = memory_inputs[:, :M_QK]
-    mem_key = memory_inputs[:, M_QK : 2 * M_QK]
-    mem_value = memory_inputs[:, 2 * M_QK : 2 * M_QK + M_V]
-    mem_outgate = memory_inputs[:, 2 * M_QK + M_V :]
-    in_pre = lax.dynamic_slice_in_dim(pre_gates, QUERY_PART + tp_index, 1, 1)
-    forget_pre = lax.dynamic_slice_in_dim(pre_gates, QUERY_PART + 8 + tp_index, 1, 1)
-    in_gate = SOFTCAP * jnp.tanh(in_pre / SOFTCAP)
-    log_forget = jax.nn.log_sigmoid(SOFTCAP * jnp.tanh((forget_pre + forget_shift) / SOFTCAP))
-    cumulative = jnp.cumsum(log_forget[:, 0])
-    relative = in_gate[:, 0] - cumulative
-    running = lax.cummax(relative)
-    ends_at = running[-1]
-    key_scale = M_QK ** (-0.5)
-    wide_value = mem_value.astype(jnp.float32)
-    weights = jnp.exp(relative - ends_at) * key_scale
-    local_matrix = lax.dot_general(
-        weights[:, None] * wide_value,
-        mem_key.astype(jnp.float32),
-        (((0,), (0,)), ((), ())),
-        precision=PRECISE,
-    )
-    local_normal = jnp.sum(weights[:, None] * mem_key.astype(jnp.float32), axis=0)
-    local_state = (
-        local_matrix[None],
-        local_normal[None],
-        (cumulative[-1] + ends_at)[None],
-        cumulative[-1:],
-    )
-    identity = (
-        jnp.zeros((mem_heads, M_V, M_QK), jnp.float32),
-        jnp.zeros((mem_heads, M_QK), jnp.float32),
-        jnp.full((mem_heads,), FAR_BELOW, jnp.float32),
-        jnp.zeros((mem_heads,), jnp.float32),
-    )
-    prefix = entering(local_state, SP, merge_states, identity)
-    start_max = jnp.maximum(prefix[3], prefix[2])
-    rescale = jnp.exp(prefix[2] - start_max)
-    start_matrix = (prefix[0] * rescale[:, None, None])[0]
-    start_normal = (prefix[1] * rescale[:, None])[0]
-    highest = jnp.maximum(start_max[0], running)
-    causal = jnp.tril(jnp.ones((length, length), dtype=bool))
-    within = jnp.where(causal, relative[None, :] - highest[:, None], -jnp.inf)
-    affinity = lax.dot_general(
-        mem_query, mem_key, (((1,), (1,)), ((), ())), preferred_element_type=jnp.float32
-    )
-    affinity = affinity * (jnp.exp(within) * key_scale)
-    across = jnp.exp(start_max[0] - highest)
-    wide_query = mem_query.astype(jnp.float32)
-    numerator = jnp.dot(affinity, wide_value, precision=PRECISE) + across[:, None] * lax.dot_general(
-        wide_query, start_matrix, (((1,), (1,)), ((), ())), precision=PRECISE
-    )
-    denominator = jnp.sum(affinity, axis=1) + across * jnp.sum(
-        wide_query * start_normal[None, :], axis=1
-    )
-    floor = jnp.exp(-(cumulative + highest))
-    cell = numerator / jnp.maximum(jnp.abs(denominator), floor)[:, None]
-    cell_total = lax.psum(jnp.sum(cell * cell, axis=1), TP)
-    gain_part = lax.dynamic_slice_in_dim(mem_gain, tp_index * mem_heads * M_V, mem_heads * M_V, 0)
-    gated = (
-        cell
-        * lax.rsqrt(cell_total / (MEMORY_HEADS * M_V) + SMALL_CONSTANT)[:, None]
-        * gain_part.astype(jnp.float32)
-    )
-    gated = gated * jax.nn.sigmoid(mem_outgate.astype(jnp.float32))
-    gated = gated.astype(jnp.bfloat16)
-    attended = attend(queries, keys_values)
+    memory_inputs, gates, queries, keys_values = project(
+        (tokens, input_gain[None, :], gains, cosine, sine_part, forget_shift.T),
+        (
+            query_down_weight.T,
+            latent_down_weight.T,
+            down_rotary.T,
+            weight_ingate.T,
+            weight_forget.T,
+        ),
+        (
+            weight_query,
+            weight_key,
+            weight_value,
+            weight_outgate,
+            query_up_weight,
+            key_up_weight,
+            value_up_weight,
+        ),
+    )
+    gain_part = lax.dynamic_slice_in_dim(mem_gain, lax.axis_index(TP) * M_V, M_V, 0)
+    attended, gated = attend(queries, keys_values, memory_inputs, gates, gain_part[None, :])
     return project_out(gated, attended, out_memory, out_attend)
 
 

time: 216 us -> 130 us (0.60)
  between operations: 48.2 us -> 0.23 us
  blocking collectives: 26.4 us -> 0 us
  local copies, waits for them, and re-layouts: 24.1 us -> 14.6 us
  Pallas kernels: 106 us -> 114 us
  other arithmetic: 5.43 us -> 0.4 us
  matrix products: 4.03 us -> 0 us
    all_gather x1 -> x0, blocking collectives: 14 us -> none  [gathered_once(): both, at, found = (lax.all_gather(jnp.concatenate(lines), axis), 0, {})]
    psum x1 -> x0, blocking collectives: 12.4 us -> none  [per_device(): cell_total = lax.psum(jnp.sum(cell * cell, axis=1), TP)]
    pallas_call x1, Pallas kernels: 62.4 us -> 68.1 us  [attend(): pl.pallas_call(attend_kernel, out_shape=(jax.ShapeDtypeStruct((ROWS, VALU...]
    slice x9 -> x0, local copies, waits for them, and re-layouts: 4.62 us -> none  [the longest x4 2.44 us: entering(): running = combine(running, jax.tree.map(lambda part: part[k], pieces))]
    dot_general x4 -> x0, matrix products: 4.03 us -> none  [the longest x1 1.95 us: per_device(): lax.dot_general(wide_query, start_matrix, (((1,), (1,)), ((), ())), preci...]
    concatenate x1 -> x0, local copies, waits for them, and re-layouts: 3.17 us -> none  [per_device(): jnp.concatenate([query_down_weight, weight_ingate, weight_forget, jnp.zer...]
    mul x3 -> x0, other arithmetic: 2.17 us -> none  [the longest x1 0.96 us: per_device(): weights = jnp.exp(relative - ends_at) * key_scale]
  transfers between devices with their start and end apart: 1 -> 0, of which waited for: 0 -> 0; matrix products, arithmetic and copies ran while one was open for 0% -> 0% of each run, Pallas kernels for 29% -> 0%
where the time goes in v3:
time: 130 us; the launch traced here: 129 us
  Pallas kernels  114 us (88%)
  local copies, waits for them, and re-layouts  14.6 us (11%)
    pallas_call x1, Pallas kernels, attend(): pl.pallas_call(attend_kernel, out_shape=(jax.ShapeDtypeStruct((ROWS, VALU...  68.1 us
    pallas_call x1, Pallas kernels, project(): pl.pallas_call(project_kernel, out_shape=(jax.ShapeDtypeStruct((ROWS, mem...  30.1 us
    pallas_call x1, Pallas kernels, project_out(): pl.pallas_call(output_kernel, out_shape=jax.ShapeDtypeStruct((SHARE, 2 *...  16 us
    unnamed x46, local copies, waits for them, and re-layouts  12.7 us

profile of v3, /device:TPU:224, one launch (start us, length us, event | category | flops | bytes accessed | tf_op | source)
XLA Modules:
  0.0 129.4 jit_solution(499828771650876934)
XLA Ops:
  0.0 0.0 copy-start.20
  0.0 0.7 broadcast_in_dim.8.gain
  0.7 0.0 copy-done.20
  0.7 0.0 copy-start.21
  0.7 0.1 reshape.76
  0.8 0.6 copy-done.21
  1.4 0.1 reshape.77
  1.5 0.0 copy-start.12
  1.5 0.1 select_maximum_fusion.gains
  1.6 0.0 copy-start.5
  1.6 0.3 multiply_sine_fusion
  1.9 0.0 copy-start.3
  1.9 0.0 copy-start
  1.9 0.1 copy.22.cosine
  2.1 0.0 copy-start.2
  2.1 0.1 copy.23.sine_part
  2.2 0.0 copy-start.11
  2.3 0.0 copy-start.13
  2.3 1.3 %copy.24.query_up_hbm = bf16[768,192]{1,0:T(8,128)(2,1)S(1)} copy(bf16[768,192]{0,1:T(8,128)(2,1)} %param.35) | data formatting | bytes 589824 | tf_op args[15]
  3.6 0.0 copy-done.12
  3.6 0.0 copy-done.5
  3.6 0.0 copy-done.3
  3.6 0.0 copy-done
  3.6 0.0 copy-done.2
  3.6 0.0 copy-done.11
  3.6 0.0 copy-done.13
  3.7 0.0 copy-start.6
  3.7 0.9 copy-done.6
  4.6 0.0 copy-start.7
  4.6 0.9 copy-done.7
  5.6 0.0 copy-start.8
  5.6 0.9 copy-done.8
  6.5 0.9 copy-done.9
  7.4 0.9 copy-done.10
  8.3 30.1 %project.1 = (bf16[512,768]{1,0:T(8,128)(2,1)S(1)}, f32[8,512]{1,0:T(8,128)S(1)}, bf16[512,256]{1,0:T(8,128)(2,1)S(1)}, bf16[1280,128]{1,0:T(8,128)(2,1)S(1)}) custom-call(bf16[64,2048]{1,0:T(8,128)(2,1)S(1)} %copy-done.6, bf16[1,2048]{1,0:T(2,128)(2,1)S(1)} %broadcast_in_dim.8.gain, f32[16,128]{1,0:T(8,128)S(1)} %select_maximum_fusion.gains, ...), custom_call_target="tpu_custom_call" | custom-call | flops 3000000000 | bytes 10000000 | tf_op jit(solution)/shard_map/project/pallas_call | solution.py:863
  38.4 0.0 copy-start.14
  38.4 0.9 copy-done.14
  39.3 0.7 copy-done.16
  40.1 0.7 copy-done.18
  40.8 0.8 dynamic_slice.3
  41.5 1.1 copy-done.15
  42.7 1.0 copy-done.17
  43.6 0.9 copy-done.19
  44.6 68.1 %attend.1 = (bf16[512,128]{1,0:T(8,128)(2,1)S(1)}, bf16[512,256]{1,0:T(8,128)(2,1)S(1)}) custom-call(bf16[512,256]{1,0:T(8,128)(2,1)S(1)} %copy-done.19, bf16[1280,128]{1,0:T(8,128)(2,1)S(1)} %copy-done.17, bf16[512,768]{1,0:T(8,128)(2,1)S(1)} %copy-done.15, f32[8,512]{1,0:T(8,128)S(1)} %get-tuple-element.14.gate_ref, ...), custom_call_target="tpu_custom_call" | custom-call | flops 4000000000 | bytes 10000000 | tf_op jit(solution)/shard_map/attend/pallas_call | solution.py:487
  112.7 0.0 copy-done.1
  112.7 0.0 copy-done.4
  112.7 16.0 %project_out.1 = bf16[64,2048]{1,0:T(8,128)(2,1)S(1)} custom-call(bf16[512,256]{1,0:T(8,128)(2,1)S(1)} %get-tuple-element.15.gated, bf16[512,128]{1,0:T(8,128)(2,1)S(1)} %get-tuple-element.16.attended, bf16[256,2048]{1,0:T(8,128)(2,1)S(1)} %copy-done.1, bf16[128,2048]{1,0:T(8,128)(2,1)S(1)} %copy-done.4), custom_call_target="tpu_custom_call" | custom-call | flops 1000000000 | bytes 10000000 | tf_op jit(solution)/shard_map/project_out/pallas_call | solution.py:1033
  128.7 0.7 copy.26
  (14 shorter events, 0.1 us)
Async XLA Ops:
  0.0 0.7 copy-start.20
  0.7 0.7 copy-start.21
  1.5 2.1 %copy-start.12 = (bf16[2048,8]{0,1:T(8,128)(2,1)S(1)}, bf16[2048,8]{0,1:T(8,128)(2,1)}, u32[]{:S(2)}) copy-start(bf16[2048,8]{0,1:T(8,128)(2,1)} %param.27) | copy-start | bytes 98308
  1.6 2.0 %copy-start.5 = (bf16[2048,96]{0,1:T(8,128)(2,1)S(1)}, bf16[2048,96]{0,1:T(8,128)(2,1)}, u32[]{:S(2)}) copy-start(bf16[2048,96]{0,1:T(8,128)(2,1)} %param.30) | copy-start | bytes 1179652
  1.9 1.7 %copy-start.3 = (bf16[2048,128]{1,0:T(8,128)(2,1)S(1)}, bf16[2048,128]{1,0:T(8,128)(2,1)}, u32[]{:S(2)}) copy-start(bf16[2048,128]{1,0:T(8,128)(2,1)} %key_hbm.1) | copy-start | bytes 1572868
  1.9 1.7 %copy-start = (bf16[2048,256]{1,0:T(8,128)(2,1)S(1)}, bf16[2048,256]{1,0:T(8,128)(2,1)}, u32[]{:S(2)}) copy-start(bf16[2048,256]{1,0:T(8,128)(2,1)} %value_hbm.1) | copy-start | bytes 3145732
  2.1 1.5 %copy-start.2 = (bf16[2048,128]{1,0:T(8,128)(2,1)S(1)}, bf16[2048,128]{1,0:T(8,128)(2,1)}, u32[]{:S(2)}) copy-start(bf16[2048,128]{1,0:T(8,128)(2,1)} %query_hbm.1) | copy-start | bytes 1572868
  2.2 1.4 %copy-start.11 = (bf16[2048,8]{0,1:T(8,128)(2,1)S(1)}, bf16[2048,8]{0,1:T(8,128)(2,1)}, u32[]{:S(2)}) copy-start(bf16[2048,8]{0,1:T(8,128)(2,1)} %param.26) | copy-start | bytes 98308
  2.3 1.4 %copy-start.13 = (f32[512,1]{0,1:T(1,128)S(1)}, f32[512,1]{0,1:T(1,128)}, u32[]{:S(2)}) copy-start(f32[512,1]{0,1:T(1,128)} %param.28) | copy-start | bytes 6148
  3.7 1.0 copy-start.6
  4.6 0.9 copy-start.7
  5.6 0.9 copy-start.8
  6.5 0.9 copy-start.9
  7.4 0.9 copy-start.10
  38.4 0.9 copy-start.14
  39.3 0.8 copy-start.16
  40.1 0.7 copy-start.18
  41.5 1.1 copy-start.15
  42.7 1.0 copy-start.17
  43.6 0.9 copy-start.19
  44.6 68.1 %copy-start.1 = (bf16[256,2048]{1,0:T(8,128)(2,1)S(1)}, bf16[256,2048]{1,0:T(8,128)(2,1)}, u32[]{:S(2)}) copy-start(bf16[256,2048]{1,0:T(8,128)(2,1)} %out_memory.1) | copy-start | bytes 3145732
  44.6 68.1 %copy-start.4 = (bf16[128,2048]{1,0:T(8,128)(2,1)S(1)}, bf16[128,2048]{1,0:T(8,128)(2,1)}, u32[]{:S(2)}) copy-start(bf16[128,2048]{1,0:T(8,128)(2,1)} %out_attend.1) | copy-start | bytes 1572868

commit v4 on v3

--- a/solution.py
+++ b/solution.py
@@ -1,3 +1,5 @@
+import functools
+
 import jax
 import jax.numpy as jnp
 from jax import lax
@@ -30,9 +32,6 @@
 LATENT_WIDTH = 512
 QUERY_PART = QUERY_LATENT // (N_Y * N_C)
 LATENT_PART = LATENT_WIDTH // (N_Y * N_C)
-PARAMS = pltpu.CompilerParams
-
-
 LOG2E = 1.4426950408889634
 N_Z = 8
 N_X = 4
@@ -40,6 +39,8 @@
 MESH_ID = pl.DeviceIdType.MESH
 CONTRACT_LAST = (((1,), (1,)), ((), ()))
 CHUNK = M_QK // N_X
+TALL = 512
+GROUP = 1
 STATE_ROWS = CHUNK + 8
 NORMAL_ROW, TOP_ROW, DECAY_ROW = CHUNK, CHUNK + 1, CHUNK + 2
 
@@ -63,13 +64,13 @@
     return jnp.broadcast_to(row, (width, row.shape[1])).T
 
 
-def attend_kernel(
+def attend_phase(
     q_ref,
     kv_ref,
     mem_ref,
     gate_ref,
     gain_ref,
-    o_ref,
+    attended_ref,
     gated_ref,
     q_all,
     kv_all,
@@ -92,6 +93,7 @@
     start_in,
     square_out,
     square_in,
+    passed,
     q_send,
     q_recv,
     up_send,
@@ -110,6 +112,8 @@
     start_recv,
     square_send,
     square_recv,
+    passed_send,
+    passed_recv,
 ):
     f32, bf16 = jnp.float32, jnp.bfloat16
     z, x = lax.axis_index("z"), lax.axis_index("x")
@@ -118,16 +122,9 @@
     peers = [lax.rem(x + d, N_X) for d in range(1, N_X)]
     right, left = peers[0], peers[-1]
     rows_y = [lax.rem(y + d, N_Y) for d in range(1, N_Y)]
+    me_tp = y * N_C + c
     half = kv_ref.shape[0] // 2
     width = PLAIN_CHANNELS
-
-    barrier = pltpu.get_barrier_semaphore()
-    devices = [{"z": lax.rem(z + d, N_Z)} for d in range(1, N_Z)]
-    devices += [{"x": other} for other in peers] + [{"y": other} for other in rows_y]
-    devices.append({"c": 1 - c})
-    for device in devices:
-        pl.semaphore_signal(barrier, inc=1, device_id=device, device_id_type=MESH_ID)
-    pl.semaphore_wait(barrier, len(devices))
 
     def remote(source, target, send, recv, device):
         return pltpu.make_async_remote_copy(
@@ -180,6 +177,16 @@
             part_out.at[d], part_in.at[d], part_send.at[d], part_recv.at[d], {"x": peers[d]}
         )
 
+    def far_copy(h, hop):
+        rows = pl.ds(h * q_half, q_half)
+        return remote(
+            part_out.at[1, rows] if hop == 0 else passed.at[h],
+            passed.at[h] if hop == 0 else part_in.at[1, rows],
+            passed_send.at[hop, h],
+            passed_recv.at[hop, h],
+            {"x": right if h == 0 else left},
+        )
+
     def stat_copy(d):
         return remote(
             stat_out.at[d], stat_in.at[d], stat_send.at[d], stat_recv.at[d], {"x": peers[d]}
@@ -240,13 +247,12 @@
     for h in range(2):
         for up in (True, False):
             start(kv_copy(up, 1, h))
+    top[...] = jnp.full(top.shape, FAR_BELOW, f32)
+    total[...] = jnp.zeros(total.shape, f32)
     for number in (0, 3, 1, 2):
         start(q_copy(number))
-
+    accum[...] = jnp.zeros(accum.shape, f32)
     q_all[x] = q_ref[...]
-    top[...] = jnp.full(top.shape, FAR_BELOW, f32)
-    total[...] = jnp.zeros(total.shape, f32)
-    accum[...] = jnp.zeros(accum.shape, f32)
 
     relative, cumulative = gate_ref[0:1], gate_ref[1:2]
     key_scale = M_QK ** (-0.5)
@@ -305,32 +311,39 @@
         k_cat[: ROWS // 2, width:] = packed * low
         k_cat[ROWS // 2 :, width:] = packed * high
 
+    def attend_tile(t, keys, values, masked):
+        shard = t // (ROWS // TALL)
+        rows = pl.ds(pl.multiple_of(t * TALL, TALL), TALL)
+        inner = pl.ds(pl.multiple_of((t % (ROWS // TALL)) * TALL, TALL), TALL)
+        scores = lax.dot_general(
+            q_all[shard, inner], keys, CONTRACT_LAST, preferred_element_type=f32
+        )
+        scores = scores * scale
+        if masked:
+            row = lax.broadcasted_iota(jnp.int32, scores.shape, 0) + t * TALL
+            col = lax.broadcasted_iota(jnp.int32, scores.shape, 1) + x * ROWS
+            scores = jnp.where(col <= row, scores, -jnp.inf)
+        old = top[rows]
+        new = jnp.maximum(old, jnp.max(scores, axis=1, keepdims=True))
+        probs = jnp.exp2(scores - jnp.concatenate([new] * (ROWS // width), axis=1))
+        shrink = jnp.exp2(old - new)
+        added = sum(probs[:, k : k + width] for k in range(0, ROWS, width))
+        total[rows] = total[rows] * shrink + added
+        accum[rows] = accum[rows] * shrink + jnp.dot(
+            probs.astype(bf16), values, preferred_element_type=f32
+        )
+        top[rows] = new
+
     def attend_rows(first, last, values, masked):
-        def one(t, carry):
-            shard = t // (ROWS // tall)
-            rows = pl.ds(pl.multiple_of(t * tall, tall), tall)
-            inner = pl.ds(pl.multiple_of((t % (ROWS // tall)) * tall, tall), tall)
-            queries = q_all[shard, inner]
-            scores = lax.dot_general(
-                queries, k_cat[...], CONTRACT_LAST, preferred_element_type=f32
-            )
-            scores = scores * scale
-            if masked:
-                row = lax.broadcasted_iota(jnp.int32, scores.shape, 0) + t * tall
-                col = lax.broadcasted_iota(jnp.int32, scores.shape, 1) + x * ROWS
-                scores = jnp.where(col <= row, scores, -jnp.inf)
-            old = top[rows]
-            new = jnp.maximum(old, jnp.max(scores, axis=1, keepdims=True))
-            probs = jnp.exp2(scores - new[:, :1])
-            shrink = jnp.exp2(old - new)
-            total[rows] = total[rows] * shrink + jnp.sum(probs, axis=1, keepdims=True)
-            accum[rows] = accum[rows] * shrink + jnp.dot(
-                probs.astype(bf16), values(), preferred_element_type=f32
-            )
-            top[rows] = new
+        def one(g, carry):
+            for u in range(GROUP):
+                attend_tile(g * GROUP + u, k_cat[...], values(), masked)
             return carry
 
         lax.fori_loop(first, last, one, 0)
+
+    last = N_Z // 2
+    steps = ROWS // (TALL * GROUP)
 
     def arrived(owner, useful):
         @pl.when(useful)
@@ -338,27 +351,28 @@
             keys_from(kv_all.at[owner])
             attend_rows(0, N_X * steps, lambda: kv_all[owner, ROWS : 2 * ROWS], False)
 
-    last = N_Z // 2
-
-    def take(step):
-        for h in range(2):
-            for up in (True, False):
-                if step == last and up != (h == 0):
-                    continue
-                kv_copy(up, step, h).wait_recv()
-                if step < last - 1 or (step == last - 1 and up == (h == 0)):
-                    start(kv_copy(up, step + 1, h))
-
-    def use(step):
+    def take(step, h):
+        for up in (True, False):
+            if step == last and up != (h == 0):
+                continue
+            kv_copy(up, step, h).wait_recv()
+            if step < last - 1 or (step == last - 1 and up == (h == 0)):
+                start(kv_copy(up, step + 1, h))
+
+    def use_up(step):
         arrived(lax.rem(z + N_Z - step, N_Z), z >= step)
-        if step < last:
-            arrived(lax.rem(z + step, N_Z), z + step >= N_Z)
-
-    steps = ROWS // tall
+
+    def use_down(step):
+        arrived(lax.rem(z + step, N_Z), z + step >= N_Z)
+
     keys_from(kv_ref)
     own_values = lambda: kv_ref[ROWS : 2 * ROWS]
     attend_rows(x * steps, (x + 1) * steps, own_values, True)
 
+    q_copy(0).wait_recv()
+    start(q_copy(4))
+    q_copy(3).wait_recv()
+    start(q_copy(5))
     for d in range(N_X - 1):
         first_copy(d).wait_recv()
     column = first_in[0]
@@ -371,14 +385,15 @@
         def _(target=target):
             column_copy(target).start()
 
-    q_copy(0).wait_recv()
-    start(q_copy(4))
-    q_copy(3).wait_recv()
-    start(q_copy(5))
-    take(1)
+    take(1, 0)
     for number in (1, 2, 4, 5):
         q_copy(number).wait_recv()
     attend_rows((x + 1) * steps, N_X * steps, own_values, False)
+    take(1, 1)
+    take(2, 0)
+    use_up(1)
+    take(2, 1)
+    use_down(1)
 
     def gather_column(k, state):
         column_arrival(k).wait_recv()
@@ -392,8 +407,10 @@
     for d in range(N_X - 1):
         start(start_copy(d))
     start_in[x] = start_out[x]
-    use(1)
-    take(2)
+    take(3, 0)
+    use_up(2)
+    take(3, 1)
+    use_down(2)
 
     for d in range(N_X - 1):
         start_copy(d).wait_recv()
@@ -418,20 +435,35 @@
     square_out[0] = jnp.broadcast_to(squares, (ROWS, width)).T[:8]
     start(square_copy(0))
 
-    use(2)
-    take(3)
+    use_up(3)
     square_copy(0).wait_recv()
     square_out[1] = square_out[0] + square_in[0]
     for number in range(1, N_Y):
         start(square_copy(number))
-    use(3)
-    take(4)
-    use(4)
+    use_down(3)
+    take(4, 0)
+    take(4, 1)
+
+    opposite = lax.rem(z + last, N_Z)
+
+    @pl.when(z >= last)
+    def _():
+        keys_from(kv_all.at[opposite])
 
     def finish(shard):
+        @pl.when(z >= last)
+        def _():
+            attend_rows(
+                shard * steps,
+                (shard + 1) * steps,
+                lambda: kv_all[opposite, ROWS : 2 * ROWS],
+                False,
+            )
+
         rows = pl.ds(pl.multiple_of(shard * ROWS, ROWS), ROWS)
-        summed = jnp.maximum(total[rows], 1.0)
-        seen = total[rows] > 0.0
+        summed = jnp.sum(total[rows], axis=1, keepdims=True)
+        seen = summed > 0.0
+        summed = jnp.maximum(summed, 1.0)
         log_total = jnp.where(seen, top[rows] + jnp.log2(summed), FAR_BELOW)
         return accum[rows] / summed, log_total
 
@@ -439,19 +471,26 @@
         part, log_total = finish(peers[d])
         part_out[d] = part.astype(bf16)
         stat_out[d] = log_total.T[:8]
-        start(part_copy(d))
+        if d == 1:
+            start(far_copy(0, 0))
+            start(far_copy(1, 0))
+        else:
+            start(part_copy(d))
         start(stat_copy(d))
+    own, own_log = finish(x)
 
     squares = square_out[1]
     for number in range(1, N_Y):
         square_copy(number).wait_recv()
         squares = squares + square_in[number]
     inverse = lax.rsqrt(squares[:1] / (MEMORY_HEADS * M_V) + SMALL_CONSTANT)
-    gated = cell[...] * twice(as_columns(inverse, width)) * gain_ref[...].astype(f32)
+    gated = cell[...] * twice(as_columns(inverse, width)) * gain_ref[pl.ds(pl.multiple_of(me_tp * M_V, M_V), M_V)].astype(f32).reshape(1, M_V)
     gated = gated * jax.nn.sigmoid(mem_ref[:, 2 * M_QK + M_V :].astype(f32))
     gated_ref[...] = gated.astype(bf16)
-
-    own, own_log = finish(x)
+    for h in range(2):
+        far_copy(h, 0).wait_recv()
+        start(far_copy(h, 1))
+
     logs = []
     for d in range(N_X - 1):
         stat_copy(d).wait_recv()
@@ -462,85 +501,24 @@
     weight = jnp.exp2(own_log - highest)
     numerator = own * weight
     denominator = weight
-    for d in range(N_X - 1):
-        part_copy(d).wait_recv()
+    for d in (0, 2, 1):
+        if d == 1:
+            far_copy(0, 1).wait_recv()
+            far_copy(1, 1).wait_recv()
+        else:
+            part_copy(d).wait_recv()
         weight = jnp.exp2(logs[d] - highest)
         numerator = numerator + part_in[d].astype(f32) * weight
         denominator = denominator + weight
-    o_ref[...] = (numerator / denominator).astype(bf16)
-    for copy in started:
-        copy.wait_send()
-    for target in range(1, N_Z):
-
-        @pl.when(target > z)
-        def _(target=target):
-            column_copy(target).wait_send()
-
-
-def attend(queries, keys_values, memory_inputs, gates, gain):
-    f32, bf16 = jnp.float32, jnp.bfloat16
-    last = N_Z // 2
-    dma = pltpu.SemaphoreType.DMA
-    vmem = pl.BlockSpec(memory_space=pltpu.VMEM)
-    state = (STATE_ROWS, M_V)
-    peers = (N_X - 1,)
-    return pl.pallas_call(
-        attend_kernel,
-        out_shape=(
-            jax.ShapeDtypeStruct((ROWS, VALUE_CHANNELS), bf16),
-            jax.ShapeDtypeStruct((ROWS, M_V), bf16),
-        ),
-        in_specs=[vmem] * 5,
-        out_specs=[vmem] * 2,
-        scratch_shapes=[
-            pltpu.VMEM((N_X, ROWS, 256), bf16),
-            pltpu.VMEM((N_Z, *keys_values.shape), bf16),
-            pltpu.VMEM((ROWS, 256), bf16),
-            pltpu.VMEM((N_X * ROWS, 128), f32),
-            pltpu.VMEM((N_X * ROWS, 128), f32),
-            pltpu.VMEM((N_X * ROWS, VALUE_CHANNELS), f32),
-            pltpu.VMEM((N_X - 1, ROWS, VALUE_CHANNELS), bf16),
-            pltpu.VMEM((N_X - 1, 8, ROWS), f32),
-            pltpu.VMEM((N_X - 1, ROWS, VALUE_CHANNELS), bf16),
-            pltpu.VMEM((N_X - 1, 8, ROWS), f32),
-            pltpu.VMEM((ROWS, M_V), f32),
-            pltpu.VMEM((ROWS, 128), f32),
-            pltpu.VMEM((ROWS, 128), f32),
-            pltpu.VMEM((N_X, *state), f32),
-            pltpu.VMEM((N_X, *state), f32),
-            pltpu.VMEM(state, f32),
-            pltpu.VMEM((N_Z, *state), f32),
-            pltpu.VMEM((N_X, *state), f32),
-            pltpu.VMEM((N_X, *state), f32),
-            pltpu.VMEM((2, 8, ROWS), f32),
-            pltpu.VMEM((N_Y, 8, ROWS), f32),
-            dma((6,)),
-            dma((6,)),
-            dma((last, 2)),
-            dma((last, 2)),
-            dma((last, 2)),
-            dma((last, 2)),
-            dma(peers),
-            dma(peers),
-            dma(peers),
-            dma(peers),
-            dma(peers),
-            dma(peers),
-            dma((N_Z,)),
-            dma((N_Z,)),
-            dma(peers),
-            dma(peers),
-            dma((N_Y,)),
-            dma((N_Y,)),
-        ],
-        compiler_params=pltpu.CompilerParams(
-            collective_id=1, has_side_effects=True, vmem_limit_bytes=48 * 1024 * 1024
-        ),
-        cost_estimate=pl.CostEstimate(
-            flops=4 * 10**9, bytes_accessed=10**7, transcendentals=4 * 10**6
-        ),
-        name="attend",
-    )(queries, keys_values, memory_inputs, gates, gain)
+    attended_ref[...] = (numerator / denominator).astype(bf16)
+    def finish_columns():
+        for target in range(1, N_Z):
+
+            @pl.when(target > z)
+            def _(target=target):
+                column_copy(target).wait_send()
+
+    return started, finish_columns
 
 
 class TpGather:
@@ -608,23 +586,15 @@
             copy.wait_send()
 
 
-def greet_tp(barrier):
-    y, c = lax.axis_index("y"), lax.axis_index("c")
-    for device in (
-        {"c": 1 - c},
-        {"y": lax.rem(y + 1, N_Y)},
-        {"y": lax.rem(y + N_Y - 1, N_Y)},
-    ):
-        pl.semaphore_signal(barrier, inc=1, device_id=device, device_id_type=MESH_ID)
-
-
-def project_kernel(
-    tokens,
+def project_phase(
+    greeted,
+    tokens_hbm,
     gain,
-    gains,
+    query_gain,
+    latent_gain,
     cosine,
     sine_part,
-    shift_row,
+    shift_hbm,
     narrow_query,
     narrow_latent,
     narrow_rotary,
@@ -650,6 +620,8 @@
     query_up,
     key_up,
     value_up,
+    tokens,
+    shift_row,
     pre_gates,
     up_query,
     up_latent,
@@ -674,6 +646,7 @@
         (query_up_hbm, query_up),
         (key_up_hbm, key_up),
         (value_up_hbm, value_up),
+        (shift_hbm, shift_row),
     )
     loads = [
         pltpu.make_async_copy(source, target, load_sem.at[k])
@@ -683,28 +656,29 @@
     for k, ref in enumerate((query_hbm, key_hbm, value_hbm, outgate_hbm)):
         columns = ref.shape[1]
         loads.append(
-            pltpu.make_async_copy(ref, big.at[:, pl.ds(at, columns)], load_sem.at[8 + k])
+            pltpu.make_async_copy(ref, big.at[:, pl.ds(at, columns)], load_sem.at[9 + k])
         )
         at += columns
+    arrival = pltpu.make_async_copy(tokens_hbm, tokens, load_sem.at[13])
+    arrival.start()
     for load in loads:
         load.start()
-
+    arrival.wait()
     wide = tokens[...].astype(f32)
     inverse = lax.rsqrt(jnp.mean(wide * wide, axis=1, keepdims=True) + SMALL_CONSTANT)
-    rows_all[mine] = (wide * inverse * gain[...].astype(f32)).astype(bf16)
+    rows_all[mine] = (wide * inverse * gain[...].astype(f32).reshape(1, -1)).astype(bf16)
     small[QUERY_PART:width] = jnp.zeros((width - QUERY_PART, small.shape[1]), bf16)
 
-    barrier = pltpu.get_barrier_semaphore()
-    greet_tp(barrier)
-    pl.semaphore_wait(barrier, 3)
+    greeted()
     gather = TpGather(rows_all, row_send, row_recv)
     gather.start()
 
     for load in loads:
         load.wait()
     up_query[...] = jnp.zeros(up_query.shape, bf16)
+    query_rows = query_up[...].astype(f32).T.astype(bf16)
     for s in range(N_Y * N_C):
-        up_query[s * width : s * width + QUERY_PART] = query_up[
+        up_query[s * width : s * width + QUERY_PART] = query_rows[
             s * QUERY_PART : (s + 1) * QUERY_PART
         ]
         part = slice(s * LATENT_PART, (s + 1) * LATENT_PART)
@@ -834,72 +808,44 @@
         + SMALL_CONSTANT
     )
     latent_scale = jnp.where(low, low_scale, high_scale)
+    query_gains = jnp.broadcast_to(query_gain[...].reshape(1, -1), (8, QUERY_LATENT))
+    latent_gains = jnp.broadcast_to(latent_gain[...].reshape(1, -1), (8, LATENT_WIDTH))
+
+    def latent_gain_of(s):
+        pair = latent_gains[:1, (s // 2) * width : (s // 2 + 1) * width]
+        turned = pltpu.roll(latent_gains, LATENT_PART, 1)
+        other = turned[:1, (s // 2) * width : (s // 2 + 1) * width]
+        if s % 2:
+            other = pltpu.roll(latent_gains, LATENT_WIDTH - LATENT_PART, 1)
+            other = other[:1, (s // 2) * width : (s // 2 + 1) * width]
+            return jnp.where(low, other, pair)
+        return jnp.where(low, pair, other)
+
+    def query_gain_of(s):
+        turned = query_gains
+        if s:
+            turned = pltpu.roll(query_gains, QUERY_LATENT - s * QUERY_PART, 1)
+        return turned[:1, :width]
+
     for s in range(N_Y * N_C):
         columns = slice(s * width, (s + 1) * width)
         part = latents[s, :ROWS].astype(f32) * query_mask
-        wide_query[:, columns] = (part * query_scale * gains[s : s + 1]).astype(bf16)
+        wide_query[:, columns] = (part * query_scale * query_gain_of(s)).astype(bf16)
         part = latents[s, ROWS:].astype(f32)
-        made = (part * latent_scale * gains[8 + s : 9 + s]).astype(bf16)
+        made = (part * latent_scale * latent_gain_of(s)).astype(bf16)
         wide_latent[:half, columns] = jnp.where(low, made, jnp.zeros_like(made))
         wide_latent[half:, columns] = jnp.where(low, jnp.zeros_like(made), made)
+    made = jnp.dot(wide_latent[...], up_latent[...], preferred_element_type=f32).astype(bf16)
+    kv_ref[:ROWS] = made[:, :width]
+    kv_ref[ROWS : 2 * ROWS] = made[:, width:]
     made = jnp.dot(wide_query[...], up_query[...], preferred_element_type=f32).astype(bf16)
     q_ref[:, :width] = made[:, :width]
     turning = jnp.concatenate([made[:, width:], jnp.zeros((ROWS, ROTARY_CHANNELS), bf16)], axis=1)
     q_ref[:, width:] = rotated(turning, 0).astype(bf16)
-    made = jnp.dot(wide_latent[...], up_latent[...], preferred_element_type=f32).astype(bf16)
-    kv_ref[:ROWS] = made[:, :width]
-    kv_ref[ROWS : 2 * ROWS] = made[:, width:]
-    gather.finish()
-    exchange.finish()
-
-
-def project(dense, narrow, weights):
-    f32, bf16 = jnp.float32, jnp.bfloat16
-    depth = weights[0].shape[0]
-    dma = pltpu.SemaphoreType.DMA
-    vmem = pl.BlockSpec(memory_space=pltpu.VMEM)
-    hbm = pl.BlockSpec(memory_space=pl.ANY)
-    mem_width = sum(one.shape[1] for one in weights[:4])
-    return pl.pallas_call(
-        project_kernel,
-        out_shape=(
-            jax.ShapeDtypeStruct((ROWS, mem_width), bf16),
-            jax.ShapeDtypeStruct((8, ROWS), f32),
-            jax.ShapeDtypeStruct((ROWS, 256), bf16),
-            jax.ShapeDtypeStruct((ROWS * 5 // 2, 128), bf16),
-        ),
-        in_specs=[vmem] * len(dense) + [hbm] * (len(narrow) + len(weights)),
-        out_specs=[vmem] * 4,
-        scratch_shapes=[
-            pltpu.VMEM((N_Y * N_C, SHARE, depth), bf16),
-            pltpu.VMEM((N_Y * N_C, ROWS * 3 // 2, 128), bf16),
-            pltpu.VMEM((256, depth), bf16),
-            pltpu.VMEM((8, depth), bf16),
-            pltpu.VMEM((8, depth), bf16),
-            pltpu.VMEM((depth, mem_width), bf16),
-            *(pltpu.VMEM(one.shape, bf16) for one in weights[4:]),
-            pltpu.VMEM((2, 8, ROWS), f32),
-            pltpu.VMEM((1024, PLAIN_CHANNELS + ROTARY_CHANNELS), bf16),
-            pltpu.VMEM((1024, 256), bf16),
-            pltpu.VMEM((ROWS, 1024), bf16),
-            pltpu.VMEM((ROWS, 1024), bf16),
-            dma((12,)),
-            dma((11,)),
-            dma((11,)),
-            dma((11,)),
-            dma((11,)),
-        ],
-        compiler_params=PARAMS(
-            collective_id=2, has_side_effects=True, vmem_limit_bytes=48 * 1024 * 1024
-        ),
-        cost_estimate=pl.CostEstimate(
-            flops=3 * 10**9, bytes_accessed=10**7, transcendentals=10**4
-        ),
-        name="project",
-    )(*dense, *narrow, *weights)
-
-
-def output_kernel(
+    return gather.started + exchange.started
+
+
+def output_phase(
     gated,
     attended,
     out_memory,
@@ -928,9 +874,6 @@
     half = out_memory.shape[1] // 2
     tile = 512
 
-    barrier = pltpu.get_barrier_semaphore()
-    greet_tp(barrier)
-
     def remote(source, target, send, recv, device):
         return pltpu.make_async_remote_copy(
             src_ref=source,
@@ -989,8 +932,6 @@
             to_core[h, :, :, at : at + tile] = block
 
         partial(1 - c, h, keep)
-        if h == 0:
-            pl.semaphore_wait(barrier, 3)
         start(core_copy(h))
     for h in range(2):
 
@@ -1020,37 +961,303 @@
         down_copy(h).wait_recv()
         made = sums[h, y] + from_below[h].astype(f32) + from_above[h].astype(f32)
         o_ref[:, h * half : (h + 1) * half] = made.astype(bf16)
+    return started
+
+
+INPUTS = (
+    "tokens_hbm",
+    "shift_hbm",
+    "narrow_query",
+    "narrow_latent",
+    "narrow_rotary",
+    "narrow_ingate",
+    "narrow_forget",
+    "query_hbm",
+    "key_hbm",
+    "value_hbm",
+    "outgate_hbm",
+    "query_up_hbm",
+    "key_up_hbm",
+    "value_up_hbm",
+    "out_memory_hbm",
+    "out_attend_hbm",
+    "input_gain",
+    "query_gain",
+    "latent_gain",
+    "mem_gain",
+    "cosine",
+    "sine_part",
+)
+
+HBM_INPUTS = 16
+
+
+def scratch(depth, mem_width):
+    f32, bf16 = jnp.float32, jnp.bfloat16
+    dma = pltpu.SemaphoreType.DMA
+    return dict(
+        rows_all=pltpu.VMEM((N_Y * N_C, SHARE, depth), bf16),
+        latents=pltpu.VMEM((N_Y * N_C, ROWS * 3 // 2, 128), bf16),
+        small=pltpu.VMEM((256, depth), bf16),
+        ingate=pltpu.VMEM((8, depth), bf16),
+        forget=pltpu.VMEM((8, depth), bf16),
+        big=pltpu.VMEM((depth, mem_width), bf16),
+        query_up=pltpu.VMEM((PLAIN_CHANNELS + ROTARY_CHANNELS, QUERY_LATENT), bf16),
+        key_up=pltpu.VMEM((LATENT_WIDTH, PLAIN_CHANNELS), bf16),
+        value_up=pltpu.VMEM((LATENT_WIDTH, VALUE_CHANNELS), bf16),
+        tokens=pltpu.VMEM((SHARE, depth), bf16),
+        shift_row=pltpu.VMEM((1, ROWS), f32),
+        pre_gates=pltpu.VMEM((2, 8, ROWS), f32),
+        up_query=pltpu.VMEM((1024, PLAIN_CHANNELS + ROTARY_CHANNELS), bf16),
+        up_latent=pltpu.VMEM((1024, 256), bf16),
+        wide_query=pltpu.VMEM((ROWS, 1024), bf16),
+        wide_latent=pltpu.VMEM((ROWS, 1024), bf16),
+        load_sem=dma((16,)),
+        row_send=dma((11,)),
+        row_recv=dma((11,)),
+        lat_send=dma((11,)),
+        lat_recv=dma((11,)),
+        mem_ref=pltpu.VMEM((ROWS, mem_width), bf16),
+        gate_ref=pltpu.VMEM((8, ROWS), f32),
+        q_ref=pltpu.VMEM((ROWS, 256), bf16),
+        kv_ref=pltpu.VMEM((ROWS * 5 // 2, 128), bf16),
+        attended_ref=pltpu.VMEM((ROWS, VALUE_CHANNELS), bf16),
+        gated_ref=pltpu.VMEM((ROWS, M_V), bf16),
+        q_all=pltpu.VMEM((N_X, ROWS, 256), bf16),
+        kv_all=pltpu.VMEM((N_Z, ROWS * 5 // 2, 128), bf16),
+        k_cat=pltpu.VMEM((ROWS, 256), bf16),
+        top=pltpu.VMEM((N_X * ROWS, 128), f32),
+        total=pltpu.VMEM((N_X * ROWS, 128), f32),
+        accum=pltpu.VMEM((N_X * ROWS, VALUE_CHANNELS), f32),
+        part_out=pltpu.VMEM((N_X - 1, ROWS, VALUE_CHANNELS), bf16),
+        stat_out=pltpu.VMEM((N_X - 1, 8, ROWS), f32),
+        part_in=pltpu.VMEM((N_X - 1, ROWS, VALUE_CHANNELS), bf16),
+        stat_in=pltpu.VMEM((N_X - 1, 8, ROWS), f32),
+        cell=pltpu.VMEM((ROWS, M_V), f32),
+        cell_sum=pltpu.VMEM((ROWS, 128), f32),
+        cell_top=pltpu.VMEM((ROWS, 128), f32),
+        first_out=pltpu.VMEM((N_X, STATE_ROWS, M_V), f32),
+        first_in=pltpu.VMEM((N_X, STATE_ROWS, M_V), f32),
+        column_out=pltpu.VMEM((STATE_ROWS, M_V), f32),
+        column_in=pltpu.VMEM((N_Z, STATE_ROWS, M_V), f32),
+        start_out=pltpu.VMEM((N_X, STATE_ROWS, M_V), f32),
+        start_in=pltpu.VMEM((N_X, STATE_ROWS, M_V), f32),
+        square_out=pltpu.VMEM((2, 8, ROWS), f32),
+        square_in=pltpu.VMEM((N_Y, 8, ROWS), f32),
+        passed=pltpu.VMEM((2, ROWS // 2, VALUE_CHANNELS), bf16),
+        q_send=dma((6,)),
+        q_recv=dma((6,)),
+        up_send=dma((N_Z // 2, 2)),
+        up_recv=dma((N_Z // 2, 2)),
+        down_send=dma((N_Z // 2, 2)),
+        down_recv=dma((N_Z // 2, 2)),
+        part_send=dma((N_X - 1,)),
+        part_recv=dma((N_X - 1,)),
+        stat_send=dma((N_X - 1,)),
+        stat_recv=dma((N_X - 1,)),
+        first_send=dma((N_X - 1,)),
+        first_recv=dma((N_X - 1,)),
+        column_send=dma((N_Z,)),
+        column_recv=dma((N_Z,)),
+        start_send=dma((N_X - 1,)),
+        start_recv=dma((N_X - 1,)),
+        square_send=dma((N_Y,)),
+        square_recv=dma((N_Y,)),
+        passed_send=dma((2, 2)),
+        passed_recv=dma((2, 2)),
+        out_memory=pltpu.VMEM((M_V, depth), bf16),
+        out_attend=pltpu.VMEM((VALUE_CHANNELS, depth), bf16),
+        to_core=pltpu.VMEM((2, N_Y, SHARE, depth // 2), bf16),
+        from_core=pltpu.VMEM((2, N_Y, SHARE, depth // 2), bf16),
+        sums=pltpu.VMEM((2, N_Y, SHARE, depth // 2), f32),
+        passing=pltpu.VMEM((6, SHARE, depth // 2), bf16),
+        from_below=pltpu.VMEM((2, SHARE, depth // 2), bf16),
+        from_above=pltpu.VMEM((2, SHARE, depth // 2), bf16),
+        relay_in=pltpu.VMEM((2, SHARE, depth // 2), bf16),
+        core_send=dma((2,)),
+        core_recv=dma((2,)),
+        relay_send=dma((2,)),
+        relay_recv=dma((2,)),
+        out_up_send=dma((2,)),
+        out_up_recv=dma((2,)),
+        out_down_send=dma((2,)),
+        out_down_recv=dma((2,)),
+    )
+
+
+def layer_kernel(names, *refs):
+    at = dict(zip(names, refs))
+    y, c = lax.axis_index("y"), lax.axis_index("c")
+    z, x = lax.axis_index("z"), lax.axis_index("x")
+    barrier = pltpu.get_barrier_semaphore()
+    devices = [{"c": 1 - c}]
+    devices += [{"y": lax.rem(y + d, N_Y)} for d in range(1, N_Y)]
+    devices += [{"x": lax.rem(x + d, N_X)} for d in range(1, N_X)]
+    devices += [{"z": lax.rem(z + d, N_Z)} for d in range(1, N_Z)]
+    for device in devices:
+        pl.semaphore_signal(barrier, inc=1, device_id=device, device_id_type=MESH_ID)
+    loads = [
+        pltpu.make_async_copy(at[name + "_hbm"], at[name], at["load_sem"].at[14 + k])
+        for k, name in enumerate(("out_memory", "out_attend"))
+    ]
+    started = project_phase(
+        lambda: pl.semaphore_wait(barrier, len(devices)),
+        *(at[name] for name in PROJECT_REFS),
+    )
+    for load in loads:
+        load.start()
+    more, finish_columns = attend_phase(*(at[name] for name in ATTEND_REFS))
+    started += more
+    for load in loads:
+        load.wait()
+    started += output_phase(*(at[name] for name in OUTPUT_REFS))
     for copy in started:
         copy.wait_send()
-
-
-def project_out(gated, attended, out_memory, out_attend):
-    f32, bf16 = jnp.float32, jnp.bfloat16
-    dma = pltpu.SemaphoreType.DMA
+    finish_columns()
+
+
+PROJECT_REFS = (
+    "tokens_hbm",
+    "input_gain",
+    "query_gain",
+    "latent_gain",
+    "cosine",
+    "sine_part",
+    "shift_hbm",
+    "narrow_query",
+    "narrow_latent",
+    "narrow_rotary",
+    "narrow_ingate",
+    "narrow_forget",
+    "query_hbm",
+    "key_hbm",
+    "value_hbm",
+    "outgate_hbm",
+    "query_up_hbm",
+    "key_up_hbm",
+    "value_up_hbm",
+    "mem_ref",
+    "gate_ref",
+    "q_ref",
+    "kv_ref",
+    "rows_all",
+    "latents",
+    "small",
+    "ingate",
+    "forget",
+    "big",
+    "query_up",
+    "key_up",
+    "value_up",
+    "tokens",
+    "shift_row",
+    "pre_gates",
+    "up_query",
+    "up_latent",
+    "wide_query",
+    "wide_latent",
+    "load_sem",
+    "row_send",
+    "row_recv",
+    "lat_send",
+    "lat_recv",
+)
+ATTEND_REFS = (
+    "q_ref",
+    "kv_ref",
+    "mem_ref",
+    "gate_ref",
+    "mem_gain",
+    "attended_ref",
+    "gated_ref",
+    "q_all",
+    "kv_all",
+    "k_cat",
+    "top",
+    "total",
+    "accum",
+    "part_out",
+    "stat_out",
+    "part_in",
+    "stat_in",
+    "cell",
+    "cell_sum",
+    "cell_top",
+    "first_out",
+    "first_in",
+    "column_out",
+    "column_in",
+    "start_out",
+    "start_in",
+    "square_out",
+    "square_in",
+    "passed",
+    "q_send",
+    "q_recv",
+    "up_send",
+    "up_recv",
+    "down_send",
+    "down_recv",
+    "part_send",
+    "part_recv",
+    "stat_send",
+    "stat_recv",
+    "first_send",
+    "first_recv",
+    "column_send",
+    "column_recv",
+    "start_send",
+    "start_recv",
+    "square_send",
+    "square_recv",
+    "passed_send",
+    "passed_recv",
+)
+OUTPUT_REFS = (
+    "gated_ref",
+    "attended_ref",
+    "out_memory",
+    "out_attend",
+    "o_ref",
+    "to_core",
+    "from_core",
+    "sums",
+    "passing",
+    "from_below",
+    "from_above",
+    "relay_in",
+    "core_send",
+    "core_recv",
+    "relay_send",
+    "relay_recv",
+    "out_up_send",
+    "out_up_recv",
+    "out_down_send",
+    "out_down_recv",
+)
+
+
+def layer(*inputs):
+    depth = inputs[0].shape[1]
+    mem_width = sum(one.shape[1] for one in inputs[7:11])
+    made = scratch(depth, mem_width)
+    names = (*INPUTS, "o_ref", *made)
     vmem = pl.BlockSpec(memory_space=pltpu.VMEM)
-    half = out_memory.shape[1] // 2
-    block = (2, SHARE, half)
+    hbm = pl.BlockSpec(memory_space=pltpu.HBM)
     return pl.pallas_call(
-        output_kernel,
-        out_shape=jax.ShapeDtypeStruct((SHARE, 2 * half), bf16),
-        in_specs=[vmem] * 4,
+        functools.partial(layer_kernel, names),
+        out_shape=jax.ShapeDtypeStruct((SHARE, depth), jnp.bfloat16),
+        in_specs=[hbm] * HBM_INPUTS + [vmem] * (len(inputs) - HBM_INPUTS),
         out_specs=vmem,
-        scratch_shapes=[
-            pltpu.VMEM((2, N_Y, SHARE, half), bf16),
-            pltpu.VMEM((2, N_Y, SHARE, half), bf16),
-            pltpu.VMEM((2, N_Y, SHARE, half), f32),
-            pltpu.VMEM((6, SHARE, half), bf16),
-            pltpu.VMEM(block, bf16),
-            pltpu.VMEM(block, bf16),
-            pltpu.VMEM(block, bf16),
-        ]
-        + [dma((2,))] * 8,
-        compiler_params=PARAMS(
-            collective_id=3, has_side_effects=True, vmem_limit_bytes=48 * 1024 * 1024
+        scratch_shapes=list(made.values()),
+        compiler_params=pltpu.CompilerParams(
+            collective_id=1, has_side_effects=True, vmem_limit_bytes=67_000_000
         ),
-        cost_estimate=pl.CostEstimate(flops=10**9, bytes_accessed=10**7, transcendentals=0),
-        name="project_out",
-    )(gated, attended, out_memory, out_attend)
+        cost_estimate=pl.CostEstimate(
+            flops=8 * 10**9, bytes_accessed=2 * 10**7, transcendentals=4 * 10**6
+        ),
+        name="layer",
+    )(*inputs)
 
 
 def per_device(
@@ -1076,41 +1283,35 @@
     out_attend,
 ):
     length = forget_shift.shape[0]
-    latent_rows = latent_gain.reshape(8, LATENT_PART)
-    gains = jnp.concatenate(
-        [
-            jnp.pad(query_gain.reshape(8, QUERY_PART), ((0, 0), (0, 128 - QUERY_PART))),
-            jnp.concatenate([latent_rows, latent_rows], axis=1),
-        ],
-        axis=0,
-    )
     positions = lax.axis_index(SP) * length + jnp.arange(length, dtype=jnp.int32)
     halfway = ROTARY_CHANNELS // 2
     inverse = jnp.power(ROTARY_BASE, -jnp.arange(halfway, dtype=jnp.float32) / halfway)
     angles = positions.astype(jnp.float32)[:, None] * inverse
     cosine, sine_part = (jnp.tile(made, (1, 4)) for made in (jnp.cos(angles), jnp.sin(angles)))
-    memory_inputs, gates, queries, keys_values = project(
-        (tokens, input_gain[None, :], gains, cosine, sine_part, forget_shift.T),
-        (
-            query_down_weight.T,
-            latent_down_weight.T,
-            down_rotary.T,
-            weight_ingate.T,
-            weight_forget.T,
-        ),
-        (
-            weight_query,
-            weight_key,
-            weight_value,
-            weight_outgate,
-            query_up_weight,
-            key_up_weight,
-            value_up_weight,
-        ),
-    )
-    gain_part = lax.dynamic_slice_in_dim(mem_gain, lax.axis_index(TP) * M_V, M_V, 0)
-    attended, gated = attend(queries, keys_values, memory_inputs, gates, gain_part[None, :])
-    return project_out(gated, attended, out_memory, out_attend)
+    return layer(
+        tokens,
+        forget_shift.T,
+        query_down_weight.T,
+        latent_down_weight.T,
+        down_rotary.T,
+        weight_ingate.T,
+        weight_forget.T,
+        weight_query,
+        weight_key,
+        weight_value,
+        weight_outgate,
+        query_up_weight.T,
+        key_up_weight,
+        value_up_weight,
+        out_memory,
+        out_attend,
+        input_gain,
+        query_gain,
+        latent_gain,
+        mem_gain,
+        cosine,
+        sine_part,
+    )
 
 
 def solution(mesh):

time: 130 us -> 104 us (0.80)
  Pallas kernels: 114 us -> 100 us
  local copies, waits for them, and re-layouts: 14.6 us -> 3.37 us
    pallas_call x3 -> x1, Pallas kernels: 114 us -> 100 us  [layer(): pl.pallas_call(functools.partial(layer_kernel, names), out_shape=jax.Shap...]
    unnamed x46 -> x1, local copies, waits for them, and re-layouts: 12.7 us -> 1.67 us
    another operation x4, local copies, waits for them, and re-layouts: 0.29 us -> 1.7 us  [per_device(): jnp.tile(made, (1, 4))]
where the time goes in v4:
time: 104 us
  Pallas kernels  100 us (96%)
  local copies, waits for them, and re-layouts  3.37 us (3%)
    pallas_call x1, Pallas kernels, layer(): pl.pallas_call(functools.partial(layer_kernel, names), out_shape=jax.Shap...  100 us

profile of v4, /device:TPU:224, one launch (start us, length us, event | category | flops | bytes accessed | tf_op | source)
XLA Modules:
  0.0 103.9 jit_solution(179730583448035426)
XLA Ops:
  0.0 0.3 multiply_sine_fusion
  0.4 0.8 copy.22.refs_21_
  1.2 0.8 copy.21.refs_20_
  2.1 100.2 %layer.1 = bf16[64,2048]{1,0:T(8,128)(2,1)} custom-call(bf16[64,2048]{1,0:T(8,128)(2,1)} %refs_0_.1, f32[1,512]{1,0:T(1,128)} %bitcast.17, bf16[96,2048]{1,0:T(8,128)(2,1)} %bitcast.11, bf16[64,2048]{1,0:T(8,128)(2,1)} %bitcast.13, bf16[64,2048]{1,0:T(8,128)(2,1)} %bitcast.14, bf16[8,2048]{1,0:T(8,128)(2,1)} %bitcast.15, bf16[8,2048]{1,0:T(8,128)(2,1)} %bitcast.16, ...), custom_call_target="tpu_custom_call" | custom-call | flops 8000000000 | bytes 20000000 | tf_op jit(solution)/shard_map/layer/pallas_call | solution.py:1247
  102.3 1.7 %copy.24 = bf16[64,2048]{1,0:T(8,128)(2,1)} copy(bf16[64,2048]{1,0:T(8,128)(2,1)} %layer.1) | data formatting | bytes 524288
  (4 shorter events, 0.1 us)

commit v5 on v4

--- a/solution.py
+++ b/solution.py
@@ -244,16 +244,6 @@
         copy.start()
         started.append(copy)
 
-    for h in range(2):
-        for up in (True, False):
-            start(kv_copy(up, 1, h))
-    top[...] = jnp.full(top.shape, FAR_BELOW, f32)
-    total[...] = jnp.zeros(total.shape, f32)
-    for number in (0, 3, 1, 2):
-        start(q_copy(number))
-    accum[...] = jnp.zeros(accum.shape, f32)
-    q_all[x] = q_ref[...]
-
     relative, cumulative = gate_ref[0:1], gate_ref[1:2]
     key_scale = M_QK ** (-0.5)
     tall = 256
@@ -300,6 +290,32 @@
         start(first_copy(d))
     first_in[x] = first_out[x]
 
+    yield
+
+    for d in range(N_X - 1):
+        first_copy(d).wait_recv()
+    column = first_in[0]
+    for k in range(1, N_X):
+        column = merge_states(column, first_in[k])
+    column_out[...] = column
+    for target in range(1, N_Z):
+
+        @pl.when(target > z)
+        def _(target=target):
+            column_copy(target).start()
+
+    yield
+
+    for h in range(2):
+        for up in (True, False):
+            start(kv_copy(up, 1, h))
+    top[...] = jnp.full(top.shape, FAR_BELOW, f32)
+    total[...] = jnp.zeros(total.shape, f32)
+    for number in (0, 3, 1, 2):
+        start(q_copy(number))
+    accum[...] = jnp.zeros(accum.shape, f32)
+    q_all[x] = q_ref[...]
+
     lane = lax.broadcasted_iota(jnp.int32, (ROWS // 2, width), 1)
     low = (lane < ROTARY_CHANNELS).astype(bf16)
     high = (lane >= ROTARY_CHANNELS).astype(bf16)
@@ -373,18 +389,19 @@
     start(q_copy(4))
     q_copy(3).wait_recv()
     start(q_copy(5))
+
+    def gather_column(k, state):
+        column_arrival(k).wait_recv()
+        return merge_states(state, column_in[k])
+
+    state = lax.fori_loop(0, z, gather_column, jnp.zeros((STATE_ROWS, M_V), f32))
+    for k in range(N_X):
+        start_out[k] = state
+        if k < N_X - 1:
+            state = merge_states(state, first_in[k])
     for d in range(N_X - 1):
-        first_copy(d).wait_recv()
-    column = first_in[0]
-    for k in range(1, N_X):
-        column = merge_states(column, first_in[k])
-    column_out[...] = column
-    for target in range(1, N_Z):
-
-        @pl.when(target > z)
-        def _(target=target):
-            column_copy(target).start()
-
+        start(start_copy(d))
+    start_in[x] = start_out[x]
     take(1, 0)
     for number in (1, 2, 4, 5):
         q_copy(number).wait_recv()
@@ -395,23 +412,6 @@
     take(2, 1)
     use_down(1)
 
-    def gather_column(k, state):
-        column_arrival(k).wait_recv()
-        return merge_states(state, column_in[k])
-
-    state = lax.fori_loop(0, z, gather_column, jnp.zeros((STATE_ROWS, M_V), f32))
-    for k in range(N_X):
-        start_out[k] = state
-        if k < N_X - 1:
-            state = merge_states(state, first_in[k])
-    for d in range(N_X - 1):
-        start(start_copy(d))
-    start_in[x] = start_out[x]
-    take(3, 0)
-    use_up(2)
-    take(3, 1)
-    use_down(2)
-
     for d in range(N_X - 1):
         start_copy(d).wait_recv()
     carried = jnp.concatenate([start_in[k, :CHUNK] for k in range(N_X)], axis=0)
@@ -435,12 +435,25 @@
     square_out[0] = jnp.broadcast_to(squares, (ROWS, width)).T[:8]
     start(square_copy(0))
 
-    use_up(3)
+    take(3, 0)
+    use_up(2)
     square_copy(0).wait_recv()
     square_out[1] = square_out[0] + square_in[0]
     for number in range(1, N_Y):
         start(square_copy(number))
+    take(3, 1)
+    use_down(2)
+    use_up(3)
     use_down(3)
+
+    squares = square_out[1]
+    for number in range(1, N_Y):
+        square_copy(number).wait_recv()
+        squares = squares + square_in[number]
+    inverse = lax.rsqrt(squares[:1] / (MEMORY_HEADS * M_V) + SMALL_CONSTANT)
+    gated = cell[...] * twice(as_columns(inverse, width)) * gain_ref[pl.ds(pl.multiple_of(me_tp * M_V, M_V), M_V)].astype(f32).reshape(1, M_V)
+    gated = gated * jax.nn.sigmoid(mem_ref[:, 2 * M_QK + M_V :].astype(f32))
+    gated_ref[...] = gated.astype(bf16)
     take(4, 0)
     take(4, 1)
 
@@ -479,14 +492,6 @@
         start(stat_copy(d))
     own, own_log = finish(x)
 
-    squares = square_out[1]
-    for number in range(1, N_Y):
-        square_copy(number).wait_recv()
-        squares = squares + square_in[number]
-    inverse = lax.rsqrt(squares[:1] / (MEMORY_HEADS * M_V) + SMALL_CONSTANT)
-    gated = cell[...] * twice(as_columns(inverse, width)) * gain_ref[pl.ds(pl.multiple_of(me_tp * M_V, M_V), M_V)].astype(f32).reshape(1, M_V)
-    gated = gated * jax.nn.sigmoid(mem_ref[:, 2 * M_QK + M_V :].astype(f32))
-    gated_ref[...] = gated.astype(bf16)
     for h in range(2):
         far_copy(h, 0).wait_recv()
         start(far_copy(h, 1))
@@ -518,7 +523,7 @@
             def _(target=target):
                 column_copy(target).wait_send()
 
-    return started, finish_columns
+    yield started, finish_columns
 
 
 class TpGather:
@@ -588,12 +593,14 @@
 
 def project_phase(
     greeted,
+    after_gates,
+    after_exchange,
     tokens_hbm,
     gain,
     query_gain,
     latent_gain,
-    cosine,
-    sine_part,
+    cosine_row,
+    sine_row,
     shift_hbm,
     narrow_query,
     narrow_latent,
@@ -675,6 +682,8 @@
 
     for load in loads:
         load.wait()
+    small[QUERY_PART : QUERY_PART + 8] = ingate[...]
+    small[QUERY_PART + 16 : QUERY_PART + 24] = forget[...]
     up_query[...] = jnp.zeros(up_query.shape, bf16)
     query_rows = query_up[...].astype(f32).T.astype(bf16)
     for s in range(N_Y * N_C):
@@ -688,6 +697,9 @@
             up_latent[at : at + LATENT_PART, width:] = value_up[part]
 
     lane = lax.broadcasted_iota(jnp.int32, (1, width), 1)
+    cosine, sine_part = (
+        jnp.concatenate([ref[...]] * 4, axis=0).T for ref in (cosine_row, sine_row)
+    )
     row_id = lax.broadcasted_iota(jnp.int32, (width, width), 0)
     col_id = lax.broadcasted_iota(jnp.int32, (width, width), 1)
     channels = lax.rem(col_id, ROTARY_CHANNELS)
@@ -704,7 +716,7 @@
     def rotated(values, offset):
         swap = jnp.where(row_id == partner + offset, sign, 0.0).astype(bf16)
         turned = jnp.dot(values, swap, preferred_element_type=f32)
-        return duplicated(values, offset) * cosine[...] + turned * sine_part[...]
+        return duplicated(values, offset) * cosine + turned * sine_part
 
     def chip_rows(chip):
         slots = [rows_all[chip * N_C + k] for k in range(N_C)]
@@ -717,21 +729,20 @@
         rows = pl.ds(pl.multiple_of(chip * span, span), span)
         here = chip_rows(chip)
         made = lax.dot_general(here, small[...], CONTRACT_LAST, preferred_element_type=f32)
-        for k, ref in enumerate((ingate, forget)):
-            pre_gates[k, :, rows] = lax.dot_general(
-                ref[...], here, CONTRACT_LAST, preferred_element_type=f32
-            )
+        turned = made[:, :width].T
+        for k in range(2):
+            at = QUERY_PART + 16 * k
+            pre_gates[k, :, rows] = turned[at : at + 8]
         rounded = made.astype(bf16)
         latents[mine, rows] = rounded[:, :width]
         wide_latent[rows, :width] = rounded[:, width:]
 
-    def project_big(chip):
-        rows = pl.ds(pl.multiple_of(chip * span, span), span)
-
+    def project_big():
         def one(t, carry):
             columns = pl.ds(pl.multiple_of(t * tile, tile), tile)
-            made = jnp.dot(chip_rows(chip), big[:, columns], preferred_element_type=f32)
-            mem_ref[rows, columns] = made.astype(bf16)
+            rows = rows_all[...].reshape(ROWS, rows_all.shape[2])
+            made = jnp.dot(rows, big[:, columns], preferred_element_type=f32)
+            mem_ref[:, columns] = made.astype(bf16)
             return carry
 
         lax.fori_loop(0, big.shape[1] // tile, one, 0)
@@ -752,11 +763,7 @@
     latents[mine, ROWS:] = packed.astype(bf16)
     exchange = TpGather(latents, lat_send, lat_recv)
     exchange.start()
-    for chip in near[:2]:
-        project_big(chip)
-    exchange.relay()
-    for chip in (near[2], opposite):
-        project_big(chip)
+    project_big()
     heads = lax.broadcasted_iota(jnp.int32, (8, ROWS), 0) == mine
     in_pre, forget_pre = (
         jnp.sum(jnp.where(heads, pre_gates[k], 0.0), axis=0, keepdims=True) for k in range(2)
@@ -780,11 +787,14 @@
     )
     top_rows = lax.broadcasted_iota(jnp.int32, (8, ROWS), 0) == 0
     gate_ref[...] = jnp.where(top_rows, in_gate - cumulative, cumulative)
+    exchange.relay()
+    after_gates()
     key_turned = rotated(second, LATENT_PART)
     kv_ref[2 * ROWS :] = jnp.where(
         lane < ROTARY_CHANNELS, key_turned[:half], key_turned[half:]
     ).astype(bf16)
     exchange.near()
+    after_exchange()
     exchange.far()
 
     query_mask = (lane < QUERY_PART).astype(f32)
@@ -964,131 +974,124 @@
     return started
 
 
-INPUTS = (
-    "tokens_hbm",
-    "shift_hbm",
-    "narrow_query",
-    "narrow_latent",
-    "narrow_rotary",
-    "narrow_ingate",
-    "narrow_forget",
-    "query_hbm",
-    "key_hbm",
-    "value_hbm",
-    "outgate_hbm",
-    "query_up_hbm",
-    "key_up_hbm",
-    "value_up_hbm",
-    "out_memory_hbm",
-    "out_attend_hbm",
-    "input_gain",
-    "query_gain",
-    "latent_gain",
-    "mem_gain",
-    "cosine",
-    "sine_part",
-)
-
-HBM_INPUTS = 16
-
-
 def scratch(depth, mem_width):
     f32, bf16 = jnp.float32, jnp.bfloat16
     dma = pltpu.SemaphoreType.DMA
-    return dict(
-        rows_all=pltpu.VMEM((N_Y * N_C, SHARE, depth), bf16),
-        latents=pltpu.VMEM((N_Y * N_C, ROWS * 3 // 2, 128), bf16),
-        small=pltpu.VMEM((256, depth), bf16),
-        ingate=pltpu.VMEM((8, depth), bf16),
-        forget=pltpu.VMEM((8, depth), bf16),
-        big=pltpu.VMEM((depth, mem_width), bf16),
-        query_up=pltpu.VMEM((PLAIN_CHANNELS + ROTARY_CHANNELS, QUERY_LATENT), bf16),
-        key_up=pltpu.VMEM((LATENT_WIDTH, PLAIN_CHANNELS), bf16),
-        value_up=pltpu.VMEM((LATENT_WIDTH, VALUE_CHANNELS), bf16),
-        tokens=pltpu.VMEM((SHARE, depth), bf16),
-        shift_row=pltpu.VMEM((1, ROWS), f32),
-        pre_gates=pltpu.VMEM((2, 8, ROWS), f32),
-        up_query=pltpu.VMEM((1024, PLAIN_CHANNELS + ROTARY_CHANNELS), bf16),
-        up_latent=pltpu.VMEM((1024, 256), bf16),
-        wide_query=pltpu.VMEM((ROWS, 1024), bf16),
-        wide_latent=pltpu.VMEM((ROWS, 1024), bf16),
-        load_sem=dma((16,)),
-        row_send=dma((11,)),
-        row_recv=dma((11,)),
-        lat_send=dma((11,)),
-        lat_recv=dma((11,)),
-        mem_ref=pltpu.VMEM((ROWS, mem_width), bf16),
-        gate_ref=pltpu.VMEM((8, ROWS), f32),
-        q_ref=pltpu.VMEM((ROWS, 256), bf16),
-        kv_ref=pltpu.VMEM((ROWS * 5 // 2, 128), bf16),
-        attended_ref=pltpu.VMEM((ROWS, VALUE_CHANNELS), bf16),
-        gated_ref=pltpu.VMEM((ROWS, M_V), bf16),
-        q_all=pltpu.VMEM((N_X, ROWS, 256), bf16),
-        kv_all=pltpu.VMEM((N_Z, ROWS * 5 // 2, 128), bf16),
-        k_cat=pltpu.VMEM((ROWS, 256), bf16),
-        top=pltpu.VMEM((N_X * ROWS, 128), f32),
-        total=pltpu.VMEM((N_X * ROWS, 128), f32),
-        accum=pltpu.VMEM((N_X * ROWS, VALUE_CHANNELS), f32),
-        part_out=pltpu.VMEM((N_X - 1, ROWS, VALUE_CHANNELS), bf16),
-        stat_out=pltpu.VMEM((N_X - 1, 8, ROWS), f32),
-        part_in=pltpu.VMEM((N_X - 1, ROWS, VALUE_CHANNELS), bf16),
-        stat_in=pltpu.VMEM((N_X - 1, 8, ROWS), f32),
-        cell=pltpu.VMEM((ROWS, M_V), f32),
-        cell_sum=pltpu.VMEM((ROWS, 128), f32),
-        cell_top=pltpu.VMEM((ROWS, 128), f32),
-        first_out=pltpu.VMEM((N_X, STATE_ROWS, M_V), f32),
-        first_in=pltpu.VMEM((N_X, STATE_ROWS, M_V), f32),
-        column_out=pltpu.VMEM((STATE_ROWS, M_V), f32),
-        column_in=pltpu.VMEM((N_Z, STATE_ROWS, M_V), f32),
-        start_out=pltpu.VMEM((N_X, STATE_ROWS, M_V), f32),
-        start_in=pltpu.VMEM((N_X, STATE_ROWS, M_V), f32),
-        square_out=pltpu.VMEM((2, 8, ROWS), f32),
-        square_in=pltpu.VMEM((N_Y, 8, ROWS), f32),
-        passed=pltpu.VMEM((2, ROWS // 2, VALUE_CHANNELS), bf16),
-        q_send=dma((6,)),
-        q_recv=dma((6,)),
-        up_send=dma((N_Z // 2, 2)),
-        up_recv=dma((N_Z // 2, 2)),
-        down_send=dma((N_Z // 2, 2)),
-        down_recv=dma((N_Z // 2, 2)),
-        part_send=dma((N_X - 1,)),
-        part_recv=dma((N_X - 1,)),
-        stat_send=dma((N_X - 1,)),
-        stat_recv=dma((N_X - 1,)),
-        first_send=dma((N_X - 1,)),
-        first_recv=dma((N_X - 1,)),
-        column_send=dma((N_Z,)),
-        column_recv=dma((N_Z,)),
-        start_send=dma((N_X - 1,)),
-        start_recv=dma((N_X - 1,)),
-        square_send=dma((N_Y,)),
-        square_recv=dma((N_Y,)),
-        passed_send=dma((2, 2)),
-        passed_recv=dma((2, 2)),
-        out_memory=pltpu.VMEM((M_V, depth), bf16),
-        out_attend=pltpu.VMEM((VALUE_CHANNELS, depth), bf16),
-        to_core=pltpu.VMEM((2, N_Y, SHARE, depth // 2), bf16),
-        from_core=pltpu.VMEM((2, N_Y, SHARE, depth // 2), bf16),
-        sums=pltpu.VMEM((2, N_Y, SHARE, depth // 2), f32),
-        passing=pltpu.VMEM((6, SHARE, depth // 2), bf16),
-        from_below=pltpu.VMEM((2, SHARE, depth // 2), bf16),
-        from_above=pltpu.VMEM((2, SHARE, depth // 2), bf16),
-        relay_in=pltpu.VMEM((2, SHARE, depth // 2), bf16),
-        core_send=dma((2,)),
-        core_recv=dma((2,)),
-        relay_send=dma((2,)),
-        relay_recv=dma((2,)),
-        out_up_send=dma((2,)),
-        out_up_recv=dma((2,)),
-        out_down_send=dma((2,)),
-        out_down_recv=dma((2,)),
-    )
-
-
-def layer_kernel(names, *refs):
-    at = dict(zip(names, refs))
+    between = (
+        pltpu.VMEM((ROWS, VALUE_CHANNELS), bf16),
+        pltpu.VMEM((ROWS, M_V), bf16),
+        pltpu.VMEM((ROWS, mem_width), bf16),
+        pltpu.VMEM((8, ROWS), f32),
+        pltpu.VMEM((ROWS, 256), bf16),
+        pltpu.VMEM((ROWS * 5 // 2, 128), bf16),
+        pltpu.VMEM((M_V, depth), bf16),
+        pltpu.VMEM((VALUE_CHANNELS, depth), bf16),
+        dma((2,)),
+    )
+    for_project = (
+        pltpu.VMEM((N_Y * N_C, SHARE, depth), bf16),
+        pltpu.VMEM((N_Y * N_C, ROWS * 3 // 2, 128), bf16),
+        pltpu.VMEM((256, depth), bf16),
+        pltpu.VMEM((8, depth), bf16),
+        pltpu.VMEM((8, depth), bf16),
+        pltpu.VMEM((depth, mem_width), bf16),
+        pltpu.VMEM((PLAIN_CHANNELS + ROTARY_CHANNELS, QUERY_LATENT), bf16),
+        pltpu.VMEM((LATENT_WIDTH, PLAIN_CHANNELS), bf16),
+        pltpu.VMEM((LATENT_WIDTH, VALUE_CHANNELS), bf16),
+        pltpu.VMEM((SHARE, depth), bf16),
+        pltpu.VMEM((1, ROWS), f32),
+        pltpu.VMEM((2, 8, ROWS), f32),
+        pltpu.VMEM((1024, PLAIN_CHANNELS + ROTARY_CHANNELS), bf16),
+        pltpu.VMEM((1024, 256), bf16),
+        pltpu.VMEM((ROWS, 1024), bf16),
+        pltpu.VMEM((ROWS, 1024), bf16),
+        dma((16,)),
+        dma((11,)),
+        dma((11,)),
+        dma((11,)),
+        dma((11,)),
+    )
+    for_attend = (
+        pltpu.VMEM((N_X, ROWS, 256), bf16),
+        pltpu.VMEM((N_Z, ROWS * 5 // 2, 128), bf16),
+        pltpu.VMEM((ROWS, 256), bf16),
+        pltpu.VMEM((N_X * ROWS, 128), f32),
+        pltpu.VMEM((N_X * ROWS, 128), f32),
+        pltpu.VMEM((N_X * ROWS, VALUE_CHANNELS), f32),
+        pltpu.VMEM((N_X - 1, ROWS, VALUE_CHANNELS), bf16),
+        pltpu.VMEM((N_X - 1, 8, ROWS), f32),
+        pltpu.VMEM((N_X - 1, ROWS, VALUE_CHANNELS), bf16),
+        pltpu.VMEM((N_X - 1, 8, ROWS), f32),
+        pltpu.VMEM((ROWS, M_V), f32),
+        pltpu.VMEM((ROWS, 128), f32),
+        pltpu.VMEM((ROWS, 128), f32),
+        pltpu.VMEM((N_X, STATE_ROWS, M_V), f32),
+        pltpu.VMEM((N_X, STATE_ROWS, M_V), f32),
+        pltpu.VMEM((STATE_ROWS, M_V), f32),
+        pltpu.VMEM((N_Z, STATE_ROWS, M_V), f32),
+        pltpu.VMEM((N_X, STATE_ROWS, M_V), f32),
+        pltpu.VMEM((N_X, STATE_ROWS, M_V), f32),
+        pltpu.VMEM((2, 8, ROWS), f32),
+        pltpu.VMEM((N_Y, 8, ROWS), f32),
+        pltpu.VMEM((2, ROWS // 2, VALUE_CHANNELS), bf16),
+        dma((6,)),
+        dma((6,)),
+        dma((N_Z // 2, 2)),
+        dma((N_Z // 2, 2)),
+        dma((N_Z // 2, 2)),
+        dma((N_Z // 2, 2)),
+        dma((N_X - 1,)),
+        dma((N_X - 1,)),
+        dma((N_X - 1,)),
+        dma((N_X - 1,)),
+        dma((N_X - 1,)),
+        dma((N_X - 1,)),
+        dma((N_Z,)),
+        dma((N_Z,)),
+        dma((N_X - 1,)),
+        dma((N_X - 1,)),
+        dma((N_Y,)),
+        dma((N_Y,)),
+        dma((2, 2)),
+        dma((2, 2)),
+    )
+    for_output = (
+        pltpu.VMEM((2, N_Y, SHARE, depth // 2), bf16),
+        pltpu.VMEM((2, N_Y, SHARE, depth // 2), bf16),
+        pltpu.VMEM((2, N_Y, SHARE, depth // 2), f32),
+        pltpu.VMEM((6, SHARE, depth // 2), bf16),
+        pltpu.VMEM((2, SHARE, depth // 2), bf16),
+        pltpu.VMEM((2, SHARE, depth // 2), bf16),
+        pltpu.VMEM((2, SHARE, depth // 2), bf16),
+        dma((2,)),
+        dma((2,)),
+        dma((2,)),
+        dma((2,)),
+        dma((2,)),
+        dma((2,)),
+        dma((2,)),
+        dma((2,)),
+    )
+    return between, for_project, for_attend, for_output
+
+
+N_INPUTS = 22
+N_PROJECT_INPUTS = 19
+IN_VMEM = (1, 2, 3, 4, 5, 19)
+
+
+def layer_kernel(counts, *refs):
     y, c = lax.axis_index("y"), lax.axis_index("c")
     z, x = lax.axis_index("z"), lax.axis_index("x")
+    project_inputs = refs[:N_PROJECT_INPUTS]
+    mem_gain, out_memory_hbm, out_attend_hbm, out_ref = refs[N_PROJECT_INPUTS : N_INPUTS + 1]
+    groups, at = [], N_INPUTS + 1
+    for count in counts:
+        groups.append(refs[at : at + count])
+        at += count
+    between, for_project, for_attend, for_output = groups
+    attended, gated, mem, gates, queries, keys_values, out_memory, out_attend, out_sem = between
+
     barrier = pltpu.get_barrier_semaphore()
     devices = [{"c": 1 - c}]
     devices += [{"y": lax.rem(y + d, N_Y)} for d in range(1, N_Y)]
@@ -1097,159 +1100,47 @@
     for device in devices:
         pl.semaphore_signal(barrier, inc=1, device_id=device, device_id_type=MESH_ID)
     loads = [
-        pltpu.make_async_copy(at[name + "_hbm"], at[name], at["load_sem"].at[14 + k])
-        for k, name in enumerate(("out_memory", "out_attend"))
+        pltpu.make_async_copy(out_memory_hbm, out_memory, out_sem.at[0]),
+        pltpu.make_async_copy(out_attend_hbm, out_attend, out_sem.at[1]),
     ]
+    attending = attend_phase(
+        queries, keys_values, mem, gates, mem_gain, attended, gated, *for_attend
+    )
     started = project_phase(
         lambda: pl.semaphore_wait(barrier, len(devices)),
-        *(at[name] for name in PROJECT_REFS),
+        lambda: next(attending),
+        lambda: next(attending),
+        *project_inputs,
+        mem,
+        gates,
+        queries,
+        keys_values,
+        *for_project,
     )
     for load in loads:
         load.start()
-    more, finish_columns = attend_phase(*(at[name] for name in ATTEND_REFS))
+    more, finish_columns = next(attending)
     started += more
     for load in loads:
         load.wait()
-    started += output_phase(*(at[name] for name in OUTPUT_REFS))
+    started += output_phase(gated, attended, out_memory, out_attend, out_ref, *for_output)
     for copy in started:
         copy.wait_send()
     finish_columns()
 
 
-PROJECT_REFS = (
-    "tokens_hbm",
-    "input_gain",
-    "query_gain",
-    "latent_gain",
-    "cosine",
-    "sine_part",
-    "shift_hbm",
-    "narrow_query",
-    "narrow_latent",
-    "narrow_rotary",
-    "narrow_ingate",
-    "narrow_forget",
-    "query_hbm",
-    "key_hbm",
-    "value_hbm",
-    "outgate_hbm",
-    "query_up_hbm",
-    "key_up_hbm",
-    "value_up_hbm",
-    "mem_ref",
-    "gate_ref",
-    "q_ref",
-    "kv_ref",
-    "rows_all",
-    "latents",
-    "small",
-    "ingate",
-    "forget",
-    "big",
-    "query_up",
-    "key_up",
-    "value_up",
-    "tokens",
-    "shift_row",
-    "pre_gates",
-    "up_query",
-    "up_latent",
-    "wide_query",
-    "wide_latent",
-    "load_sem",
-    "row_send",
-    "row_recv",
-    "lat_send",
-    "lat_recv",
-)
-ATTEND_REFS = (
-    "q_ref",
-    "kv_ref",
-    "mem_ref",
-    "gate_ref",
-    "mem_gain",
-    "attended_ref",
-    "gated_ref",
-    "q_all",
-    "kv_all",
-    "k_cat",
-    "top",
-    "total",
-    "accum",
-    "part_out",
-    "stat_out",
-    "part_in",
-    "stat_in",
-    "cell",
-    "cell_sum",
-    "cell_top",
-    "first_out",
-    "first_in",
-    "column_out",
-    "column_in",
-    "start_out",
-    "start_in",
-    "square_out",
-    "square_in",
-    "passed",
-    "q_send",
-    "q_recv",
-    "up_send",
-    "up_recv",
-    "down_send",
-    "down_recv",
-    "part_send",
-    "part_recv",
-    "stat_send",
-    "stat_recv",
-    "first_send",
-    "first_recv",
-    "column_send",
-    "column_recv",
-    "start_send",
-    "start_recv",
-    "square_send",
-    "square_recv",
-    "passed_send",
-    "passed_recv",
-)
-OUTPUT_REFS = (
-    "gated_ref",
-    "attended_ref",
-    "out_memory",
-    "out_attend",
-    "o_ref",
-    "to_core",
-    "from_core",
-    "sums",
-    "passing",
-    "from_below",
-    "from_above",
-    "relay_in",
-    "core_send",
-    "core_recv",
-    "relay_send",
-    "relay_recv",
-    "out_up_send",
-    "out_up_recv",
-    "out_down_send",
-    "out_down_recv",
-)
-
-
 def layer(*inputs):
     depth = inputs[0].shape[1]
-    mem_width = sum(one.shape[1] for one in inputs[7:11])
-    made = scratch(depth, mem_width)
-    names = (*INPUTS, "o_ref", *made)
+    mem_width = 2 * M_QK + 2 * M_V
+    groups = scratch(depth, mem_width)
     vmem = pl.BlockSpec(memory_space=pltpu.VMEM)
     hbm = pl.BlockSpec(memory_space=pltpu.HBM)
     return pl.pallas_call(
-        functools.partial(layer_kernel, names),
+        functools.partial(layer_kernel, tuple(len(group) for group in groups)),
         out_shape=jax.ShapeDtypeStruct((SHARE, depth), jnp.bfloat16),
-        in_specs=[hbm] * HBM_INPUTS + [vmem] * (len(inputs) - HBM_INPUTS),
+        in_specs=[vmem if k in IN_VMEM else hbm for k in range(N_INPUTS)],
         out_specs=vmem,
-        scratch_shapes=list(made.values()),
+        scratch_shapes=[one for group in groups for one in group],
         compiler_params=pltpu.CompilerParams(
             collective_id=1, has_side_effects=True, vmem_limit_bytes=67_000_000
         ),
@@ -1286,10 +1177,14 @@
     positions = lax.axis_index(SP) * length + jnp.arange(length, dtype=jnp.int32)
     halfway = ROTARY_CHANNELS // 2
     inverse = jnp.power(ROTARY_BASE, -jnp.arange(halfway, dtype=jnp.float32) / halfway)
-    angles = positions.astype(jnp.float32)[:, None] * inverse
-    cosine, sine_part = (jnp.tile(made, (1, 4)) for made in (jnp.cos(angles), jnp.sin(angles)))
+    angles = positions.astype(jnp.float32)[None, :] * inverse[:, None]
     return layer(
         tokens,
+        input_gain,
+        query_gain,
+        latent_gain,
+        jnp.cos(angles),
+        jnp.sin(angles),
         forget_shift.T,
         query_down_weight.T,
         latent_down_weight.T,
@@ -1303,14 +1198,9 @@
         query_up_weight.T,
         key_up_weight,
         value_up_weight,
+        mem_gain,
         out_memory,
         out_attend,
-        input_gain,
-        query_gain,
-        latent_gain,
-        mem_gain,
-        cosine,
-        sine_part,
     )
 
 

time: 104 us -> 96.3 us (0.926)
  Pallas kernels: 100 us -> 93 us
  local copies, waits for them, and re-layouts: 3.37 us -> 1.67 us
    pallas_call x1, Pallas kernels: 100 us -> 93 us  [layer(): pl.pallas_call(functools.partial(layer_kernel, tuple((len(group) for grou...]
    another operation x4 -> x0, local copies, waits for them, and re-layouts: 1.7 us -> none  [per_device(): jnp.tile(made, (1, 4))]
where the time goes in v5:
time: 96.3 us; the launch traced here: 95.6 us
  Pallas kernels  93 us (97%)
  local copies, waits for them, and re-layouts  1.67 us (2%)
  other arithmetic  0.97 us (1%)
    pallas_call x1, Pallas kernels, layer(): pl.pallas_call(functools.partial(layer_kernel, tuple((len(group) for grou...  93 us

profile of v5, /device:TPU:224, one launch (start us, length us, event | category | flops | bytes accessed | tf_op | source)
XLA Modules:
  0.0 95.6 jit_solution(15307583065643728976)
XLA Ops:
  0.0 1.0 multiply_sine_fusion
  1.0 93.0 %layer.1 = bf16[64,2048]{1,0:T(8,128)(2,1)} custom-call(bf16[64,2048]{1,0:T(8,128)(2,1)} %refs_0_.1, bf16[2048]{0:T(1024)(128)(2,1)} %refs_1_.1, f32[768]{0:T(1024)} %refs_2_.1, f32[512]{0:T(512)} %refs_3_.1, f32[32,512]{1,0:T(8,128)} %get-tuple-element.6.refs_4_, f32[32,512]{1,0:T(8,128)} %get-tuple-element.5.refs_5_, f32[1,512]{1,0:T(1,128)} %bitcast.13, ...), custom_call_target="tpu_custom_call" | custom-call | flops 8000000000 | bytes 20000000 | tf_op jit(solution)/shard_map/layer/pallas_call | solution.py:1138
  93.9 1.7 %copy.22 = bf16[64,2048]{1,0:T(8,128)(2,1)} copy(bf16[64,2048]{1,0:T(8,128)(2,1)} %layer.1) | data formatting | bytes 524288
  (2 shorter events, 0.0 us)

commit v6 on v5

--- a/solution.py
+++ b/solution.py
@@ -309,6 +309,8 @@
     for h in range(2):
         for up in (True, False):
             start(kv_copy(up, 1, h))
+    yield
+
     top[...] = jnp.full(top.shape, FAR_BELOW, f32)
     total[...] = jnp.zeros(total.shape, f32)
     for number in (0, 3, 1, 2):
@@ -595,6 +597,7 @@
     greeted,
     after_gates,
     after_exchange,
+    after_keys,
     tokens_hbm,
     gain,
     query_gain,
@@ -619,6 +622,7 @@
     q_ref,
     kv_ref,
     rows_all,
+    query_latents,
     latents,
     small,
     ingate,
@@ -639,6 +643,8 @@
     row_recv,
     lat_send,
     lat_recv,
+    query_send,
+    query_recv,
 ):
     f32, bf16 = jnp.float32, jnp.bfloat16
     y, c = lax.axis_index("y"), lax.axis_index("c")
@@ -734,7 +740,7 @@
             at = QUERY_PART + 16 * k
             pre_gates[k, :, rows] = turned[at : at + 8]
         rounded = made.astype(bf16)
-        latents[mine, rows] = rounded[:, :width]
+        query_latents[mine, rows] = rounded[:, :width]
         wide_latent[rows, :width] = rounded[:, width:]
 
     def project_big():
@@ -760,9 +766,11 @@
     both = duplicated(second, 0)
     half = ROWS // 2
     packed = jnp.where(lane < LATENT_PART, both[:half], both[half:])
-    latents[mine, ROWS:] = packed.astype(bf16)
+    latents[mine] = packed.astype(bf16)
     exchange = TpGather(latents, lat_send, lat_recv)
+    query_exchange = TpGather(query_latents, query_send, query_recv)
     exchange.start()
+    query_exchange.start()
     project_big()
     heads = lax.broadcasted_iota(jnp.int32, (8, ROWS), 0) == mine
     in_pre, forget_pre = (
@@ -787,8 +795,9 @@
     )
     top_rows = lax.broadcasted_iota(jnp.int32, (8, ROWS), 0) == 0
     gate_ref[...] = jnp.where(top_rows, in_gate - cumulative, cumulative)
+    after_gates()
     exchange.relay()
-    after_gates()
+    query_exchange.relay()
     key_turned = rotated(second, LATENT_PART)
     kv_ref[2 * ROWS :] = jnp.where(
         lane < ROTARY_CHANNELS, key_turned[:half], key_turned[half:]
@@ -797,39 +806,28 @@
     after_exchange()
     exchange.far()
 
-    query_mask = (lane < QUERY_PART).astype(f32)
-    squares = jnp.zeros((ROWS, width), f32)
-    low_squares = jnp.zeros((half, width), f32)
+    squares = jnp.zeros((half, width), f32)
     for s in range(N_Y * N_C):
-        part = latents[s, :ROWS].astype(f32) * query_mask
+        part = latents[s].astype(f32)
         squares = squares + part * part
-        part = latents[s, ROWS:].astype(f32)
-        low_squares = low_squares + part * part
-    query_scale = lax.rsqrt(
-        jnp.sum(squares, axis=1, keepdims=True) / QUERY_LATENT + SMALL_CONSTANT
-    )
     low = lane < LATENT_PART
-    low_scale = lax.rsqrt(
-        jnp.sum(jnp.where(low, low_squares, 0.0), axis=1, keepdims=True) / LATENT_WIDTH
-        + SMALL_CONSTANT
-    )
-    high_scale = lax.rsqrt(
-        jnp.sum(jnp.where(low, 0.0, low_squares), axis=1, keepdims=True) / LATENT_WIDTH
-        + SMALL_CONSTANT
+    low_scale, high_scale = (
+        lax.rsqrt(
+            jnp.sum(jnp.where(low == first, squares, 0.0), axis=1, keepdims=True) / LATENT_WIDTH
+            + SMALL_CONSTANT
+        )
+        for first in (True, False)
     )
     latent_scale = jnp.where(low, low_scale, high_scale)
     query_gains = jnp.broadcast_to(query_gain[...].reshape(1, -1), (8, QUERY_LATENT))
     latent_gains = jnp.broadcast_to(latent_gain[...].reshape(1, -1), (8, LATENT_WIDTH))
 
     def latent_gain_of(s):
-        pair = latent_gains[:1, (s // 2) * width : (s // 2 + 1) * width]
-        turned = pltpu.roll(latent_gains, LATENT_PART, 1)
-        other = turned[:1, (s // 2) * width : (s // 2 + 1) * width]
-        if s % 2:
-            other = pltpu.roll(latent_gains, LATENT_WIDTH - LATENT_PART, 1)
-            other = other[:1, (s // 2) * width : (s // 2 + 1) * width]
-            return jnp.where(low, other, pair)
-        return jnp.where(low, pair, other)
+        pair = slice((s // 2) * width, (s // 2 + 1) * width)
+        shift = LATENT_WIDTH - LATENT_PART if s % 2 else LATENT_PART
+        here = latent_gains[:1, pair]
+        other = pltpu.roll(latent_gains, shift, 1)[:1, pair]
+        return jnp.where(low, other, here) if s % 2 else jnp.where(low, here, other)
 
     def query_gain_of(s):
         turned = query_gains
@@ -839,20 +837,34 @@
 
     for s in range(N_Y * N_C):
         columns = slice(s * width, (s + 1) * width)
-        part = latents[s, :ROWS].astype(f32) * query_mask
-        wide_query[:, columns] = (part * query_scale * query_gain_of(s)).astype(bf16)
-        part = latents[s, ROWS:].astype(f32)
+        part = latents[s].astype(f32)
         made = (part * latent_scale * latent_gain_of(s)).astype(bf16)
         wide_latent[:half, columns] = jnp.where(low, made, jnp.zeros_like(made))
         wide_latent[half:, columns] = jnp.where(low, jnp.zeros_like(made), made)
     made = jnp.dot(wide_latent[...], up_latent[...], preferred_element_type=f32).astype(bf16)
     kv_ref[:ROWS] = made[:, :width]
     kv_ref[ROWS : 2 * ROWS] = made[:, width:]
+    after_keys()
+
+    query_exchange.near()
+    query_exchange.far()
+    query_mask = (lane < QUERY_PART).astype(f32)
+    squares = jnp.zeros((ROWS, width), f32)
+    for s in range(N_Y * N_C):
+        part = query_latents[s].astype(f32) * query_mask
+        squares = squares + part * part
+    query_scale = lax.rsqrt(
+        jnp.sum(squares, axis=1, keepdims=True) / QUERY_LATENT + SMALL_CONSTANT
+    )
+    for s in range(N_Y * N_C):
+        columns = slice(s * width, (s + 1) * width)
+        part = query_latents[s].astype(f32) * query_mask
+        wide_query[:, columns] = (part * query_scale * query_gain_of(s)).astype(bf16)
     made = jnp.dot(wide_query[...], up_query[...], preferred_element_type=f32).astype(bf16)
     q_ref[:, :width] = made[:, :width]
     turning = jnp.concatenate([made[:, width:], jnp.zeros((ROWS, ROTARY_CHANNELS), bf16)], axis=1)
     q_ref[:, width:] = rotated(turning, 0).astype(bf16)
-    return gather.started + exchange.started
+    return gather.started + exchange.started + query_exchange.started
 
 
 def output_phase(
@@ -990,7 +1002,8 @@
     )
     for_project = (
         pltpu.VMEM((N_Y * N_C, SHARE, depth), bf16),
-        pltpu.VMEM((N_Y * N_C, ROWS * 3 // 2, 128), bf16),
+        pltpu.VMEM((N_Y * N_C, ROWS, 128), bf16),
+        pltpu.VMEM((N_Y * N_C, ROWS // 2, 128), bf16),
         pltpu.VMEM((256, depth), bf16),
         pltpu.VMEM((8, depth), bf16),
         pltpu.VMEM((8, depth), bf16),
@@ -1006,6 +1019,8 @@
         pltpu.VMEM((ROWS, 1024), bf16),
         pltpu.VMEM((ROWS, 1024), bf16),
         dma((16,)),
+        dma((11,)),
+        dma((11,)),
         dma((11,)),
         dma((11,)),
         dma((11,)),
@@ -1108,8 +1123,7 @@
     )
     started = project_phase(
         lambda: pl.semaphore_wait(barrier, len(devices)),
-        lambda: next(attending),
-        lambda: next(attending),
+        *[lambda: next(attending)] * 3,
         *project_inputs,
         mem,
         gates,

time: 96.3 us -> 93.6 us (0.972)
  Pallas kernels: 93 us -> 90.5 us
    pallas_call x1, Pallas kernels: 93 us -> 90.5 us  [layer(): pl.pallas_call(functools.partial(layer_kernel, tuple((len(group) for grou...]
where the time goes in v6:
time: 93.6 us; the launch traced here: 93.1 us
  Pallas kernels  90.5 us (97%)
  local copies, waits for them, and re-layouts  1.67 us (2%)
  other arithmetic  0.97 us (1%)
    pallas_call x1, Pallas kernels, layer(): pl.pallas_call(functools.partial(layer_kernel, tuple((len(group) for grou...  90.5 us

profile of v6, /device:TPU:224, one launch (start us, length us, event | category | flops | bytes accessed | tf_op | source)
XLA Modules:
  0.0 93.1 jit_solution(1104840367884045237)
XLA Ops:
  0.0 1.0 %multiply_sine_fusion = (f32[32,512]{1,0:T(8,128)}, f32[32,512]{1,0:T(8,128)}) fusion(f32[32]{0:T(128)S(1)} %multiply_power_fusion, f32[512]{0:T(512)S(1)} %add_convert_fusion), kind=kLoop, calls=%fused_computation | loop fusion | flops 16384 | bytes 133248 | tf_op jit(solution)/shard_map/sin | solution.py:1201
  1.0 90.5 %layer.1 = bf16[64,2048]{1,0:T(8,128)(2,1)} custom-call(bf16[64,2048]{1,0:T(8,128)(2,1)} %refs_0_.1, bf16[2048]{0:T(1024)(128)(2,1)} %refs_1_.1, f32[768]{0:T(1024)} %refs_2_.1, f32[512]{0:T(512)} %refs_3_.1, f32[32,512]{1,0:T(8,128)} %get-tuple-element.6.refs_4_, f32[32,512]{1,0:T(8,128)} %get-tuple-element.5.refs_5_, f32[1,512]{1,0:T(1,128)} %bitcast.13, ...), custom_call_target="tpu_custom_call" | custom-call | flops 8000000000 | bytes 20000000 | tf_op jit(solution)/shard_map/layer/pallas_call | solution.py:1152
  91.5 1.7 %copy.22 = bf16[64,2048]{1,0:T(8,128)(2,1)} copy(bf16[64,2048]{1,0:T(8,128)(2,1)} %layer.1) | data formatting | bytes 524288
  (2 shorter events, 0.0 us)

commit v7 on v6

--- a/solution.py
+++ b/solution.py
@@ -387,6 +387,7 @@
     own_values = lambda: kv_ref[ROWS : 2 * ROWS]
     attend_rows(x * steps, (x + 1) * steps, own_values, True)
 
+    take(1, 0)
     q_copy(0).wait_recv()
     start(q_copy(4))
     q_copy(3).wait_recv()
@@ -404,11 +405,10 @@
     for d in range(N_X - 1):
         start(start_copy(d))
     start_in[x] = start_out[x]
-    take(1, 0)
+    take(1, 1)
     for number in (1, 2, 4, 5):
         q_copy(number).wait_recv()
     attend_rows((x + 1) * steps, N_X * steps, own_values, False)
-    take(1, 1)
     take(2, 0)
     use_up(1)
     take(2, 1)
@@ -456,6 +456,8 @@
     gated = cell[...] * twice(as_columns(inverse, width)) * gain_ref[pl.ds(pl.multiple_of(me_tp * M_V, M_V), M_V)].astype(f32).reshape(1, M_V)
     gated = gated * jax.nn.sigmoid(mem_ref[:, 2 * M_QK + M_V :].astype(f32))
     gated_ref[...] = gated.astype(bf16)
+    yield
+
     take(4, 0)
     take(4, 1)
 
@@ -873,6 +875,7 @@
     out_memory,
     out_attend,
     o_ref,
+    kept,
     to_core,
     from_core,
     sums,
@@ -910,12 +913,25 @@
         picked = [ref[pl.ds(pl.multiple_of((k * N_C + core) * SHARE, SHARE), SHARE)] for k in range(N_Y)]
         return jnp.concatenate(picked, axis=0)
 
-    def partial(core, h, store):
-        memory_rows, attend_rows = rows_of(gated, core), rows_of(attended, core)
+    def columns_of(h, t):
+        return slice(h * half + t * tile, h * half + (t + 1) * tile)
+
+    for k, core in enumerate((1 - c, c)):
+        memory_rows = rows_of(gated, core)
+        for h in range(2):
+            for t in range(half // tile):
+                kept[k, h, :, t * tile : (t + 1) * tile] = jnp.dot(
+                    memory_rows, out_memory[:, columns_of(h, t)], preferred_element_type=f32
+                )
+    yield
+
+    def partial(k, h, store):
+        attend_rows = rows_of(attended, c if k else 1 - c)
         for t in range(half // tile):
-            columns = slice(h * half + t * tile, h * half + (t + 1) * tile)
-            made = jnp.dot(memory_rows, out_memory[:, columns], preferred_element_type=f32)
-            made = made + jnp.dot(attend_rows, out_attend[:, columns], preferred_element_type=f32)
+            made = jnp.dot(
+                attend_rows, out_attend[:, columns_of(h, t)], preferred_element_type=f32
+            )
+            made = kept[k, h, :, t * tile : (t + 1) * tile] + made
             store(t * tile, made.astype(bf16).reshape(N_Y, SHARE, tile))
 
     def core_copy(h):
@@ -953,14 +969,14 @@
         def keep(at, block, h=h):
             to_core[h, :, :, at : at + tile] = block
 
-        partial(1 - c, h, keep)
+        partial(0, h, keep)
         start(core_copy(h))
     for h in range(2):
 
         def keep(at, block, h=h):
             sums[h, :, :, at : at + tile] = block.astype(f32)
 
-        partial(c, h, keep)
+        partial(1, h, keep)
     for h in range(2):
         core_copy(h).wait_recv()
         sums[h] = sums[h] + from_core[h].astype(f32)
@@ -982,8 +998,8 @@
         up_copy(h).wait_recv()
         down_copy(h).wait_recv()
         made = sums[h, y] + from_below[h].astype(f32) + from_above[h].astype(f32)
-        o_ref[:, h * half : (h + 1) * half] = made.astype(bf16)
-    return started
+        o_ref[:, h * half : (h + 1) * half] = made
+    yield started
 
 
 def scratch(depth, mem_width):
@@ -1071,6 +1087,7 @@
         dma((2, 2)),
     )
     for_output = (
+        pltpu.VMEM((2, 2, N_Y * SHARE, depth // 2), f32),
         pltpu.VMEM((2, N_Y, SHARE, depth // 2), bf16),
         pltpu.VMEM((2, N_Y, SHARE, depth // 2), bf16),
         pltpu.VMEM((2, N_Y, SHARE, depth // 2), f32),
@@ -1133,11 +1150,14 @@
     )
     for load in loads:
         load.start()
+    outputting = output_phase(gated, attended, out_memory, out_attend, out_ref, *for_output)
+    next(attending)
+    for load in loads:
+        load.wait()
+    next(outputting)
     more, finish_columns = next(attending)
     started += more
-    for load in loads:
-        load.wait()
-    started += output_phase(gated, attended, out_memory, out_attend, out_ref, *for_output)
+    started += next(outputting)
     for copy in started:
         copy.wait_send()
     finish_columns()
@@ -1151,7 +1171,7 @@
     hbm = pl.BlockSpec(memory_space=pltpu.HBM)
     return pl.pallas_call(
         functools.partial(layer_kernel, tuple(len(group) for group in groups)),
-        out_shape=jax.ShapeDtypeStruct((SHARE, depth), jnp.bfloat16),
+        out_shape=jax.ShapeDtypeStruct((SHARE, depth), jnp.float32),
         in_specs=[vmem if k in IN_VMEM else hbm for k in range(N_INPUTS)],
         out_specs=vmem,
         scratch_shapes=[one for group in groups for one in group],
@@ -1192,7 +1212,7 @@
     halfway = ROTARY_CHANNELS // 2
     inverse = jnp.power(ROTARY_BASE, -jnp.arange(halfway, dtype=jnp.float32) / halfway)
     angles = positions.astype(jnp.float32)[None, :] * inverse[:, None]
-    return layer(
+    mixed = layer(
         tokens,
         input_gain,
         query_gain,
@@ -1216,6 +1236,7 @@
         out_memory,
         out_attend,
     )
+    return mixed.astype(jnp.bfloat16)
 
 
 def solution(mesh):

time: 93.6 us -> 94.1 us (level)
  other arithmetic: 0.97 us -> 2.76 us
  local copies, waits for them, and re-layouts: 1.67 us -> 0 us
    convert_element_type x0 -> x1, other arithmetic: none -> 1.77 us  [per_device(): return mixed.astype(jnp.bfloat16)]
    unnamed x1 -> x0, local copies, waits for them, and re-layouts: 1.67 us -> none
where the time goes in v7:
time: 94.1 us; the launch traced here: 93.1 us
  Pallas kernels  90.4 us (96%)
  other arithmetic  2.76 us (3%)
    pallas_call x1, Pallas kernels, layer(): pl.pallas_call(functools.partial(layer_kernel, tuple((len(group) for grou...  90.4 us

profile of v7, /device:TPU:224, one launch (start us, length us, event | category | flops | bytes accessed | tf_op | source)
XLA Modules:
  0.0 93.1 jit_solution(17401703555763210777)
XLA Ops:
  0.0 1.0 %multiply_sine_fusion = (f32[32,512]{1,0:T(8,128)}, f32[32,512]{1,0:T(8,128)}) fusion(f32[32]{0:T(128)S(1)} %multiply_power_fusion, f32[512]{0:T(512)S(1)} %add_convert_fusion), kind=kLoop, calls=%fused_computation | loop fusion | flops 16384 | bytes 133248 | tf_op jit(solution)/shard_map/sin | solution.py:1221
  1.0 90.4 %layer.1 = f32[64,2048]{1,0:T(8,128)} custom-call(bf16[64,2048]{1,0:T(8,128)(2,1)} %refs_0_.1, bf16[2048]{0:T(1024)(128)(2,1)} %refs_1_.1, f32[768]{0:T(1024)} %refs_2_.1, f32[512]{0:T(512)} %refs_3_.1, f32[32,512]{1,0:T(8,128)} %get-tuple-element.6.refs_4_, f32[32,512]{1,0:T(8,128)} %get-tuple-element.5.refs_5_, f32[1,512]{1,0:T(1,128)} %bitcast.13, ...), custom_call_target="tpu_custom_call" | custom-call | flops 8000000000 | bytes 20000000 | tf_op jit(solution)/shard_map/layer/pallas_call | solution.py:1172
  91.4 1.8 %convert_element_type.11 = bf16[64,2048]{1,0:T(8,128)(2,1)} convert(f32[64,2048]{1,0:T(8,128)} %layer.1) | non-fusion elementwise | flops 131072 | bytes 786432 | tf_op jit(solution)/shard_map/convert_element_type | solution.py:1239
  (2 shorter events, 0.0 us)

commit v8 on v7

--- a/solution.py
+++ b/solution.py
@@ -409,10 +409,11 @@
     for number in (1, 2, 4, 5):
         q_copy(number).wait_recv()
     attend_rows((x + 1) * steps, N_X * steps, own_values, False)
+    use_up(1)
     take(2, 0)
-    use_up(1)
+    use_down(1)
     take(2, 1)
-    use_down(1)
+    use_up(2)
 
     for d in range(N_X - 1):
         start_copy(d).wait_recv()
@@ -438,25 +439,14 @@
     start(square_copy(0))
 
     take(3, 0)
-    use_up(2)
+    use_down(2)
     square_copy(0).wait_recv()
     square_out[1] = square_out[0] + square_in[0]
     for number in range(1, N_Y):
         start(square_copy(number))
     take(3, 1)
-    use_down(2)
     use_up(3)
     use_down(3)
-
-    squares = square_out[1]
-    for number in range(1, N_Y):
-        square_copy(number).wait_recv()
-        squares = squares + square_in[number]
-    inverse = lax.rsqrt(squares[:1] / (MEMORY_HEADS * M_V) + SMALL_CONSTANT)
-    gated = cell[...] * twice(as_columns(inverse, width)) * gain_ref[pl.ds(pl.multiple_of(me_tp * M_V, M_V), M_V)].astype(f32).reshape(1, M_V)
-    gated = gated * jax.nn.sigmoid(mem_ref[:, 2 * M_QK + M_V :].astype(f32))
-    gated_ref[...] = gated.astype(bf16)
-    yield
 
     take(4, 0)
     take(4, 1)
@@ -496,9 +486,19 @@
         start(stat_copy(d))
     own, own_log = finish(x)
 
+    squares = square_out[1]
+    for number in range(1, N_Y):
+        square_copy(number).wait_recv()
+        squares = squares + square_in[number]
+    inverse = lax.rsqrt(squares[:1] / (MEMORY_HEADS * M_V) + SMALL_CONSTANT)
+    gated = cell[...] * twice(as_columns(inverse, width)) * gain_ref[pl.ds(pl.multiple_of(me_tp * M_V, M_V), M_V)].astype(f32).reshape(1, M_V)
+    gated = gated * jax.nn.sigmoid(mem_ref[:, 2 * M_QK + M_V :].astype(f32))
+    gated_ref[...] = gated.astype(bf16)
     for h in range(2):
         far_copy(h, 0).wait_recv()
         start(far_copy(h, 1))
+    yield
+
 
     logs = []
     for d in range(N_X - 1):
@@ -998,7 +998,7 @@
         up_copy(h).wait_recv()
         down_copy(h).wait_recv()
         made = sums[h, y] + from_below[h].astype(f32) + from_above[h].astype(f32)
-        o_ref[:, h * half : (h + 1) * half] = made
+        o_ref[:, h * half : (h + 1) * half] = made.astype(bf16)
     yield started
 
 
@@ -1171,7 +1171,7 @@
     hbm = pl.BlockSpec(memory_space=pltpu.HBM)
     return pl.pallas_call(
         functools.partial(layer_kernel, tuple(len(group) for group in groups)),
-        out_shape=jax.ShapeDtypeStruct((SHARE, depth), jnp.float32),
+        out_shape=jax.ShapeDtypeStruct((SHARE, depth), jnp.bfloat16),
         in_specs=[vmem if k in IN_VMEM else hbm for k in range(N_INPUTS)],
         out_specs=vmem,
         scratch_shapes=[one for group in groups for one in group],
@@ -1212,7 +1212,7 @@
     halfway = ROTARY_CHANNELS // 2
     inverse = jnp.power(ROTARY_BASE, -jnp.arange(halfway, dtype=jnp.float32) / halfway)
     angles = positions.astype(jnp.float32)[None, :] * inverse[:, None]
-    mixed = layer(
+    return layer(
         tokens,
         input_gain,
         query_gain,
@@ -1236,7 +1236,6 @@
         out_memory,
         out_attend,
     )
-    return mixed.astype(jnp.bfloat16)
 
 
 def solution(mesh):

time: 94.1 us -> 92.2 us (0.980)
  Pallas kernels: 90.4 us -> 87.7 us
  other arithmetic: 2.76 us -> 0.97 us
  local copies, waits for them, and re-layouts: 0 us -> 1.67 us
    pallas_call x1, Pallas kernels: 90.4 us -> 87.7 us  [layer(): pl.pallas_call(functools.partial(layer_kernel, tuple((len(group) for grou...]
    convert_element_type x1 -> x0, other arithmetic: 1.77 us -> none  [per_device(): return mixed.astype(jnp.bfloat16)]
    unnamed x0 -> x1, local copies, waits for them, and re-layouts: none -> 1.67 us
where the time goes in v8:
time: 92.2 us; the launch traced here: 90.4 us
  Pallas kernels  87.7 us (95%)
  local copies, waits for them, and re-layouts  1.67 us (2%)
  other arithmetic  0.97 us (1%)
    pallas_call x1, Pallas kernels, layer(): pl.pallas_call(functools.partial(layer_kernel, tuple((len(group) for grou...  87.7 us

profile of v8, /device:TPU:224, one launch (start us, length us, event | category | flops | bytes accessed | tf_op | source)
XLA Modules:
  0.0 90.4 jit_solution(6705982726260086666)
XLA Ops:
  0.0 1.0 %multiply_sine_fusion = (f32[32,512]{1,0:T(8,128)}, f32[32,512]{1,0:T(8,128)}) fusion(f32[32]{0:T(128)S(1)} %multiply_power_fusion, f32[512]{0:T(512)S(1)} %add_convert_fusion), kind=kLoop, calls=%fused_computation | loop fusion | flops 16384 | bytes 133248 | tf_op jit(solution)/shard_map/sin | solution.py:1221
  1.0 87.7 %layer.1 = bf16[64,2048]{1,0:T(8,128)(2,1)} custom-call(bf16[64,2048]{1,0:T(8,128)(2,1)} %refs_0_.1, bf16[2048]{0:T(1024)(128)(2,1)} %refs_1_.1, f32[768]{0:T(1024)} %refs_2_.1, f32[512]{0:T(512)} %refs_3_.1, f32[32,512]{1,0:T(8,128)} %get-tuple-element.6.refs_4_, f32[32,512]{1,0:T(8,128)} %get-tuple-element.5.refs_5_, f32[1,512]{1,0:T(1,128)} %bitcast.13, ...), custom_call_target="tpu_custom_call" | custom-call | flops 8000000000 | bytes 20000000 | tf_op jit(solution)/shard_map/layer/pallas_call | solution.py:1172
  88.7 1.7 %copy.22 = bf16[64,2048]{1,0:T(8,128)(2,1)} copy(bf16[64,2048]{1,0:T(8,128)(2,1)} %layer.1) | data formatting | bytes 524288
  (2 shorter events, 0.0 us)

commit v9 on v8

--- a/solution.py
+++ b/solution.py
@@ -41,6 +41,9 @@
 CHUNK = M_QK // N_X
 TALL = 512
 GROUP = 1
+TURNED = 128
+KEYS_AT, VALUES_AT = TURNED, TURNED + ROWS
+TURNED_AT = TURNED + 2 * ROWS
 STATE_ROWS = CHUNK + 8
 NORMAL_ROW, TOP_ROW, DECAY_ROW = CHUNK, CHUNK + 1, CHUNK + 2
 
@@ -114,6 +117,8 @@
     square_recv,
     passed_send,
     passed_recv,
+    turned_send,
+    turned_recv,
 ):
     f32, bf16 = jnp.float32, jnp.bfloat16
     z, x = lax.axis_index("z"), lax.axis_index("x")
@@ -123,7 +128,7 @@
     right, left = peers[0], peers[-1]
     rows_y = [lax.rem(y + d, N_Y) for d in range(1, N_Y)]
     me_tp = y * N_C + c
-    half = kv_ref.shape[0] // 2
+    half = (TURNED + 2 * ROWS) // 2
     width = PLAIN_CHANNELS
 
     def remote(source, target, send, recv, device):
@@ -139,7 +144,7 @@
     def kv_copy(up, step, h):
         shift = (N_Z - step + 1) if up else (step - 1)
         owner = lax.rem(z + shift, N_Z)
-        rows = pl.ds(h * half, half)
+        rows = pl.ds(pl.multiple_of(c * TURNED + h * half, 64), half)
         source = kv_ref.at[rows] if step == 1 else kv_all.at[owner, rows]
         send, recv = (up_send, up_recv) if up else (down_send, down_recv)
         return remote(
@@ -148,6 +153,17 @@
             send.at[step - 1, h],
             recv.at[step - 1, h],
             {"z": above if up else below},
+        )
+
+    def turned_copy(step, up):
+        owner = lax.rem(z + (N_Z - step if up else step), N_Z)
+        rows = pl.ds(pl.multiple_of(c * TURNED_AT, TURNED), TURNED)
+        return remote(
+            kv_all.at[owner, rows],
+            kv_all.at[owner, rows],
+            turned_send.at[step - 1, int(up)],
+            turned_recv.at[step - 1, int(up)],
+            {"c": 1 - c},
         )
 
     q_half = ROWS // 2
@@ -318,16 +334,16 @@
     accum[...] = jnp.zeros(accum.shape, f32)
     q_all[x] = q_ref[...]
 
-    lane = lax.broadcasted_iota(jnp.int32, (ROWS // 2, width), 1)
+    lane = lax.broadcasted_iota(jnp.int32, (TURNED, width), 1)
     low = (lane < ROTARY_CHANNELS).astype(bf16)
     high = (lane >= ROTARY_CHANNELS).astype(bf16)
     scale = LOG2E * (PLAIN_CHANNELS + ROTARY_CHANNELS) ** (-0.5)
 
     def keys_from(ref):
-        k_cat[:, :width] = ref[:ROWS]
-        packed = ref[2 * ROWS :]
-        k_cat[: ROWS // 2, width:] = packed * low
-        k_cat[ROWS // 2 :, width:] = packed * high
+        k_cat[:, :width] = ref[KEYS_AT : KEYS_AT + ROWS]
+        for k, mask in enumerate((low, low, high, high)):
+            at = TURNED_AT if k % 2 else 0
+            k_cat[k * TURNED : (k + 1) * TURNED, width:] = ref[at : at + TURNED] * mask
 
     def attend_tile(t, keys, values, masked):
         shard = t // (ROWS // TALL)
@@ -367,7 +383,7 @@
         @pl.when(useful)
         def _():
             keys_from(kv_all.at[owner])
-            attend_rows(0, N_X * steps, lambda: kv_all[owner, ROWS : 2 * ROWS], False)
+            attend_rows(0, N_X * steps, lambda: kv_all[owner, VALUES_AT : VALUES_AT + ROWS], False)
 
     def take(step, h):
         for up in (True, False):
@@ -376,15 +392,21 @@
             kv_copy(up, step, h).wait_recv()
             if step < last - 1 or (step == last - 1 and up == (h == 0)):
                 start(kv_copy(up, step + 1, h))
+        if h == 1:
+            for up in (True, False):
+                if step < last or up:
+                    start(turned_copy(step, up))
 
     def use_up(step):
+        turned_copy(step, True).wait_recv()
         arrived(lax.rem(z + N_Z - step, N_Z), z >= step)
 
     def use_down(step):
+        turned_copy(step, False).wait_recv()
         arrived(lax.rem(z + step, N_Z), z + step >= N_Z)
 
     keys_from(kv_ref)
-    own_values = lambda: kv_ref[ROWS : 2 * ROWS]
+    own_values = lambda: kv_ref[VALUES_AT : VALUES_AT + ROWS]
     attend_rows(x * steps, (x + 1) * steps, own_values, True)
 
     take(1, 0)
@@ -450,6 +472,7 @@
 
     take(4, 0)
     take(4, 1)
+    turned_copy(last, True).wait_recv()
 
     opposite = lax.rem(z + last, N_Z)
 
@@ -463,7 +486,7 @@
             attend_rows(
                 shard * steps,
                 (shard + 1) * steps,
-                lambda: kv_all[opposite, ROWS : 2 * ROWS],
+                lambda: kv_all[opposite, VALUES_AT : VALUES_AT + ROWS],
                 False,
             )
 
@@ -801,9 +824,11 @@
     exchange.relay()
     query_exchange.relay()
     key_turned = rotated(second, LATENT_PART)
-    kv_ref[2 * ROWS :] = jnp.where(
+    key_turned = jnp.where(
         lane < ROTARY_CHANNELS, key_turned[:half], key_turned[half:]
     ).astype(bf16)
+    kv_ref[:TURNED] = key_turned[:TURNED]
+    kv_ref[TURNED_AT:] = key_turned[TURNED:]
     exchange.near()
     after_exchange()
     exchange.far()
@@ -844,8 +869,8 @@
         wide_latent[:half, columns] = jnp.where(low, made, jnp.zeros_like(made))
         wide_latent[half:, columns] = jnp.where(low, jnp.zeros_like(made), made)
     made = jnp.dot(wide_latent[...], up_latent[...], preferred_element_type=f32).astype(bf16)
-    kv_ref[:ROWS] = made[:, :width]
-    kv_ref[ROWS : 2 * ROWS] = made[:, width:]
+    kv_ref[KEYS_AT : KEYS_AT + ROWS] = made[:, :width]
+    kv_ref[VALUES_AT : VALUES_AT + ROWS] = made[:, width:]
     after_keys()
 
     query_exchange.near()
@@ -1085,6 +1110,8 @@
         dma((N_Y,)),
         dma((2, 2)),
         dma((2, 2)),
+        dma((N_Z // 2, 2)),
+        dma((N_Z // 2, 2)),
     )
     for_output = (
         pltpu.VMEM((2, 2, N_Y * SHARE, depth // 2), f32),

time: 92.2 us -> 93.6 us (1.015)
  Pallas kernels: 87.7 us -> 89.4 us
    pallas_call x1, Pallas kernels: 87.7 us -> 89.4 us  [layer(): pl.pallas_call(functools.partial(layer_kernel, tuple((len(group) for grou...]
where the time goes in v9:
time: 93.6 us; the launch traced here: 92.1 us
  Pallas kernels  89.4 us (96%)
  local copies, waits for them, and re-layouts  1.67 us (2%)
  other arithmetic  0.97 us (1%)
    pallas_call x1, Pallas kernels, layer(): pl.pallas_call(functools.partial(layer_kernel, tuple((len(group) for grou...  89.4 us

profile of v9, /device:TPU:224, one launch (start us, length us, event | category | flops | bytes accessed | tf_op | source)
XLA Modules:
  0.0 92.1 jit_solution(18102197810314802414)
XLA Ops:
  0.0 1.0 %multiply_sine_fusion = (f32[32,512]{1,0:T(8,128)}, f32[32,512]{1,0:T(8,128)}) fusion(f32[32]{0:T(128)S(1)} %multiply_power_fusion, f32[512]{0:T(512)S(1)} %add_convert_fusion), kind=kLoop, calls=%fused_computation | loop fusion | flops 16384 | bytes 133248 | tf_op jit(solution)/shard_map/sin | solution.py:1248
  1.0 89.4 %layer.1 = bf16[64,2048]{1,0:T(8,128)(2,1)} custom-call(bf16[64,2048]{1,0:T(8,128)(2,1)} %refs_0_.1, bf16[2048]{0:T(1024)(128)(2,1)} %refs_1_.1, f32[768]{0:T(1024)} %refs_2_.1, f32[512]{0:T(512)} %refs_3_.1, f32[32,512]{1,0:T(8,128)} %get-tuple-element.6.refs_4_, f32[32,512]{1,0:T(8,128)} %get-tuple-element.5.refs_5_, f32[1,512]{1,0:T(1,128)} %bitcast.13, ...), custom_call_target="tpu_custom_call" | custom-call | flops 8000000000 | bytes 20000000 | tf_op jit(solution)/shard_map/layer/pallas_call | solution.py:1199
  90.4 1.7 %copy.22 = bf16[64,2048]{1,0:T(8,128)(2,1)} copy(bf16[64,2048]{1,0:T(8,128)(2,1)} %layer.1) | data formatting | bytes 524288
  (2 shorter events, 0.0 us)

commit v10 on v8

--- a/solution.py
+++ b/solution.py
@@ -797,8 +797,8 @@
     )
     top_rows = lax.broadcasted_iota(jnp.int32, (8, ROWS), 0) == 0
     gate_ref[...] = jnp.where(top_rows, in_gate - cumulative, cumulative)
+    exchange.relay()
     after_gates()
-    exchange.relay()
     query_exchange.relay()
     key_turned = rotated(second, LATENT_PART)
     kv_ref[2 * ROWS :] = jnp.where(

time: 92.2 us -> 92.1 us (level)
  no operation moved by 1% of the time
where the time goes in v10:
time: 92.1 us; the launch traced here: 90.5 us
  Pallas kernels  87.9 us (95%)
  local copies, waits for them, and re-layouts  1.67 us (2%)
  other arithmetic  0.97 us (1%)
    pallas_call x1, Pallas kernels, layer(): pl.pallas_call(functools.partial(layer_kernel, tuple((len(group) for grou...  87.9 us

profile of v10, /device:TPU:224, one launch (start us, length us, event | category | flops | bytes accessed | tf_op | source)
XLA Modules:
  0.0 90.5 jit_solution(13788856793371860423)
XLA Ops:
  0.0 1.0 %multiply_sine_fusion = (f32[32,512]{1,0:T(8,128)}, f32[32,512]{1,0:T(8,128)}) fusion(f32[32]{0:T(128)S(1)} %multiply_power_fusion, f32[512]{0:T(512)S(1)} %add_convert_fusion), kind=kLoop, calls=%fused_computation | loop fusion | flops 16384 | bytes 133248 | tf_op jit(solution)/shard_map/sin | solution.py:1221
  1.0 87.9 %layer.1 = bf16[64,2048]{1,0:T(8,128)(2,1)} custom-call(bf16[64,2048]{1,0:T(8,128)(2,1)} %refs_0_.1, bf16[2048]{0:T(1024)(128)(2,1)} %refs_1_.1, f32[768]{0:T(1024)} %refs_2_.1, f32[512]{0:T(512)} %refs_3_.1, f32[32,512]{1,0:T(8,128)} %get-tuple-element.6.refs_4_, f32[32,512]{1,0:T(8,128)} %get-tuple-element.5.refs_5_, f32[1,512]{1,0:T(1,128)} %bitcast.13, ...), custom_call_target="tpu_custom_call" | custom-call | flops 8000000000 | bytes 20000000 | tf_op jit(solution)/shard_map/layer/pallas_call | solution.py:1172
  88.9 1.7 %copy.22 = bf16[64,2048]{1,0:T(8,128)(2,1)} copy(bf16[64,2048]{1,0:T(8,128)(2,1)} %layer.1) | data formatting | bytes 524288
  (2 shorter events, 0.0 us)
